TPU v7x, 256 devices: a whole 4x4x8 slice. The times are simulated.
256 devices in a mesh: sp: 32 (over z, x), tp: 4 (over y), dp: 2 (over core).
Axes of the slice: x: 4, y: 4, z: 8, core: 2. Of those that a mesh axis runs over, the one named last changes fastest.
Arguments:
- latent: bfloat16 [2, 16384, 2048], P('dp', ('sp', 'tp')), may hold values from -6 to 6
- condition: float32 [2, 2048], P('dp'), may hold values from -6 to 6
- context: bfloat16 [2, 1024, 2048], P('dp', 'sp'), may hold values from -6 to 6
- context_cond: float32 [2048], replicated, may hold values from -6 to 6
- shift_matrix: bfloat16 [2048, 2048], P(('sp', 'tp')), may hold values from -0.125 to 0.125
- scale_matrix: bfloat16 [2048, 2048], P(('sp', 'tp')), may hold values from -0.125 to 0.125
- gate_matrix: bfloat16 [2048, 2048], P(('sp', 'tp')), may hold values from -0.125 to 0.125
- value_proj: bfloat16 [2048, 2048], P(None, 'tp'), may hold values from -0.125 to 0.125
- gate_proj: bfloat16 [2048, 2048], P(None, 'tp'), may hold values from -0.125 to 0.125
- write_proj: bfloat16 [2048, 1024], P(None, 'tp'), may hold values from -0.125 to 0.125
- read_proj: bfloat16 [2048, 1024], P(None, 'tp'), may hold values from -0.125 to 0.125
- step_proj: bfloat16 [2048, 2, 32], replicated, may hold values from -0.125 to 0.125
- decay_rate: float32 [2, 32], replicated, may hold values from 3.0456543e-05 to 0.0601
- pacing: float32 [2, 16384], P('dp'), may hold values from 0.2 to 4.3
- value_taps: float32 [5, 2048], replicated, may hold values from -2.5 to 2.5
- write_taps: float32 [5, 1024], replicated, may hold values from -2.5 to 2.5
- read_taps: float32 [5, 1024], replicated, may hold values from -2.5 to 2.5
- norm_gain: float32 [2048], replicated, may hold values from 0.1 to 1.9
- out_proj: bfloat16 [2048, 2048], P('tp'), may hold values from -0.125 to 0.125
Outputs:
- updated: bfloat16 [2, 16384, 2048], P('dp', ('sp', 'tp'))
All inputs are finite; a program needn't handle non-finite values.
Results may differ from a plain program's by a relative error of at most 0.006.
Values may be sent and summed in bfloat16 or wider, within the bound.
A program may use at most 128 MiB of HBM per device.

v0:
```python
import jax
import jax.numpy as jnp
from jax import lax
from jax.sharding import Mesh
from jax.sharding import PartitionSpec as P

HEAD = 64
STATE = 128
ROW = 64
BLOCK = 128
SP = ("sp_0", "sp_1")
SP_TP = ("sp_0", "sp_1", "tp")


NORM_FLOOR = 1e-05
GATED_FLOOR = 1e-06


def over_axes(value, axes):
    for axis in axes:
        value = lax.psum(value, axis)
    return value


def sent_together(arrays, axis, dim, along):
    widths = [a.shape[along] for a in arrays]
    both = jnp.concatenate(arrays, axis=along)
    result = lax.all_gather(both, axis, axis=dim, tiled=True)
    return tuple(jnp.split(result, [sum(widths[:k]) for k in range(1, len(widths))], axis=along))


def cut_along(value, dim, length):
    dims = value.shape
    pieces = value.reshape(*dims[:dim], length, dims[dim] // length, *dims[dim + 1 :])
    return jnp.moveaxis(pieces, dim, 0)


def sum_at_owner(value, axis, dim):
    pieces = cut_along(value, dim, lax.axis_size(axis))
    arrived = lax.all_to_all(pieces, axis, split_axis=0, concat_axis=0, tiled=True)
    return arrived.astype(jnp.float32).sum(axis=0)


def masked_exp(exponent, allowed):
    return jnp.where(allowed, jnp.exp(jnp.where(allowed, exponent, 0.0)), 0.0)


def modulate(row_block, shift_row, scale_row):
    values = row_block.astype(jnp.float32)
    center = jnp.mean(values, -1, keepdims=True)
    spread = jnp.mean(jnp.square(values - center), -1, keepdims=True)
    normed = (values - center) * lax.rsqrt(spread + NORM_FLOOR)
    return (normed * (1.0 + shift_row * 0.0 + scale_row) + shift_row).astype(jnp.bfloat16)


def convolve(values, kernel, run_count):
    length, channels = values.shape
    tap_count = kernel.shape[0]
    margin = tap_count // 2
    stretch = length // run_count
    blocked = values.astype(jnp.float32).reshape(run_count, stretch, channels)
    padded = jnp.pad(blocked, ((0, 0), (margin, margin), (0, 0)))
    summed = jnp.zeros_like(blocked)
    for offset in range(tap_count):
        summed = summed + padded[:, offset : offset + stretch] * kernel[offset]
    return jax.nn.silu(summed).reshape(length, channels).astype(jnp.bfloat16)


def context_state(values, writes, weight, groups):
    length = values.shape[0]
    per_group = weight.shape[1] // groups
    scaled = (
        writes.reshape(length, groups, 1, STATE) * weight.reshape(length, groups, per_group, 1)
    ).astype(jnp.bfloat16)
    head_values = values.reshape(length, groups, per_group, HEAD)
    return jnp.einsum("lgrn,lgrp->grnp", scaled, head_values, preferred_element_type=jnp.float32)


def block_inputs(values, writes, decays, steps, groups):
    length = values.shape[0]
    per_group = decays.shape[1] // groups
    blocks = length // BLOCK
    head_values = values.reshape(blocks, BLOCK, groups, per_group, HEAD)
    write_rows = writes.reshape(blocks, BLOCK, groups, STATE)
    cumulative = jnp.cumsum(decays.reshape(blocks, BLOCK, groups, per_group), axis=1)
    step_rows = steps.reshape(blocks, BLOCK, groups, per_group)
    weight = jnp.exp(cumulative[:, -1:] - cumulative) * step_rows
    scaled = (write_rows[:, :, :, None, :] * weight[..., None]).astype(jnp.bfloat16)
    increment = jnp.einsum(
        "kqgrn,kqgrp->kgrnp", scaled, head_values, preferred_element_type=jnp.float32
    )

    def advance(carry_state, paired):
        block_decay, block_increment = paired
        return (jnp.exp(block_decay)[..., None, None] * carry_state + block_increment, carry_state)

    empty_state = jnp.zeros(increment.shape[1:], jnp.float32)
    final_state, before = lax.scan(advance, empty_state, (cumulative[:, -1], increment))
    return (cumulative, final_state, before)


def block_outputs(values, reads, affinity, cumulative, steps, before, start):
    blocks, block_rows, groups, per_group = cumulative.shape
    head_values = values.reshape(blocks, block_rows, groups, per_group, HEAD)
    read_rows = reads.reshape(blocks, block_rows, groups, STATE).astype(jnp.float32)
    step_rows = steps.reshape(blocks, block_rows, groups, per_group)
    lower_mask = jnp.tril(jnp.ones((block_rows, block_rows), bool))[:, :, None, None]
    exponent = cumulative[:, :, None] - cumulative[:, None, :]
    mixing = (affinity[..., None] * masked_exp(exponent, lower_mask) * step_rows[:, None]).astype(
        jnp.bfloat16
    )
    within = jnp.einsum(
        "ktsgr,ksgrp->ktgrp", mixing, head_values, preferred_element_type=jnp.float32
    )
    block_decay = cumulative[:, -1]
    earlier = jnp.cumsum(block_decay, axis=0) - block_decay
    entering = before + jnp.exp(earlier)[..., None, None] * start[None]
    carried = jnp.einsum("ktgn,kgrnp->ktgrp", read_rows, entering) * jnp.exp(cumulative)[..., None]
    return (within + carried).reshape(blocks * block_rows, groups * per_group * HEAD)


def per_device(
    latent,
    condition,
    context,
    context_cond,
    shift_matrix,
    scale_matrix,
    gate_matrix,
    value_proj,
    gate_proj,
    write_proj,
    read_proj,
    step_proj,
    decay_rate,
    pacing,
    value_taps,
    write_taps,
    read_taps,
    norm_gain,
    out_proj,
):
    sp_count = lax.axis_size(SP)
    sp_index = lax.axis_index(SP)
    tp_index = lax.axis_index("tp")
    model_width = latent.shape[2]
    width_dev = value_proj.shape[1]
    keys_dev = write_proj.shape[1]
    heads_dev = width_dev // HEAD
    groups_dev = keys_dev // STATE
    state_shape = (groups_dev, heads_dev // groups_dev, STATE, HEAD)
    row_share = shift_matrix.shape[0]
    activated = jax.nn.silu(jnp.stack([condition[0], context_cond])).astype(jnp.bfloat16)
    own_cols = lax.dynamic_slice_in_dim(
        activated, (sp_index * lax.axis_size("tp") + tp_index) * row_share, row_share, 1
    )
    shift_part = jnp.dot(own_cols, shift_matrix, preferred_element_type=jnp.float32)
    scale_part = jnp.dot(own_cols, scale_matrix, preferred_element_type=jnp.float32)
    gate_part = jnp.dot(own_cols[:1], gate_matrix, preferred_element_type=jnp.float32)
    shifts, scales, gate_row = (
        over_axes(shift_part, SP_TP),
        over_axes(scale_part, SP_TP),
        over_axes(gate_part, SP_TP),
    )
    step_cols = lax.dynamic_slice_in_dim(step_proj, tp_index * heads_dev, heads_dev, 2).reshape(
        model_width, 2 * heads_dev
    )
    own_rows = modulate(latent[0], shifts[0], scales[0])
    row_piece = lax.all_gather(own_rows, "tp", axis=0, tiled=True)
    projected = jnp.concatenate(
        [
            jnp.dot(row_piece, value_proj, preferred_element_type=jnp.float32),
            jnp.dot(row_piece, gate_proj, preferred_element_type=jnp.float32),
            jnp.dot(row_piece, write_proj, preferred_element_type=jnp.float32),
            jnp.dot(row_piece, read_proj, preferred_element_type=jnp.float32),
            jnp.dot(row_piece, step_cols, preferred_element_type=jnp.float32),
        ],
        axis=1,
    )
    tokens = projected.shape[0]
    run_count = tokens // ROW
    gate_end = 2 * width_dev
    write_end = gate_end + keys_dev
    read_end = write_end + keys_dev
    value_kernel = lax.dynamic_slice_in_dim(value_taps, tp_index * width_dev, width_dev, 1)
    write_kernel = lax.dynamic_slice_in_dim(write_taps, tp_index * keys_dev, keys_dev, 1)
    read_kernel = lax.dynamic_slice_in_dim(read_taps, tp_index * keys_dev, keys_dev, 1)
    values = convolve(projected[:, :width_dev].astype(jnp.bfloat16), value_kernel, run_count)
    gate_pre = projected[:, width_dev:gate_end].astype(jnp.bfloat16)
    writes = convolve(
        projected[:, gate_end:write_end].astype(jnp.bfloat16), write_kernel, run_count
    )
    reads = convolve(projected[:, write_end:read_end].astype(jnp.bfloat16), read_kernel, run_count)
    step_raw = projected[:, read_end:].astype(jnp.bfloat16)
    latent_raw = (
        lax.optimization_barrier(step_raw).astype(jnp.float32).reshape(tokens, 2, heads_dev)
    )
    rates = lax.dynamic_slice_in_dim(decay_rate, tp_index * heads_dev, heads_dev, 1)
    local_pace = lax.dynamic_slice_in_dim(pacing[0], sp_index * tokens, tokens, 0)
    forward_step = jax.nn.softplus(latent_raw[:, 0]) * local_pace[:, None]
    forward_decay = -rates[0][None, :] * forward_step
    backward_step = jax.nn.softplus(latent_raw[:, 1]) * local_pace[:, None]
    backward_decay = -rates[1][None, :] * backward_step
    forward_cumul, forward_end, forward_before = block_inputs(
        values, writes, forward_decay, forward_step, groups_dev
    )
    backward_cumul, backward_end, backward_before = block_inputs(
        values[::-1], writes[::-1], backward_decay[::-1], backward_step[::-1], groups_dev
    )
    context_hidden = modulate(context[0], shifts[1], scales[1])
    context_value = jnp.dot(context_hidden, value_proj, preferred_element_type=jnp.float32).astype(
        jnp.bfloat16
    )
    context_write = jnp.dot(context_hidden, write_proj, preferred_element_type=jnp.float32).astype(
        jnp.bfloat16
    )
    context_raw = jnp.dot(context_hidden, step_cols, preferred_element_type=jnp.float32).astype(
        jnp.bfloat16
    )
    ctx_value_all, ctx_write_all, ctx_raw_all, latent_raw_all = (
        *sent_together((context_value, context_write, context_raw), SP, 0, 1),
        lax.all_gather(step_raw, SP, axis=0, tiled=True),
    )
    ctx_values = convolve(ctx_value_all, value_kernel, 1)
    ctx_writes = convolve(ctx_write_all, write_kernel, 1)
    ctx_raw = lax.optimization_barrier(ctx_raw_all).astype(jnp.float32).reshape(-1, 2, heads_dev)
    ctx_fwd_step = jax.nn.softplus(ctx_raw[:, 0])
    ctx_fwd_decay = -rates[0][None, :] * ctx_fwd_step
    ctx_cumul = jnp.cumsum(ctx_fwd_decay, axis=0)
    ctx_forward = context_state(
        ctx_values, ctx_writes, jnp.exp(ctx_cumul[-1:] - ctx_cumul) * ctx_fwd_step, groups_dev
    )
    ctx_bwd_step = jax.nn.softplus(ctx_raw[:, 1])
    ctx_bwd_decay = -rates[1][None, :] * ctx_bwd_step
    ctx_back_cumul = jnp.cumsum(ctx_bwd_decay, axis=0)
    ctx_backward = context_state(
        ctx_values, ctx_writes, jnp.exp(ctx_back_cumul - ctx_bwd_decay) * ctx_bwd_step, groups_dev
    )
    ctx_forward = ctx_forward.reshape(heads_dev, STATE, HEAD)
    ctx_backward = ctx_backward.reshape(heads_dev, STATE, HEAD)
    empty_state = jnp.zeros((heads_dev, STATE, HEAD), jnp.float32)
    all_raw = (
        lax.optimization_barrier(latent_raw_all)
        .astype(jnp.float32)
        .reshape(sp_count, tokens, 2, heads_dev)
    )
    all_steps = jax.nn.softplus(all_raw) * pacing[0].reshape(sp_count, tokens)[:, :, None, None]
    totals = jnp.sum(-rates[None, None] * all_steps, axis=1)
    forward_totals = totals[:, 0]
    backward_totals = totals[:, 1]
    forward_prefix = jnp.cumsum(forward_totals, axis=0) - forward_totals
    backward_suffix = jnp.cumsum(backward_totals[::-1], axis=0)[::-1] - backward_totals
    forward_through = forward_prefix + forward_totals
    backward_through = backward_suffix + backward_totals
    own_prefix = forward_prefix[sp_index]
    own_suffix = backward_suffix[sp_index]
    forward_piece, backward_piece = tuple(
        (
            part.astype(jnp.float32)
            for part in sent_together(
                (
                    forward_end.reshape(1, heads_dev, STATE, HEAD).astype(jnp.bfloat16),
                    backward_end.reshape(1, heads_dev, STATE, HEAD).astype(jnp.bfloat16),
                ),
                SP,
                0,
                1,
            )
        )
    )
    shard_count = forward_piece.shape[0]
    sources = jnp.arange(shard_count)
    forward_gap = own_prefix[None] - forward_through
    backward_gap = own_suffix[None] - backward_through
    forward_weight = masked_exp(forward_gap, (sources < sp_index)[:, None])
    backward_weight = masked_exp(backward_gap, (sources > sp_index)[:, None])
    forward_in = empty_state + jnp.sum(forward_weight[:, :, None, None] * forward_piece, axis=0)
    backward_in = empty_state + jnp.sum(backward_weight[:, :, None, None] * backward_piece, axis=0)
    forward_start = forward_in + jnp.exp(own_prefix)[:, None, None] * ctx_forward
    backward_start = backward_in + jnp.exp(own_suffix)[:, None, None] * ctx_backward
    blocks = tokens // BLOCK
    forward_affinity = jnp.einsum(
        "ktgn,ksgn->ktsg",
        reads.reshape(blocks, BLOCK, groups_dev, STATE),
        writes.reshape(blocks, BLOCK, groups_dev, STATE),
        preferred_element_type=jnp.float32,
    )
    backward_affinity = forward_affinity[::-1, ::-1, ::-1]
    forward_out = block_outputs(
        values,
        reads,
        forward_affinity,
        forward_cumul,
        forward_step,
        forward_before,
        forward_start.reshape(state_shape),
    )
    backward_out = block_outputs(
        values[::-1],
        reads[::-1],
        backward_affinity,
        backward_cumul,
        backward_step[::-1],
        backward_before,
        backward_start.reshape(state_shape),
    )[::-1]
    gated_heads = (forward_out + backward_out) * jax.nn.silu(gate_pre.astype(jnp.float32))
    grouped = gated_heads.reshape(tokens, groups_dev, -1)
    grouped = grouped * lax.rsqrt(jnp.mean(grouped * grouped, -1, keepdims=True) + GATED_FLOOR)
    gain_dev = lax.dynamic_slice_in_dim(norm_gain, tp_index * width_dev, width_dev, 0)
    inner_rows = (grouped.reshape(tokens, width_dev) * gain_dev).astype(jnp.bfloat16)
    mixed = sum_at_owner(
        jnp.dot(inner_rows, out_proj, preferred_element_type=jnp.float32).astype(jnp.bfloat16),
        "tp",
        0,
    ).astype(jnp.bfloat16)
    updated = (
        latent[0].astype(jnp.float32)
        + gate_row[0] * lax.optimization_barrier(mixed).astype(jnp.float32)
    ).astype(jnp.bfloat16)
    return updated[None]


def solution(mesh):
    torus = Mesh(
        mesh.devices.reshape(8, 4, mesh.shape["tp"], mesh.shape["dp"]), ("sp_0", "sp_1", "tp", "dp")
    )
    placed = (
        P("dp", SP_TP, None),
        P("dp", None),
        P("dp", SP, None),
        P(),
        P(SP_TP, None),
        P(SP_TP, None),
        P(SP_TP, None),
        P(None, "tp"),
        P(None, "tp"),
        P(None, "tp"),
        P(None, "tp"),
        P(),
        P(),
        P("dp", None),
        P(),
        P(),
        P(),
        P(),
        P("tp", None),
    )
    return jax.shard_map(
        per_device, mesh=torus, in_specs=placed, out_specs=P("dp", SP_TP, None), check_vma=False
    )
```

profile of v0, /device:TPU:8, one launch (start us, length us, event | category | flops | bytes accessed | tf_op | source)
XLA Modules:
  0.0 367.3 jit_solution(16203024841715670939)
XLA Ops:
  13.0 33.2 %all-reduce.5 = (f32[2,2048]{1,0:T(2,128)S(1)}, f32[2,2048]{1,0:T(2,128)S(1)}, f32[1,2048]{1,0:T(1,128)S(1)}) all-reduce(f32[2,2048]{1,0:T(2,128)S(1)} %fusion.172, f32[2,2048]{1,0:T(2,128)S(1)} %fusion.173, f32[1,2048]{1,0:T(1,128)S(1)} %fusion.153), channel_id=1, replica_groups=mesh['sp_0'=8,'sp_1'=4,'tp'=4,'dp'=2] {'sp_0'}, use_global_device_ids=true, to_apply=%region_5.6 | all-reduce | flops 10240 | bytes 81920 | tf_op jit(solution)/shard_map/psum | solution.py:21
  46.1 17.4 %all-reduce.7 = (f32[2,2048]{1,0:T(2,128)S(1)}, f32[2,2048]{1,0:T(2,128)S(1)}, f32[1,2048]{1,0:T(1,128)S(1)}) all-reduce(f32[2,2048]{1,0:T(2,128)S(1)} %get-tuple-element.183, f32[2,2048]{1,0:T(2,128)S(1)} %get-tuple-element.184, f32[1,2048]{1,0:T(1,128)S(1)} %get-tuple-element.185), channel_id=1, replica_groups=mesh['sp_0'=8,'sp_1'=4,'tp'=4,'dp'=2] {'sp_1'}, use_global_device_ids=true, to_apply=%region_6.7 | all-reduce | flops 10240 | bytes 81920 | tf_op jit(solution)/shard_map/psum | solution.py:21
  63.5 15.2 %all-reduce.6 = (f32[2,2048]{1,0:T(2,128)S(1)}, f32[2,2048]{1,0:T(2,128)S(1)}, f32[2048]{0:T(1024)}) all-reduce(f32[2,2048]{1,0:T(2,128)S(1)} %get-tuple-element.189, f32[2,2048]{1,0:T(2,128)S(1)} %get-tuple-element.190, f32[2048]{0:T(1024)S(1)} %bitcast.366), channel_id=1, replica_groups=mesh['sp_0'=8,'sp_1'=4,'tp'=4,'dp'=2] {'tp'}, use_global_device_ids=true, to_apply=%region_7.8 | all-reduce | flops 10240 | bytes 81920 | tf_op jit(solution)/shard_map/psum | solution.py:21
  91.0 20.2 %all-gather.4.cloned.1.call-done = bf16[512,2048]{1,0:T(8,128)(2,1)} async-done(((bf16[128,2048]{1,0:T(8,128)(2,1)}), bf16[512,2048]{1,0:T(8,128)(2,1)}) %all-gather.4.cloned.1.call-update) | async-done | bytes 2097168 | tf_op jit(solution)/shard_map/all_gather | solution.py:169
  118.4 2.7 fusion.169
  122.3 3.5 convolution_convert_fusion.2
  127.6 8.3 %rev.32 = bf16[512,512]{1,0:T(8,128)(2,1)} reverse(bf16[512,512]{1,0:T(8,128)(2,1)} %bitcast.310), dimensions={0} | reverse | bytes 1048576 | tf_op jit(solution)/shard_map/rev | solution.py:208
  135.9 2.9 reshape.563
  144.2 2.6 rev.30
  150.0 3.6 fusion.75
  155.2 8.1 %while.27 = (s32[]{:T(128)}, f32[2,4,128,64]{3,2,1,0:T(8,128)S(1)}, f32[4,2,4,128,64]{4,3,2,1,0:T(8,128)}, f32[4,2,4]{2,1,0:T(2,128)S(1)}, f32[4,2,4,128,64]{4,3,2,1,0:T(8,128)}, /*index=5*/s32[]{:T(128)}, s32[]{:T(128)}) while((s32[]{:T(128)}, f32[2,4,128,64]{3,2,1,0:T(8,128)S(1)}, f32[4,2,4,128,64]{4,3,2,1,0:T(8,128)}, ...), condition=%wide.region_19.20_spmd.clone, body=%wide.region_18.19_spmd.clone.sunk | while | flops 262147 | bytes 1573568 | solution.py:98
  169.6 2.9 reshape.562
  182.2 10.8 %while.26 = (s32[]{:T(128)}, f32[2,4,128,64]{3,2,1,0:T(8,128)S(1)}, f32[4,2,4,128,64]{4,3,2,1,0:T(8,128)}, f32[4,2,4]{2,1,0:T(2,128)}, f32[4,2,4,128,64]{4,3,2,1,0:T(8,128)}, /*index=5*/s32[]{:T(128)}, s32[]{:T(128)}) while((s32[]{:T(128)}, f32[2,4,128,64]{3,2,1,0:T(8,128)S(1)}, f32[4,2,4,128,64]{4,3,2,1,0:T(8,128)}, ...), condition=%wide.region_13.14_spmd.clone, body=%wide.region_12.13_spmd.clone.sunk | while | flops 262147 | bytes 1573568 | solution.py:98
  211.6 2.8 fusion.118
  214.4 2.7 reshape.555
  220.4 3.8 %multiply_convert_fusion.5 = bf16[1,1024,512]{1,2,0:T(8,128)(2,1)} fusion(f32[1,1024,512]{1,2,0:T(8,128)S(1)} %convert_bitcast_fusion, bf16[1024,512]{0,1:T(8,128)(2,1)S(1)} %copy.289, f32[512]{0:T(512)S(1)} %bitcast.351, f32[512]{0:T(512)S(1)} %bitcast.345, f32[512]{0:T(512)S(1)} %bitcast.347, f32[512]{0:T(512)S(1)} %bitcast.349, f32[512]{0:T(512)S(1)} %bitcast.343), kind=kLoop, calls=%fused_computation.37 | loop fusion | flops 7864320 | bytes 4204544 | tf_op jit(solution)/shard_map/convert_element_type | solution.py:66
  230.3 3.0 rev.33
  234.1 51.8 %all_gather.13 = bf16[16384,16]{0,1:T(8,128)(2,1)S(1)} all-gather(bf16[512,16]{0,1:T(8,128)(2,1)S(1)} %convolution_convert_fusion.7), channel_id=1, replica_groups=mesh['sp_0'=8,'sp_1'=4,'tp'=4,'dp'=2] {'sp_0','sp_1'}, dimensions={0}, use_global_device_ids=true | all-gather | bytes 540672 | tf_op jit(solution)/shard_map/all_gather | solution.py:222
  295.7 2.9 rev.36
  303.1 2.9 convolution_bitcast_fusion.1
  308.0 4.5 %multiply_reduce_fusion.1 = (f32[8,128,64]{1,2,0:T(8,128)S(1)}, f32[8,128,64]{1,2,0:T(8,128)S(1)}) fusion(bf16[32,16,128,64]{2,3,1,0:T(8,128)(2,1)} %all-gather.6.cloned.1.call-done, f32[32,8]{1,0:T(8,128)S(1)} %exponential_select_fusion.1, f32[32,8]{1,0:T(8,128)S(1)} %get-tuple-element.211), kind=kLoop, calls=%fused_computation.7 | loop fusion | flops 12451840 | bytes 8914944 | tf_op jit(solution)/shard_map/reduce_sum | solution.py:277
  324.0 6.0 %rev.37 = f32[512,512]{0,1:T(8,128)} reverse(f32[512,512]{0,1:T(8,128)S(1)} %bitcast.312), dimensions={0} | reverse | bytes 2097152 | tf_op jit(solution)/shard_map/rev | solution.py:298
  329.9 4.3 %bitcast_reduce_fusion = (f32[512,2]{0,1:T(2,128)S(1)}, f32[512,512]{0,1:T(8,128)S(1)}) fusion(bf16[512,2048]{1,0:T(8,128)(2,1)} %all-gather.4.cloned.1.call-done, bf16[2048,512]{1,0:T(8,128)(2,1)} %param.31, f32[512,512]{0,1:T(8,128)} %rev.37, f32[64,8,4,128]{3,2,1,0:T(4,128)} %bitcast.318), kind=kOutput, calls=%fused_computation.119 | convolution fusion | flops 1076362240 | bytes 7344128 | tf_op jit(solution)/shard_map/dot_general | solution.py:173
  335.8 21.9 %all_to_all.5 = bf16[4,128,2048]{2,1,0:T(8,128)(2,1)} all-to-all(bf16[4,128,2048]{2,1,0:T(8,128)(2,1)S(1)} %bitcast.316), channel_id=1, replica_groups=mesh['sp_0'=8,'sp_1'=4,'tp'=4,'dp'=2] {'tp'}, dimensions={0} | all-to-all | bytes 4194304 | tf_op jit(solution)/shard_map/all_to_all | solution.py:40
  (308 shorter events, 133.6 us)
Async XLA Ops:
  6.5 328.0 %copy-start = (bf16[512,2048]{1,0:T(8,128)(2,1)S(1)}, bf16[512,2048]{1,0:T(8,128)(2,1)}, u32[]{:S(2)}) copy-start(bf16[512,2048]{1,0:T(8,128)(2,1)} %param.41) | copy-start | bytes 6291460
  6.5 74.5 %copy-start.14 = (bf16[1,32,2048]{2,1,0:T(8,128)(2,1)S(1)}, bf16[1,32,2048]{2,1,0:T(8,128)(2,1)}, u32[]{:S(2)}) copy-start(bf16[1,32,2048]{2,1,0:T(8,128)(2,1)} %param.25) | copy-start | bytes 393220
  6.5 76.0 %copy-start.16 = (bf16[2048,256]{1,0:T(8,128)(2,1)S(1)}, bf16[2048,256]{1,0:T(8,128)(2,1)}, u32[]{:S(2)}) copy-start(bf16[2048,256]{1,0:T(8,128)(2,1)} %param.32) | copy-start | bytes 3145732
  6.5 104.7 %all-gather.4.cloned.1.call-start = ((), (), s32[]{:S(2)}) async-start(), calls=%async_computation.1 | async-start | bytes 2621440 | tf_op jit(solution)/shard_map/all_gather | solution.py:169
  81.0 118.0 %all-gather.8.cloned.1.call-start = ((), (), s32[]{:S(2)}) async-start(), calls=%async_computation.3 | async-start | bytes 1892352 | tf_op jit(solution)/shard_map/all_gather | solution.py:28
  85.7 222.3 %all-gather.6.cloned.1.call-start = ((), (), s32[]{:S(2)}) async-start(), calls=%async_computation.2 | async-start | bytes 8650752 | tf_op jit(solution)/shard_map/all_gather | solution.py:28
  86.9 31.5 %copy-start.56 = (f32[8]{0:T(128)}, f32[8]{0:T(128)S(1)}, u32[]{:S(2)}) copy-start(f32[8]{0:T(128)S(1)} %get-tuple-element.232) | copy-start | bytes 100
  89.2 36.8 %copy-start.31 = (f32[1,512]{1,0:T(1,128)}, f32[1,512]{1,0:T(1,128)S(1)}, u32[]{:S(2)}) copy-start(f32[1,512]{1,0:T(1,128)S(1)} %get-tuple-element.204) | copy-start | bytes 6148
  89.2 36.8 %copy-start.33 = (f32[1,512]{1,0:T(1,128)}, f32[1,512]{1,0:T(1,128)S(1)}, u32[]{:S(2)}) copy-start(f32[1,512]{1,0:T(1,128)S(1)} %get-tuple-element.205) | copy-start | bytes 6148
  89.2 36.8 %copy-start.35 = (f32[1,512]{1,0:T(1,128)}, f32[1,512]{1,0:T(1,128)S(1)}, u32[]{:S(2)}) copy-start(f32[1,512]{1,0:T(1,128)S(1)} %get-tuple-element.206) | copy-start | bytes 6148
  89.2 36.8 %copy-start.37 = (f32[1,512]{1,0:T(1,128)}, f32[1,512]{1,0:T(1,128)S(1)}, u32[]{:S(2)}) copy-start(f32[1,512]{1,0:T(1,128)S(1)} %get-tuple-element.207) | copy-start | bytes 6148
  89.2 36.8 %copy-start.39 = (f32[1,512]{1,0:T(1,128)}, f32[1,512]{1,0:T(1,128)S(1)}, u32[]{:S(2)}) copy-start(f32[1,512]{1,0:T(1,128)S(1)} %get-tuple-element.208) | copy-start | bytes 6148
  90.9 52.8 %copy-start.45 = (f32[1,256]{1,0:T(1,128)}, f32[1,256]{1,0:T(1,128)S(1)}, u32[]{:S(2)}) copy-start(f32[1,256]{1,0:T(1,128)S(1)} %get-tuple-element.215) | copy-start | bytes 3076
  90.9 52.8 %copy-start.47 = (f32[1,256]{1,0:T(1,128)}, f32[1,256]{1,0:T(1,128)S(1)}, u32[]{:S(2)}) copy-start(f32[1,256]{1,0:T(1,128)S(1)} %get-tuple-element.216) | copy-start | bytes 3076
  91.0 52.8 %copy-start.49 = (f32[1,256]{1,0:T(1,128)}, f32[1,256]{1,0:T(1,128)S(1)}, u32[]{:S(2)}) copy-start(f32[1,256]{1,0:T(1,128)S(1)} %get-tuple-element.217) | copy-start | bytes 3076
  91.0 52.8 %copy-start.51 = (f32[1,256]{1,0:T(1,128)}, f32[1,256]{1,0:T(1,128)S(1)}, u32[]{:S(2)}) copy-start(f32[1,256]{1,0:T(1,128)S(1)} %get-tuple-element.218) | copy-start | bytes 3076
  91.0 52.8 %copy-start.53 = (f32[1,256]{1,0:T(1,128)}, f32[1,256]{1,0:T(1,128)S(1)}, u32[]{:S(2)}) copy-start(f32[1,256]{1,0:T(1,128)S(1)} %get-tuple-element.219) | copy-start | bytes 3076
  182.2 12.3 %copy-start.23 = (f32[1,16384]{1,0:T(1,128)S(1)}, f32[1,16384]{1,0:T(1,128)}, u32[]{:S(2)}) copy-start(f32[1,16384]{1,0:T(1,128)} %param.36) | copy-start | bytes 196612
  228.0 57.8 %copy-start.28 = (f32[32,512]{1,0:T(8,128)S(1)}, f32[32,512]{1,0:T(8,128)}, u32[]{:S(2)}) copy-start(f32[32,512]{1,0:T(8,128)} %mul.746) | copy-start | bytes 196612
  234.1 61.7 %copy-start.9 = (bf16[8,64,256]{2,1,0:T(8,128)(2,1)S(1)}, bf16[8,64,256]{2,1,0:T(8,128)(2,1)}, u32[]{:S(2)}) copy-start(bf16[8,64,256]{2,1,0:T(8,128)(2,1)} %copy-done.8) | copy-start | bytes 786436
  285.8 17.2 %copy-start.13 = (bf16[4,128,2,4,64]{1,4,3,2,0:T(8,128)(2,1)S(1)}, bf16[4,128,2,4,64]{1,4,3,2,0:T(8,128)(2,1)}, u32[]{:S(2)}) copy-start(bf16[4,128,2,4,64]{1,4,3,2,0:T(8,128)(2,1)} %copy-done.12) | copy-start | bytes 1572868
  285.9 17.2 %copy-start.26 = (f32[4,128,2,4]{1,3,2,0:T(4,128)S(1)}, f32[4,128,2,4]{1,3,2,0:T(4,128)}, u32[]{:S(2)}) copy-start(f32[4,128,2,4]{1,3,2,0:T(4,128)} %get-tuple-element.195) | copy-start | bytes 49156
  285.9 17.2 %copy-start.27 = (f32[4,128,2,4]{1,3,2,0:T(4,128)S(1)}, f32[4,128,2,4]{1,3,2,0:T(4,128)}, u32[]{:S(2)}) copy-start(f32[4,128,2,4]{1,3,2,0:T(4,128)} %copy.232) | copy-start | bytes 49156
  285.9 17.2 %copy-start.42 = (pred[128,128]{1,0:T(8,128)(4,1)S(1)}, pred[128,128]{1,0:T(8,128)(4,1)}, u32[]{:S(2)}) copy-start(pred[128,128]{1,0:T(8,128)(4,1)} %iota_compare_fusion) | copy-start | bytes 49156
  (50 other events, 167.0 us)
Sparse Core Ops, SparseCore 0:
  81.1 30.1 all-gather.3
  113.8 78.5 all-gather.7
  195.0 100.4 all-gather.5
where the time goes:
time: 371 us; the launch traced here: 367 us
  blocking collectives  139 us (37%)
  local copies, waits for them, and re-layouts  88 us (24%)
  other arithmetic  63.3 us (17%)
  matrix products  41.8 us (11%)
  waiting for transfers between devices  20.3 us (5%)
  between operations  14.3 us (4%)
    psum x3, blocking collectives, over_axes(): value = lax.psum(value, axis)  65.7 us
    all_gather x1, blocking collectives, per_device(): lax.all_gather(step_raw, SP, axis=0, tiled=True)  51.8 us
    all_to_all x1, blocking collectives, sum_at_owner(): lax.all_to_all(pieces, axis, split_axis=0, concat_axis=0, tiled=True)  21.9 us
    all_gather x1, waiting for transfers between devices, per_device(): row_piece = lax.all_gather(own_rows, 'tp', axis=0, tiled=True)  20.2 us
    add x8, other arithmetic, advance(): jnp.exp(block_decay)[..., None, None] * carry_state + block_increment  9.3 us
    rev x1, local copies, waits for them, and re-layouts, per_device(): values[::-1]  8.32 us
  transfers between devices with their start and end apart: 3, of which 1 were waited for; matrix products, arithmetic and copies ran while one was open for 41% of the time, Pallas kernels for 0%

commit v1 on v0

v1 whole, which is shorter than its diff:
```python
import functools

import jax
import jax.numpy as jnp
from jax import lax
from jax.experimental import pallas as pl
from jax.experimental.pallas import tpu as pltpu
from jax.sharding import Mesh
from jax.sharding import PartitionSpec as P

HEAD = 64
STATE = 128
ROW = 64
BLOCK = 128
HALO = 16
SP = ("sp_0", "sp_1")
SP_TP = ("sp_0", "sp_1", "tp")
NZ, NX, NY = 8, 4, 4
NS = NZ * NX

NORM_FLOOR = 1e-05
GATED_FLOOR = 1e-06
MESH = pl.DeviceIdType.MESH
F32 = jnp.float32
BF16 = jnp.bfloat16
HIGHEST = lax.Precision.HIGHEST
VMEM = pl.BlockSpec(memory_space=pltpu.VMEM)
ANY = pl.BlockSpec(memory_space=pl.ANY)


def silu(v):
    return v / (1.0 + jnp.exp(-v))


def remote(src, dst, send, recv, **where):
    return pltpu.make_async_remote_copy(
        src_ref=src, dst_ref=dst, send_sem=send, recv_sem=recv, device_id=where, device_id_type=MESH
    )


def position():
    return lax.axis_index("sp_0"), lax.axis_index("sp_1"), lax.axis_index("tp")


def lanes(start, size):
    return pl.ds(pl.multiple_of(start, 128), size)


def rows(start, size):
    return pl.ds(pl.multiple_of(start, 16), size)


def gather_kernel(
    lat, ctx, cond, ccond, shift_m, scale_m, gate_m,
    gat, ctx_ext, mod,
    part, ybuf, summed, zbuf, qbuf, xbuf, fbuf, mbuf,
    y_send, y_recv, z_send, z_recv, x_send, x_recv, g_send, g_recv,
    l_send, l_recv, f_send, f_recv, h_send, h_recv,
):
    z, x, y = position()
    s = z * NX + x
    rank = s * NY + y
    nxt, prv = lax.rem(s + 1, NS), lax.rem(s + NS - 1, NS)
    nxt_at = {"sp_0": nxt // NX, "sp_1": lax.rem(nxt, NX)}
    prv_at = {"sp_0": prv // NX, "sp_1": lax.rem(prv, NX)}
    right, left = lax.rem(y + 1, NY), lax.rem(y + NY - 1, NY)

    barrier = pltpu.get_barrier_semaphore()
    for d in range(1, NY):
        pl.semaphore_signal(
            barrier, inc=1, device_id={"tp": lax.rem(y + d, NY)}, device_id_type=MESH
        )
    for d in range(1, NZ):
        pl.semaphore_signal(
            barrier, inc=1, device_id={"sp_0": lax.rem(z + d, NZ)}, device_id_type=MESH
        )
    for d in range(1, NX):
        pl.semaphore_signal(
            barrier, inc=1, device_id={"sp_1": lax.rem(x + d, NX)}, device_id_type=MESH
        )
    pl.semaphore_signal(barrier, inc=1, device_id=nxt_at, device_id_type=MESH)
    pl.semaphore_signal(barrier, inc=1, device_id=prv_at, device_id_type=MESH)

    vec_row, vec_off = rank // 8, lax.rem(rank, 8) * 16
    lane = lax.broadcasted_iota(jnp.int32, (8, 128), 1)
    window = (lane >= vec_off) & (lane < vec_off + 16)
    own = cond[pl.ds(vec_row, 1), :]
    shared = ccond[pl.ds(vec_row, 1), :]
    line = lax.broadcasted_iota(jnp.int32, (8, 128), 0)
    both = jnp.where(
        line == 0, jnp.broadcast_to(own, (8, 128)), jnp.broadcast_to(shared, (8, 128))
    )
    acts = jnp.where(window, silu(both), 0.0).astype(BF16)

    def product(matrix):
        tall = jnp.concatenate([matrix[...]] * 8, axis=0)
        return jnp.dot(acts, tall, preferred_element_type=F32)

    part[0:2, :] = product(shift_m)[0:2]
    part[2:4, :] = product(scale_m)[0:2]
    part[4:8, :] = product(gate_m)[0:4]
    pl.semaphore_wait(barrier, NY + NZ + NX - 3 + 2)

    y_copies = []
    for d in range(1, NY):
        copy = remote(
            part, ybuf.at[d - 1], y_send.at[d - 1], y_recv.at[d - 1], tp=lax.rem(y + d, NY)
        )
        copy.start()
        y_copies.append(copy)
    l_copies = {}
    for side, half in ((0, 0), (1, 1), (0, 1), (1, 0)):
        copy = remote(
            lat.at[pl.ds(half * 64, 64)],
            gat.at[rows(y * 128 + half * 64, 64)],
            l_send.at[side * 2 + half],
            l_recv.at[side * 2 + half],
            tp=right if side == 0 else left,
        )
        copy.start()
        l_copies[side, half] = copy
    halo_next = remote(
        ctx.at[pl.ds(HALO, HALO)], ctx_ext.at[pl.ds(0, HALO)], h_send.at[0], h_recv.at[0], **nxt_at
    )
    halo_prev = remote(
        ctx.at[pl.ds(0, HALO)],
        ctx_ext.at[pl.ds(3 * HALO, HALO)],
        h_send.at[1],
        h_recv.at[1],
        **prv_at,
    )
    halo_next.start()
    halo_prev.start()

    for copy in y_copies:
        copy.wait()
    summed[...] = (part[...] + ybuf[0]) + (ybuf[1] + ybuf[2])

    z_copies = []
    for d in range(1, NZ):
        to = lax.rem(z + d, NZ)
        copy = remote(
            summed.at[:, lanes(to * 256, 256)],
            zbuf.at[d - 1],
            z_send.at[d - 1],
            z_recv.at[d - 1],
            sp_0=to,
        )
        copy.start()
        z_copies.append(copy)
    total = summed[:, lanes(z * 256, 256)]
    gat[rows(y * 128, 128), :] = lat[...]
    ctx_ext[pl.ds(HALO, 2 * HALO), :] = ctx[...]
    for d, copy in enumerate(z_copies):
        copy.wait()
        total = total + zbuf[d]
    qbuf[...] = total
    x_copies = []
    for d in range(1, NX):
        copy = remote(
            qbuf, xbuf.at[d - 1], x_send.at[d - 1], x_recv.at[d - 1], sp_1=lax.rem(x + d, NX)
        )
        copy.start()
        x_copies.append(copy)

    l_copies[0, 0].wait_recv()
    ahead = remote(
        gat.at[rows(left * 128, 64)],
        gat.at[rows(left * 128, 64)],
        f_send.at[0],
        f_recv.at[0],
        tp=right,
    )
    ahead.start()
    l_copies[1, 1].wait_recv()
    back = remote(
        gat.at[rows(right * 128 + 64, 64)],
        gat.at[rows(right * 128 + 64, 64)],
        f_send.at[1],
        f_recv.at[1],
        tp=left,
    )
    back.start()

    for copy in x_copies:
        copy.wait()
    fbuf[...] = (qbuf[...] + xbuf[0]) + (xbuf[1] + xbuf[2])
    g_copies = []
    for d in range(1, NZ):
        copy = remote(
            fbuf,
            mbuf.at[:, lanes(z * 256, 256)],
            g_send.at[d - 1],
            g_recv.at[d - 1],
            sp_0=lax.rem(z + d, NZ),
        )
        copy.start()
        g_copies.append(copy)
    mbuf[:, lanes(z * 256, 256)] = fbuf[...]
    for copy in g_copies:
        copy.wait()
    mod[...] = mbuf[...]
    halo_next.wait()
    halo_prev.wait()
    for side, half in ((0, 0), (1, 1)):
        l_copies[side, half].wait_send()
    for side, half in ((0, 1), (1, 0)):
        l_copies[side, half].wait()
    ahead.wait()
    back.wait()


def gather_call(lat, ctx, cond, ccond, shift_m, scale_m, gate_m):
    width = lat.shape[1]
    dma = pltpu.SemaphoreType.DMA
    return pl.pallas_call(
        gather_kernel,
        out_shape=(
            jax.ShapeDtypeStruct((NY * 128, width), BF16),
            jax.ShapeDtypeStruct((4 * HALO, width), BF16),
            jax.ShapeDtypeStruct((8, width), F32),
        ),
        in_specs=[VMEM] * 7,
        out_specs=(VMEM, VMEM, VMEM),
        scratch_shapes=[
            pltpu.VMEM((8, width), F32),
            pltpu.VMEM((NY - 1, 8, width), F32),
            pltpu.VMEM((8, width), F32),
            pltpu.VMEM((NZ - 1, 8, 256), F32),
            pltpu.VMEM((8, 256), F32),
            pltpu.VMEM((NX - 1, 8, 256), F32),
            pltpu.VMEM((8, 256), F32),
            pltpu.VMEM((8, width), F32),
            dma((NY - 1,)), dma((NY - 1,)),
            dma((NZ - 1,)), dma((NZ - 1,)),
            dma((NX - 1,)), dma((NX - 1,)),
            dma((NZ - 1,)), dma((NZ - 1,)),
            dma((4,)), dma((4,)),
            dma((2,)), dma((2,)),
            dma((2,)), dma((2,)),
        ],
        compiler_params=pltpu.CompilerParams(
            collective_id=0, has_side_effects=True, vmem_limit_bytes=16 << 20
        ),
        name="gather",
    )(lat, ctx, cond, ccond, shift_m, scale_m, gate_m)


def normed_rows(block, shift, scale):
    values = block.astype(F32)
    center = jnp.mean(values, -1, keepdims=True)
    off = values - center
    spread = jnp.mean(off * off, -1, keepdims=True)
    return (off * lax.rsqrt(spread + NORM_FLOOR) * (1.0 + scale) + shift).astype(BF16)


def conv_rows(pre, taps, run):
    length = pre.shape[0]
    at = lax.rem(lax.broadcasted_iota(jnp.int32, pre.shape, 0), run)
    total = pre * taps[2:3]
    for k in (0, 1, 3, 4):
        moved = pltpu.roll(pre, (2 - k) % length, 0)
        inside = (at + (k - 2) >= 0) & (at + (k - 2) < run)
        total = total + jnp.where(inside, moved, 0.0) * taps[k : k + 1]
    return silu(total)


def split2(v):
    high = v.astype(BF16)
    return high, (v - high.astype(F32)).astype(BF16)


def expand(v, spread):
    high, low = split2(v)
    return jnp.dot(high, spread, preferred_element_type=F32) + jnp.dot(
        low, spread, preferred_element_type=F32
    )


def softplus(v):
    return jnp.maximum(v, 0.0) + jnp.log1p(jnp.exp(-jnp.abs(v)))


def spread_matrix(spread):
    shape = spread.shape
    row = lax.broadcasted_iota(jnp.int32, shape, 0)
    col = lax.broadcasted_iota(jnp.int32, shape, 1)
    spread[...] = jnp.where(row == col // HEAD, 1.0, 0.0).astype(BF16)


def compute_kernel(
    gat, ctx_ext, mod, w_value, w_gate, w_write, w_read, w_step, rates, pace,
    t_value, t_write, t_read,
    ends, totals, local, reads, gates, carry_decay,
    hid, val, wri, cum, stp, spread, inc, before, etot, tot,
):
    z, x, y = position()
    s = z * NX + x
    heads = 8
    spread_matrix(spread)
    row64 = lax.broadcasted_iota(jnp.int32, (64, 128), 0)
    col64 = lax.broadcasted_iota(jnp.int32, (64, 128), 1)
    wanted = jnp.where(col64 < heads, y * heads + col64, 32 + y * heads + col64 - heads)
    pick = jnp.where((row64 == wanted) & (col64 < 2 * heads), 1.0, 0.0)
    pick16 = pick.astype(BF16)
    rate_row = jnp.dot(
        jnp.broadcast_to(rates[...], (8, 64)), pick, precision=HIGHEST, preferred_element_type=F32
    )[0:1]
    value_taps = t_value[:, lanes(y * 512, 512)]
    write_taps = t_write[:, lanes(y * 256, 256)]
    read_taps = t_read[:, lanes(y * 256, 256)]
    row = lax.broadcasted_iota(jnp.int32, (BLOCK, BLOCK), 0)
    col = lax.broadcasted_iota(jnp.int32, (BLOCK, BLOCK), 1)
    lower = jnp.where(col <= row, 1.0, 0.0)
    upper = jnp.where(col >= row, 1.0, 0.0)
    forward_lane = col < heads

    def mix_dot(a, b, ca, cb):
        return lax.dot_general(a, b, (((ca,), (cb,)), ((), ())), preferred_element_type=F32)

    def steps_of(hidden, count):
        raw = jnp.dot(hidden, w_step[...], preferred_element_type=F32).astype(BF16)
        return softplus(jnp.dot(raw, pick16, preferred_element_type=F32))

    for part in range(4):
        rs = pl.ds(part * HALO, HALO)
        hid[rs, :] = normed_rows(ctx_ext[rs, :], mod[1:2, :], mod[3:4, :])
    hidden = hid[0 : 4 * HALO, :]
    at = lax.broadcasted_iota(jnp.int32, (4 * HALO, 1), 0)
    first = jnp.where(s == 0, HALO, 0)
    last = jnp.where(s == NS - 1, 3 * HALO, 4 * HALO)
    present = (at >= first) & (at < last)
    cv = jnp.dot(hidden, w_value[...], preferred_element_type=F32).astype(BF16).astype(F32)
    cw = jnp.dot(hidden, w_write[...], preferred_element_type=F32).astype(BF16).astype(F32)
    cv = conv_rows(jnp.where(present, cv, 0.0), value_taps, 4 * HALO)[HALO : 3 * HALO].astype(BF16)
    cw = conv_rows(jnp.where(present, cw, 0.0), write_taps, 4 * HALO)[HALO : 3 * HALO].astype(BF16)
    cstep = steps_of(hidden, 4 * HALO)[HALO : 3 * HALO]
    cdecay = -rate_row * cstep
    r32 = lax.broadcasted_iota(jnp.int32, (2 * HALO, 2 * HALO), 0)
    c32 = lax.broadcasted_iota(jnp.int32, (2 * HALO, 2 * HALO), 1)
    later = jnp.dot(
        jnp.where(c32 > r32, 1.0, 0.0), cdecay, precision=HIGHEST, preferred_element_type=F32
    )
    earlier = jnp.dot(
        jnp.where(c32 < r32, 1.0, 0.0), cdecay, precision=HIGHEST, preferred_element_type=F32
    )
    f32lane = lax.broadcasted_iota(jnp.int32, (2 * HALO, 128), 1) < heads
    cweight = jnp.exp(jnp.where(f32lane, later, earlier)) * cstep
    cvf = cv.astype(F32)
    cscaled = (jnp.concatenate([cvf, cvf], axis=1) * expand(cweight, spread[...])).astype(BF16)
    for g in range(2):
        wg = cw[:, g * 128 : (g + 1) * 128]
        for d in range(2):
            lg = d * 2 + g
            got = mix_dot(wg, cscaled[:, lg * 256 : (lg + 1) * 256], 0, 0)
            ends[:, lg * 512 + 256 : lg * 512 + 512] = got.astype(BF16)
    ctotal = jnp.exp(jnp.sum(cdecay, axis=0, keepdims=True))

    def project(b, none):
        for part in range(4):
            rs = pl.ds(part * 32, 32)
            hid[rs, :] = normed_rows(gat[rows(b * 128 + part * 32, 32), :], mod[0:1, :], mod[2:3, :])
        hidden = hid[...]
        at_b = rows(b * 128, 128)
        pre = jnp.dot(hidden, w_value[...], preferred_element_type=F32).astype(BF16).astype(F32)
        v = conv_rows(pre, value_taps, ROW)
        vb = v.astype(BF16)
        val[at_b, :] = vb
        pre = jnp.dot(hidden, w_write[...], preferred_element_type=F32).astype(BF16).astype(F32)
        w = conv_rows(pre, write_taps, ROW).astype(BF16)
        wri[at_b, :] = w
        pre = jnp.dot(hidden, w_read[...], preferred_element_type=F32).astype(BF16).astype(F32)
        reads[at_b, :] = conv_rows(pre, read_taps, ROW).astype(BF16)
        gates[at_b, :] = jnp.dot(hidden, w_gate[...], preferred_element_type=F32).astype(BF16)
        pace_row = pace[pl.ds(s * 4 + b, 1), :]
        pace_col = jnp.transpose(jnp.broadcast_to(pace_row, (128, 128)))
        step = steps_of(hidden, 128) * pace_col
        decay = -rate_row * step
        down = jnp.dot(lower, decay, precision=HIGHEST, preferred_element_type=F32)
        up = jnp.dot(upper, decay, precision=HIGHEST, preferred_element_type=F32)
        cums = jnp.where(forward_lane, down, up)
        total = jnp.where(forward_lane[0:1], down[127:128], up[0:1])
        cum[at_b, :] = cums
        stp[at_b, :] = step
        weight = jnp.exp(total - cums) * step
        vf = vb.astype(F32)
        scaled = (jnp.concatenate([vf, vf], axis=1) * expand(weight, spread[...])).astype(BF16)
        for g in range(2):
            wg = w[:, g * 128 : (g + 1) * 128]
            for d in range(2):
                lg = d * 2 + g
                inc[b, :, lg * 256 : (lg + 1) * 256] = mix_dot(
                    wg, scaled[:, lg * 256 : (lg + 1) * 256], 0, 0
                )
        tot[pl.ds(b, 1), :] = total
        return none

    lax.fori_loop(0, 4, project, 0)

    t0, t1, t2, t3 = (tot[b : b + 1, :] for b in range(4))
    zero = jnp.zeros_like(t0)
    fl = forward_lane[0:1]
    since = [
        jnp.where(fl, zero, t1 + t2 + t3),
        jnp.where(fl, t0, t2 + t3),
        jnp.where(fl, t0 + t1, t3),
        jnp.where(fl, t0 + t1 + t2, zero),
    ]
    stack = jnp.concatenate(
        [jnp.exp(t0), jnp.exp(t1), jnp.exp(t2), jnp.exp(t3), jnp.exp(t0 + t1 + t2 + t3), ctotal,
         zero, zero], axis=0,
    )
    high = stack.astype(BF16)
    rest = stack - high.astype(F32)
    etot[...] = jnp.dot(high, spread[...], preferred_element_type=F32) + expand(rest, spread[...])
    totals[...] = etot[4:6, :]
    for b in range(4):
        tot[b : b + 1, :] = since[b]
    for d, order in ((0, (0, 1, 2, 3)), (1, (3, 2, 1, 0))):
        for g in range(2):
            lg = d * 2 + g
            ls = slice(lg * 256, (lg + 1) * 256)
            state = jnp.zeros((STATE, 256), F32)
            for b in order:
                before[b, :, ls] = state.astype(BF16)
                state = etot[b : b + 1, ls] * state + inc[b, :, ls]
            ends[:, lg * 512 : lg * 512 + 256] = state.astype(BF16)

    def within(b, none):
        at_b = rows(b * 128, 128)
        cums = cum[at_b, :]
        step = stp[at_b, :]
        cums_t = jnp.transpose(cums)
        step_t = jnp.transpose(step)
        carry_decay[at_b, :] = jnp.exp(cums + tot[pl.ds(b, 1), :])
        grown = expand(jnp.exp(cums), spread[...])
        for g in range(2):
            r = reads[at_b, g * 128 : (g + 1) * 128]
            w = wri[at_b, g * 128 : (g + 1) * 128]
            affinity = mix_dot(r, w, 1, 1)
            carried = jnp.zeros((128, 256), F32)
            for d in range(2):
                ls = slice((d * 2 + g) * 256, (d * 2 + g + 1) * 256)
                carried = carried + (
                    jnp.dot(r, before[b, :, ls], preferred_element_type=F32) * grown[:, ls]
                )
            for q in range(2):
                mixes = []
                for h in (g * 4 + q * 2, g * 4 + q * 2 + 1):
                    exponent = jnp.where(
                        col <= row,
                        cums[:, h : h + 1] - cums_t[h : h + 1, :],
                        cums[:, 8 + h : 9 + h] - cums_t[8 + h : 9 + h, :],
                    )
                    sf, sb = step_t[h : h + 1, :], step_t[8 + h : 9 + h, :]
                    amount = jnp.where(col < row, sf, jnp.where(col > row, sb, sf + sb))
                    mixes.append((affinity * jnp.exp(exponent) * amount).astype(BF16))
                ls = slice((g * 2 + q) * 128, (g * 2 + q + 1) * 128)
                pair = val[at_b, ls]
                none16 = jnp.zeros_like(pair)
                tall = jnp.concatenate(
                    [jnp.where(col < HEAD, pair, none16), jnp.where(col >= HEAD, pair, none16)],
                    axis=0,
                )
                got = jnp.dot(
                    jnp.concatenate(mixes, axis=1), tall, preferred_element_type=F32
                )
                local[at_b, ls] = got + carried[:, q * 128 : (q + 1) * 128]
        return none

    lax.fori_loop(0, 4, within, 0)


def compute_call(*args):
    tokens = args[0].shape[0]
    return pl.pallas_call(
        compute_kernel,
        out_shape=(
            jax.ShapeDtypeStruct((STATE, 2048), BF16),
            jax.ShapeDtypeStruct((2, 1024), F32),
            jax.ShapeDtypeStruct((tokens, 512), F32),
            jax.ShapeDtypeStruct((tokens, 256), BF16),
            jax.ShapeDtypeStruct((tokens, 512), BF16),
            jax.ShapeDtypeStruct((tokens, 128), F32),
        ),
        in_specs=[VMEM] * 13,
        out_specs=(VMEM,) * 6,
        scratch_shapes=[
            pltpu.VMEM((128, 2048), BF16),
            pltpu.VMEM((tokens, 512), BF16),
            pltpu.VMEM((tokens, 256), BF16),
            pltpu.VMEM((tokens, 128), F32),
            pltpu.VMEM((tokens, 128), F32),
            pltpu.VMEM((128, 1024), BF16),
            pltpu.VMEM((4, STATE, 1024), F32),
            pltpu.VMEM((4, STATE, 1024), BF16),
            pltpu.VMEM((8, 1024), F32),
            pltpu.VMEM((8, 128), F32),
        ],
        compiler_params=pltpu.CompilerParams(vmem_limit_bytes=48 << 20),
        name="compute",
    )(*args)


def state_kernel(
    ends, totals, start,
    got, got_tot, sent, landing,
    a_send, a_recv, t_send, t_recv, b_send, b_recv,
):
    z, x, y = position()
    s = z * NX + x

    def at(t):
        return {"sp_0": t // NX, "sp_1": lax.rem(t, NX)}

    barrier = pltpu.get_barrier_semaphore()

    def greet(p, none):
        pl.semaphore_signal(
            barrier, inc=1, device_id=at(lax.rem(s + p, NS)), device_id_type=MESH
        )
        return none

    lax.fori_loop(1, NS, greet, 0)
    pl.semaphore_wait(barrier, NS - 1)

    def out_copy(p):
        t = lax.rem(s + p, NS)
        return (
            remote(
                ends.at[rows((t // NX) * 16, 16), lanes(lax.rem(t, NX) * 512, 512)],
                got.at[s],
                a_send.at[t],
                a_recv.at[s],
                **at(t),
            ),
            remote(
                totals.at[:, lanes(lax.rem(t, NX) * 256, 256)],
                got_tot.at[s],
                t_send.at[t],
                t_recv.at[s],
                **at(t),
            ),
        )

    def send_out(p, none):
        for copy in out_copy(p):
            copy.start()
        return none

    lax.fori_loop(1, NS, send_out, 0)
    got[s] = ends[rows(z * 16, 16), lanes(x * 512, 512)]
    got_tot[s] = totals[:, lanes(x * 256, 256)]

    def take_in(p, none):
        f = lax.rem(s + NS - p, NS)
        remote(got.at[f], got.at[f], a_send.at[f], a_recv.at[f], **at(f)).wait_recv()
        remote(got_tot.at[f], got_tot.at[f], t_send.at[f], t_recv.at[f], **at(f)).wait_recv()
        return none

    lax.fori_loop(1, NS, take_in, 0)

    turned = x // 2

    def order(k):
        return k + turned * (NS - 1 - 2 * k)

    def context(k, state):
        j = order(k)
        return got_tot[j, 1:2, :] * state + got[j, :, 256:512].astype(F32)

    state = lax.fori_loop(0, NS, context, jnp.zeros((16, 256), F32))

    def back_copy(j):
        return remote(
            sent.at[j],
            landing.at[rows(z * 16, 16), lanes(x * 256, 256)],
            b_send.at[j],
            b_recv.at[s],
            **at(j),
        )

    def latent(k, state):
        j = order(k)
        sent[j] = state.astype(BF16)

        @pl.when(j != s)
        def _():
            back_copy(j).start()

        return got_tot[j, 0:1, :] * state + got[j, :, 0:256].astype(F32)

    lax.fori_loop(0, NS, latent, state)
    landing[rows(z * 16, 16), lanes(x * 256, 256)] = sent[s]

    def finish(p, none):
        f = lax.rem(s + NS - p, NS)
        piece = landing.at[rows((f // NX) * 16, 16), lanes(lax.rem(f, NX) * 256, 256)]
        remote(piece, piece, b_send.at[f], b_recv.at[f], **at(f)).wait_recv()
        t = lax.rem(s + p, NS)
        for copy in out_copy(p):
            copy.wait_send()
        back_copy(t).wait_send()
        return none

    lax.fori_loop(1, NS, finish, 0)
    start[...] = landing[...]


def state_call(ends, totals):
    dma = pltpu.SemaphoreType.DMA
    return pl.pallas_call(
        state_kernel,
        out_shape=jax.ShapeDtypeStruct((STATE, 1024), BF16),
        in_specs=[VMEM] * 2,
        out_specs=VMEM,
        scratch_shapes=[
            pltpu.VMEM((NS, 16, 512), BF16),
            pltpu.VMEM((NS, 2, 256), F32),
            pltpu.VMEM((NS, 16, 256), BF16),
            pltpu.VMEM((STATE, 1024), BF16),
        ]
        + [dma((NS,))] * 6,
        compiler_params=pltpu.CompilerParams(
            collective_id=1, has_side_effects=True, vmem_limit_bytes=16 << 20
        ),
        name="state",
    )(ends, totals)


def output_kernel(
    start, local, reads, gates, carry_decay, gain, w_out, mod, lat,
    out,
    spread, inner, far, near_r, near_l, mine, got_far, got_r, got_l,
    s1, r1, s2, r2,
):
    z, x, y = position()
    right, left = lax.rem(y + 1, NY), lax.rem(y + NY - 1, NY)
    opposite = lax.rem(y + 2, NY)
    barrier = pltpu.get_barrier_semaphore()
    pl.semaphore_signal(barrier, inc=1, device_id={"tp": right}, device_id_type=MESH)
    pl.semaphore_signal(barrier, inc=1, device_id={"tp": left}, device_id_type=MESH)
    spread_matrix(spread)
    gains = gain[:, lanes(y * 512, 512)]
    half = w_out.shape[1] // 2

    def make_inner(b):
        at_b = rows(b * 128, 128)
        grown = expand(carry_decay[at_b, :], spread[...])
        for g in range(2):
            r = reads[at_b, g * 128 : (g + 1) * 128]
            ch = slice(g * 256, (g + 1) * 256)
            total = local[at_b, ch]
            for d in range(2):
                ls = slice((d * 2 + g) * 256, (d * 2 + g + 1) * 256)
                total = total + jnp.dot(r, start[:, ls], preferred_element_type=F32) * grown[:, ls]
            gated = total * silu(gates[at_b, ch].astype(F32))
            power = jnp.mean(gated * gated, -1, keepdims=True)
            inner[:, ch] = (gated * lax.rsqrt(power + GATED_FLOOR) * gains[:, ch]).astype(BF16)

    def product(side):
        return jnp.dot(
            inner[...], w_out[:, side * half : (side + 1) * half], preferred_element_type=F32
        ).astype(BF16)

    make_inner(opposite)
    far[0] = product(0)
    pl.semaphore_wait(barrier, 2)
    far_r = remote(far.at[0], got_far.at[0], s1.at[0], r1.at[0], tp=right)
    far_r.start()
    far[1] = product(1)
    far_l = remote(far.at[1], got_far.at[1], s1.at[1], r1.at[1], tp=left)
    far_l.start()
    make_inner(right)
    near_r[1] = product(1)
    raw_r = remote(near_r.at[1], got_r.at[1], s2.at[0], r2.at[0], tp=right)
    raw_r.start()
    near_r[0] = product(0)
    make_inner(left)
    near_l[0] = product(0)
    raw_l = remote(near_l.at[0], got_l.at[0], s2.at[1], r2.at[1], tp=left)
    raw_l.start()
    near_l[1] = product(1)
    far_r.wait_recv()
    near_r[0] = (near_r[0].astype(F32) + got_far[0].astype(F32)).astype(BF16)
    sum_r = remote(near_r.at[0], got_r.at[0], s2.at[2], r2.at[2], tp=right)
    sum_r.start()
    far_l.wait_recv()
    near_l[1] = (near_l[1].astype(F32) + got_far[1].astype(F32)).astype(BF16)
    sum_l = remote(near_l.at[1], got_l.at[1], s2.at[3], r2.at[3], tp=left)
    sum_l.start()
    make_inner(y)
    mine[0] = product(0)
    mine[1] = product(1)

    def close(side):
        cs = slice(side * half, (side + 1) * half)
        mixed = (
            mine[side].astype(F32) + got_r[side].astype(F32) + got_l[side].astype(F32)
        ).astype(BF16)
        out[:, cs] = (lat[:, cs].astype(F32) + mod[4:5, cs] * mixed.astype(F32)).astype(BF16)

    raw_r.wait_recv()
    raw_l.wait_recv()
    sum_r.wait_recv()
    sum_l.wait_recv()
    close(0)
    close(1)
    far_r.wait_send()
    far_l.wait_send()
    raw_r.wait_send()
    raw_l.wait_send()
    sum_r.wait_send()
    sum_l.wait_send()


def output_call(*args):
    width = args[6].shape[1]
    dma = pltpu.SemaphoreType.DMA
    piece = pltpu.VMEM((2, 128, width // 2), BF16)
    return pl.pallas_call(
        output_kernel,
        out_shape=jax.ShapeDtypeStruct((128, width), BF16),
        in_specs=[VMEM] * 9,
        out_specs=VMEM,
        scratch_shapes=[
            pltpu.VMEM((128, 1024), BF16),
            pltpu.VMEM((128, 512), BF16),
        ]
        + [piece] * 7
        + [dma((2,)), dma((2,)), dma((4,)), dma((4,))],
        compiler_params=pltpu.CompilerParams(
            collective_id=2, has_side_effects=True, vmem_limit_bytes=32 << 20
        ),
        name="output",
    )(*args)


def per_device(
    latent, condition, context, context_cond, shift_matrix, scale_matrix, gate_matrix,
    value_proj, gate_proj, write_proj, read_proj, step_proj, decay_rate, pacing,
    value_taps, write_taps, read_taps, norm_gain, out_proj,
):
    width = latent.shape[2]
    gathered, ctx_ext, mod = gather_call(
        latent[0],
        context[0],
        condition.reshape(width // 128, 128),
        context_cond.reshape(width // 128, 128),
        shift_matrix,
        scale_matrix,
        gate_matrix,
    )
    ends, totals, local, reads, gates, carry_decay = compute_call(
        gathered, ctx_ext, mod, value_proj, gate_proj, write_proj, read_proj,
        step_proj.reshape(width, 64), decay_rate.reshape(1, 64),
        pacing.reshape(128, 128), value_taps, write_taps, read_taps,
    )
    start = state_call(ends, totals)
    updated = output_call(
        start, local, reads, gates, carry_decay, norm_gain.reshape(1, -1), out_proj, mod, latent[0]
    )
    return updated[None]


def solution(mesh):
    torus = Mesh(
        mesh.devices.reshape(NZ, NX, mesh.shape["tp"], mesh.shape["dp"]),
        ("sp_0", "sp_1", "tp", "dp"),
    )
    placed = (
        P("dp", SP_TP, None), P("dp", None), P("dp", SP, None), P(),
        P(SP_TP, None), P(SP_TP, None), P(SP_TP, None),
        P(None, "tp"), P(None, "tp"), P(None, "tp"), P(None, "tp"),
        P(), P(), P("dp", None), P(), P(), P(), P(), P("tp", None),
    )
    return jax.shard_map(
        per_device, mesh=torus, in_specs=placed, out_specs=P("dp", SP_TP, None), check_vma=False
    )
```

time: 371 us -> 117 us (0.32)
  blocking collectives: 139 us -> 0 us
  Pallas kernels: 0 us -> 99.4 us
  local copies, waits for them, and re-layouts: 88 us -> 15.6 us
  other arithmetic: 63.3 us -> 0 us
  matrix products: 41.8 us -> 0 us
  waiting for transfers between devices: 20.3 us -> 0 us
  between operations: 14.3 us -> 0.09 us
    pallas_call x0 -> x4, Pallas kernels: none -> 99.4 us  [the longest x1 32.1 us: state_call(): pl.pallas_call(state_kernel, out_shape=jax.ShapeDtypeStruct((STATE, 1024)...]
    psum x3 -> x0, blocking collectives: 65.7 us -> none  [over_axes(): value = lax.psum(value, axis)]
    all_gather x1 -> x0, blocking collectives: 51.8 us -> none  [per_device(): lax.all_gather(step_raw, SP, axis=0, tiled=True)]
    dot_general x21 -> x0, matrix products: 41.8 us -> none  [the longest x2 6.25 us: block_inputs(): jnp.einsum('kqgrn,kqgrp->kgrnp', scaled, head_values, preferred_element_t...]
    rev x10 -> x0, local copies, waits for them, and re-layouts: 25.5 us -> none  [the longest x1 8.32 us: per_device(): values[::-1]]
    all_to_all x1 -> x0, blocking collectives: 21.9 us -> none  [sum_at_owner(): lax.all_to_all(pieces, axis, split_axis=0, concat_axis=0, tiled=True)]
    all_gather x3 -> x0, waiting for transfers between devices: 20.2 us -> none  [the longest x1 20.2 us: per_device(): row_piece = lax.all_gather(own_rows, 'tp', axis=0, tiled=True)]
    convert_element_type x12 -> x0, local copies, waits for them, and re-layouts: 15.8 us -> none  [the longest x4 6.39 us: convolve(): return jax.nn.silu(summed).reshape(length, channels).astype(jnp.bfloat16)]
  transfers between devices with their start and end apart: 3 -> 0, of which waited for: 1 -> 0; matrix products, arithmetic and copies ran while one was open for 41% -> 0% of each run, Pallas kernels for 0% -> 0%
where the time goes in v1:
time: 117 us; the launch traced here: 115 us
  Pallas kernels  99.4 us (85%)
  local copies, waits for them, and re-layouts  15.6 us (13%)
    pallas_call x1, Pallas kernels, state_call(): pl.pallas_call(state_kernel, out_shape=jax.ShapeDtypeStruct((STATE, 1024)...  32.1 us
    pallas_call x1, Pallas kernels, gather_call(): pl.pallas_call(gather_kernel, out_shape=(jax.ShapeDtypeStruct((NY * 128,...  30.2 us
    pallas_call x1, Pallas kernels, output_call(): pl.pallas_call(output_kernel, out_shape=jax.ShapeDtypeStruct((128, width)...  19.6 us
    pallas_call x1, Pallas kernels, compute_call(): pl.pallas_call(compute_kernel, out_shape=(jax.ShapeDtypeStruct((STATE, 20...  17.4 us
    unnamed x35, local copies, waits for them, and re-layouts  13.6 us

profile of v1, /device:TPU:8, one launch (start us, length us, event | category | flops | bytes accessed | tf_op | source)
XLA Modules:
  0.0 115.1 jit_solution(4248095481091290043)
XLA Ops:
  0.0 0.8 reshape.21.rates
  0.8 1.2 %copy.21.w_step = bf16[2048,64]{1,0:T(8,128)(2,1)S(1)} copy(bf16[2048,64]{0,1:T(8,128)(2,1)} %bitcast.16) | data formatting | bytes 524288 | tf_op jit(solution)/shard_map/reshape | solution.py:756
  2.0 0.0 copy-start.2
  2.0 1.0 copy-done.2
  3.0 0.9 copy-done.6
  3.9 0.8 copy-done.9
  4.8 0.8 copy-done.10
  5.6 0.8 copy-done.11
  6.5 0.7 copy-done.14
  7.2 0.7 copy-done.15
  7.9 30.2 %gather.1 = (bf16[512,2048]{1,0:T(8,128)(2,1)S(1)}, bf16[64,2048]{1,0:T(8,128)(2,1)S(1)}, f32[8,2048]{1,0:T(8,128)S(1)}) custom-call(bf16[128,2048]{1,0:T(8,128)(2,1)S(1)} %bitcast.8, bf16[32,2048]{1,0:T(8,128)(2,1)S(1)} %bitcast.11, f32[16,128]{1,0:T(8,128)S(1)} %bitcast.13, f32[16,128]{1,0:T(8,128)S(1)} %bitcast.14, bf16[16,2048]{1,0:T(8,128)(2,1)S(1)} %copy-done.9, ...), custom_call_target="tpu_custom_call" | custom-call | tf_op jit(solution)/shard_map/gather/pallas_call | solution.py:216
  38.1 1.3 %copy-done = bf16[512,2048]{1,0:T(8,128)(2,1)} copy-done((bf16[512,2048]{1,0:T(8,128)(2,1)}, bf16[512,2048]{1,0:T(8,128)(2,1)S(1)}, u32[]{:S(2)}) %copy-start) | copy-done | bytes 2097176
  39.4 1.2 %copy-done.4 = bf16[2048,256]{1,0:T(8,128)(2,1)S(1)} copy-done((bf16[2048,256]{1,0:T(8,128)(2,1)S(1)}, bf16[2048,256]{1,0:T(8,128)(2,1)}, u32[]{:S(2)}) %copy-start.4) | copy-done | bytes 1048600
  40.6 1.2 %copy-done.5 = bf16[2048,256]{1,0:T(8,128)(2,1)S(1)} copy-done((bf16[2048,256]{1,0:T(8,128)(2,1)S(1)}, bf16[2048,256]{1,0:T(8,128)(2,1)}, u32[]{:S(2)}) %copy-start.5) | copy-done | bytes 1048600
  41.9 0.8 copy-done.7
  42.7 0.8 copy-done.8
  43.5 0.8 copy-done.12
  44.3 0.8 copy-done.13
  45.1 17.4 %compute.1 = (bf16[128,2048]{1,0:T(8,128)(2,1)S(1)}, f32[2,1024]{1,0:T(2,128)S(1)}, f32[512,512]{1,0:T(8,128)S(1)}, bf16[512,256]{1,0:T(8,128)(2,1)S(1)}, bf16[5...) custom-call(bf16[512,2048]{1,0:T(8,128)(2,1)} %copy-done, bf16[64,2048]{1,0:T(8,128)(2,1)S(1)} %get-tuple-element.15.ctx_ext, ...), custom_call_target="tpu_custom_call" | custom-call | tf_op jit(solution)/shard_map/compute/pallas_call | solution.py:476
  62.5 32.1 %state.1.start = bf16[128,1024]{1,0:T(8,128)(2,1)S(1)} custom-call(bf16[128,2048]{1,0:T(8,128)(2,1)S(1)} %get-tuple-element.17.ends, f32[2,1024]{1,0:T(2,128)S(1)} %get-tuple-element.18.totals), custom_call_target="tpu_custom_call" | custom-call | tf_op jit(solution)/shard_map/state/pallas_call | solution.py:612
  94.6 0.0 copy-done.1
  94.6 0.0 copy-done.3
  94.6 19.6 %output.1 = bf16[128,2048]{1,0:T(8,128)(2,1)S(1)} custom-call(bf16[128,1024]{1,0:T(8,128)(2,1)S(1)} %state.1.start, f32[512,512]{1,0:T(8,128)S(1)} %get-tuple-element.19.local, bf16[512,256]{1,0:T(8,128)(2,1)S(1)} %get-tuple-element.20.reads, bf16[512,512]{1,0:T(8,128)(2,1)S(1)} %get-tuple-element.21.gates, f32[512,128]{1,0:T(8,128)S(1)} %get-tuple-element.22.carry_decay, ...), custom_call_target="tpu_custom_call" | custom-call | tf_op jit(solution)/shard_map/output/pallas_call | solution.py:721
  114.3 0.8 copy.23
  (17 shorter events, 0.0 us)
Async XLA Ops:
  2.0 1.0 copy-start.2
  3.0 0.9 copy-start.6
  3.9 0.8 copy-start.9
  4.8 0.8 copy-start.10
  5.6 0.8 copy-start.11
  6.5 0.7 copy-start.14
  7.2 0.7 copy-start.15
  38.1 1.3 %copy-start = (bf16[512,2048]{1,0:T(8,128)(2,1)}, bf16[512,2048]{1,0:T(8,128)(2,1)S(1)}, u32[]{:S(2)}) copy-start(bf16[512,2048]{1,0:T(8,128)(2,1)S(1)} %get-tuple-element.14.gat) | copy-start | bytes 6291460
  39.4 1.2 %copy-start.4 = (bf16[2048,256]{1,0:T(8,128)(2,1)S(1)}, bf16[2048,256]{1,0:T(8,128)(2,1)}, u32[]{:S(2)}) copy-start(bf16[2048,256]{1,0:T(8,128)(2,1)} %w_write.1) | copy-start | bytes 3145732
  40.6 1.2 %copy-start.5 = (bf16[2048,256]{1,0:T(8,128)(2,1)S(1)}, bf16[2048,256]{1,0:T(8,128)(2,1)}, u32[]{:S(2)}) copy-start(bf16[2048,256]{1,0:T(8,128)(2,1)} %w_read.1) | copy-start | bytes 3145732
  41.9 0.8 copy-start.7
  42.7 0.8 copy-start.8
  43.5 0.8 copy-start.12
  44.3 0.8 copy-start.13
  45.0 49.5 %copy-start.1 = (bf16[512,2048]{1,0:T(8,128)(2,1)S(1)}, bf16[512,2048]{1,0:T(8,128)(2,1)}, u32[]{:S(2)}) copy-start(bf16[512,2048]{1,0:T(8,128)(2,1)} %w_out.1) | copy-start | bytes 6291460
  45.0 49.6 %copy-start.3 = (bf16[1,128,2048]{2,1,0:T(8,128)(2,1)S(1)}, bf16[1,128,2048]{2,1,0:T(8,128)(2,1)}, u32[]{:S(2)}) copy-start(bf16[1,128,2048]{2,1,0:T(8,128)(2,1)} %param.19) | copy-start | bytes 1572868
  45.1 49.6 %copy-start.16 = (f32[2048]{0:T(1024)S(1)}, f32[2048]{0:T(1024)}, u32[]{:S(2)}) copy-start(f32[2048]{0:T(1024)} %param.36) | copy-start | bytes 24580

commit v2 on v1

v2 whole, which is shorter than its diff:
```python
import jax
import jax.numpy as jnp
from jax import lax
from jax.experimental import pallas as pl
from jax.experimental.pallas import tpu as pltpu
from jax.sharding import Mesh
from jax.sharding import PartitionSpec as P

HEAD = 64
STATE = 128
ROW = 64
BLOCK = 128
HALO = 16
SP = ("sp_0", "sp_1")
SP_TP = ("sp_0", "sp_1", "tp")
NZ, NX, NY = 8, 4, 4
NS = NZ * NX

NORM_FLOOR = 1e-05
GATED_FLOOR = 1e-06
MESH = pl.DeviceIdType.MESH
F32 = jnp.float32
BF16 = jnp.bfloat16
HIGHEST = lax.Precision.HIGHEST
VMEM = pl.BlockSpec(memory_space=pltpu.VMEM)
ANY = pl.BlockSpec(memory_space=pl.ANY)


def silu(v):
    return v / (1.0 + jnp.exp(-v))


def remote(src, dst, send, recv, **where):
    return pltpu.make_async_remote_copy(
        src_ref=src, dst_ref=dst, send_sem=send, recv_sem=recv, device_id=where, device_id_type=MESH
    )


def position():
    return lax.axis_index("sp_0"), lax.axis_index("sp_1"), lax.axis_index("tp")


def lanes(start, size):
    return pl.ds(pl.multiple_of(start, 128), size)


def rows(start, size):
    return pl.ds(pl.multiple_of(start, 16), size)


def normed_rows(block, shift, scale):
    values = block.astype(F32)
    center = jnp.mean(values, -1, keepdims=True)
    off = values - center
    spread = jnp.mean(off * off, -1, keepdims=True)
    return (off * lax.rsqrt(spread + NORM_FLOOR) * (1.0 + scale) + shift).astype(BF16)


def conv_rows(pre, taps, run):
    length = pre.shape[0]
    at = lax.rem(lax.broadcasted_iota(jnp.int32, pre.shape, 0), run)
    total = pre * taps[2:3]
    for k in (0, 1, 3, 4):
        moved = pltpu.roll(pre, (2 - k) % length, 0)
        inside = (at + (k - 2) >= 0) & (at + (k - 2) < run)
        total = total + jnp.where(inside, moved, 0.0) * taps[k : k + 1]
    return silu(total)


def split2(v):
    high = v.astype(BF16)
    return high, (v - high.astype(F32)).astype(BF16)


def expand(v, spread):
    high, low = split2(v)
    return jnp.dot(high, spread, preferred_element_type=F32) + jnp.dot(
        low, spread, preferred_element_type=F32
    )


def softplus(v):
    return jnp.maximum(v, 0.0) + jnp.log1p(jnp.exp(-jnp.abs(v)))


def spread_matrix(spread):
    shape = spread.shape
    row = lax.broadcasted_iota(jnp.int32, shape, 0)
    col = lax.broadcasted_iota(jnp.int32, shape, 1)
    spread[...] = jnp.where(row == col // HEAD, 1.0, 0.0).astype(BF16)


def dot_on(a, b, ca, cb):
    return lax.dot_general(a, b, (((ca,), (cb,)), ((), ())), preferred_element_type=F32)


def mixer_kernel(
    lat_h, ctx_h, cond_h, ccond_h, shift_h, scale_h, gatem_h,
    wv_h, wg_h, ww_h, wr_h, ws_h, rate_h, pace_h, tv_h, tw_h, tr_h, gain_h, wo_h,
    out,
    cond, ccond, shift_m, scale_m, gate_m,
    w_value, w_gate, w_write, w_read, w_step, rates, pace, t_value, t_write, t_read, gain, w_out,
    part, zbuf, qbuf, ybuf, ybox, xbuf, fbuf, mod,
    gat, ctx_ext, hid, hid_c, val, wri, reads, gates, local,
    cum, stp, cdec, spread, inc, before, etot, tot,
    ends_s, ends_c, tot_s, tot_c, got_s, got_c, gtot_s, gtot_c, sent, start,
    inner, far, near_r, near_l, mine, got_far, got_r, got_l,
    in_sem, z_send, z_recv, y_send, y_recv, x_send, x_recv, g_send, g_recv,
    l_send, l_recv, f_send, f_recv, h_send, h_recv,
    s_send, s_recv, st_send, st_recv, c_send, c_recv, ct_send, ct_recv, b_send, b_recv,
    s1, r1, s2, r2,
):
    z, x, y = position()
    s = z * NX + x
    rank = s * NY + y
    right, left = lax.rem(y + 1, NY), lax.rem(y + NY - 1, NY)
    opposite = lax.rem(y + 2, NY)

    def at(t):
        return {"sp_0": t // NX, "sp_1": lax.rem(t, NX)}

    own_rows = gat.at[rows(y * 128, 128)]
    pairs = [
        (cond_h, cond), (ccond_h, ccond), (shift_h, shift_m), (scale_h, scale_m),
        (gatem_h, gate_m), (lat_h, own_rows), (ctx_h, ctx_ext.at[pl.ds(HALO, 2 * HALO)]),
        (wv_h, w_value), (ww_h, w_write), (ws_h, w_step), (rate_h, rates), (pace_h, pace),
        (tv_h, t_value), (tw_h, t_write), (wr_h, w_read), (wg_h, w_gate), (tr_h, t_read),
        (gain_h, gain), (wo_h, w_out),
    ]
    fetch = [pltpu.make_async_copy(a, b, in_sem.at[k]) for k, (a, b) in enumerate(pairs)]
    for copy in fetch:
        copy.start()

    barrier = pltpu.get_barrier_semaphore()

    def greet(p, none):
        pl.semaphore_signal(
            barrier, inc=1, device_id=at(lax.rem(s + p, NS)), device_id_type=MESH
        )
        return none

    lax.fori_loop(1, NS, greet, 0)
    for d in range(1, NY):
        pl.semaphore_signal(
            barrier, inc=1, device_id={"tp": lax.rem(y + d, NY)}, device_id_type=MESH
        )

    for copy in fetch[:5]:
        copy.wait()
    vec_row, vec_off = rank // 8, lax.rem(rank, 8) * 16
    lane = lax.broadcasted_iota(jnp.int32, (8, 128), 1)
    line = lax.broadcasted_iota(jnp.int32, (8, 128), 0)
    window = (lane >= vec_off) & (lane < vec_off + 16)
    both = jnp.where(
        line == 0,
        jnp.broadcast_to(cond[pl.ds(vec_row, 1), :], (8, 128)),
        jnp.broadcast_to(ccond[pl.ds(vec_row, 1), :], (8, 128)),
    )
    acts = jnp.where(window, silu(both), 0.0).astype(BF16)

    def product_of(matrix):
        tall = jnp.concatenate([matrix[...]] * 8, axis=0)
        return jnp.dot(acts, tall, preferred_element_type=F32)

    part[0:2, :] = product_of(shift_m)[0:2]
    part[2:4, :] = product_of(scale_m)[0:2]
    part[4:8, :] = product_of(gate_m)[0:4]
    fetch[5].wait()
    fetch[6].wait()
    pl.semaphore_wait(barrier, NS - 1 + NY - 1)

    z_copies = []
    for d in range(1, NZ):
        to = lax.rem(z + d, NZ)
        z_copies.append(
            remote(
                part.at[:, lanes(to * 256, 256)], zbuf.at[d - 1], z_send.at[d - 1],
                z_recv.at[d - 1], sp_0=to,
            )
        )
        z_copies[-1].start()

    l_copies = {}

    def latent_half(side, half):
        piece = gat.at[rows(y * 128 + half * 64, 64)]
        k = side * 2 + half
        copy = remote(
            piece, piece, l_send.at[k], l_recv.at[k], tp=right if side == 0 else left
        )
        copy.start()
        l_copies[side, half] = copy

    latent_half(0, 0)
    latent_half(1, 1)
    nxt, prv = lax.rem(s + 1, NS), lax.rem(s + NS - 1, NS)
    halo_next = remote(
        ctx_ext.at[pl.ds(2 * HALO, HALO)], ctx_ext.at[pl.ds(0, HALO)],
        h_send.at[0], h_recv.at[0], **at(nxt),
    )
    halo_prev = remote(
        ctx_ext.at[pl.ds(HALO, HALO)], ctx_ext.at[pl.ds(3 * HALO, HALO)],
        h_send.at[1], h_recv.at[1], **at(prv),
    )
    halo_next.start()
    halo_prev.start()

    total = part[:, lanes(z * 256, 256)]
    for d, copy in enumerate(z_copies):
        copy.wait()
        total = total + zbuf[d]
    qbuf[...] = total
    y_copies = []
    for d in range(1, NY):
        y_copies.append(
            remote(qbuf, ybuf.at[d - 1], y_send.at[d - 1], y_recv.at[d - 1], tp=lax.rem(y + d, NY))
        )
        y_copies[-1].start()
    latent_half(0, 1)
    latent_half(1, 0)

    spread_matrix(spread)
    heads = 8
    row64 = lax.broadcasted_iota(jnp.int32, (64, 128), 0)
    col64 = lax.broadcasted_iota(jnp.int32, (64, 128), 1)
    wanted = jnp.where(col64 < heads, y * heads + col64, 32 + y * heads + col64 - heads)
    pick = jnp.where((row64 == wanted) & (col64 < 2 * heads), 1.0, 0.0)
    pick16 = pick.astype(BF16)
    row = lax.broadcasted_iota(jnp.int32, (BLOCK, BLOCK), 0)
    col = lax.broadcasted_iota(jnp.int32, (BLOCK, BLOCK), 1)
    lower = jnp.where(col <= row, 1.0, 0.0)
    upper = jnp.where(col >= row, 1.0, 0.0)
    forward_lane = col < heads
    fl = forward_lane[0:1]

    for copy in y_copies:
        copy.wait()
    ybox[...] = (qbuf[...] + ybuf[0]) + (ybuf[1] + ybuf[2])
    x_copies = []
    for d in range(1, NX):
        x_copies.append(
            remote(
                ybox, xbuf.at[d - 1], x_send.at[d - 1], x_recv.at[d - 1], sp_1=lax.rem(x + d, NX)
            )
        )
        x_copies[-1].start()

    def forward(side):
        owner = left if side == 0 else right
        piece = gat.at[rows(owner * 128 + side * 64, 64)]
        return remote(
            piece, piece, f_send.at[side], f_recv.at[side], tp=right if side == 0 else left
        )

    for copy in x_copies:
        copy.wait()
    fbuf[...] = (ybox[...] + xbuf[0]) + (xbuf[1] + xbuf[2])
    g_copies = []
    for d in range(1, NZ):
        g_copies.append(
            remote(
                fbuf, mod.at[:, lanes(z * 256, 256)], g_send.at[d - 1], g_recv.at[d - 1],
                sp_0=lax.rem(z + d, NZ),
            )
        )
        g_copies[-1].start()
    mod[:, lanes(z * 256, 256)] = fbuf[...]

    ahead, back = forward(0), forward(1)
    l_copies[0, 0].wait_recv()
    ahead.start()
    l_copies[1, 1].wait_recv()
    back.start()

    for copy in fetch[7:]:
        copy.wait()
    rate_row = (
        jnp.dot(
            jnp.broadcast_to(rates[0:1, :], (8, 32)), pick[0:32], precision=HIGHEST,
            preferred_element_type=F32,
        )
        + jnp.dot(
            jnp.broadcast_to(rates[1:2, :], (8, 32)), pick[32:64], precision=HIGHEST,
            preferred_element_type=F32,
        )
    )[0:1]
    value_taps = t_value[:, lanes(y * 512, 512)]
    write_taps = t_write[:, lanes(y * 256, 256)]
    read_taps = t_read[:, lanes(y * 256, 256)]

    def steps_of(hidden):
        raw = dot_on(hidden, w_step[...], 1, 1).astype(BF16)
        return softplus(jnp.dot(raw, pick16, preferred_element_type=F32))

    for copy in g_copies:
        copy.wait()

    halo_next.wait()
    halo_prev.wait()
    for k in range(4):
        rs = pl.ds(k * HALO, HALO)
        hid_c[rs, :] = normed_rows(ctx_ext[rs, :], mod[1:2, :], mod[3:4, :])
    hidden_c = hid_c[...]
    line_c = lax.broadcasted_iota(jnp.int32, (4 * HALO, 1), 0)
    first = jnp.where(s == 0, HALO, 0)
    last = jnp.where(s == NS - 1, 3 * HALO, 4 * HALO)
    present = (line_c >= first) & (line_c < last)
    own_c = slice(HALO, 3 * HALO)
    cv = jnp.dot(hidden_c, w_value[...], preferred_element_type=F32).astype(BF16).astype(F32)
    cw = jnp.dot(hidden_c, w_write[...], preferred_element_type=F32).astype(BF16).astype(F32)
    cv = conv_rows(jnp.where(present, cv, 0.0), value_taps, 4 * HALO)[own_c].astype(BF16)
    cw = conv_rows(jnp.where(present, cw, 0.0), write_taps, 4 * HALO)[own_c].astype(BF16)
    cstep = steps_of(hidden_c)[own_c]
    cdecay = -rate_row * cstep
    r32 = lax.broadcasted_iota(jnp.int32, (2 * HALO, 2 * HALO), 0)
    c32 = lax.broadcasted_iota(jnp.int32, (2 * HALO, 2 * HALO), 1)
    later = jnp.dot(
        jnp.where(c32 > r32, 1.0, 0.0), cdecay, precision=HIGHEST, preferred_element_type=F32
    )
    earlier = jnp.dot(
        jnp.where(c32 < r32, 1.0, 0.0), cdecay, precision=HIGHEST, preferred_element_type=F32
    )
    cweight = jnp.exp(jnp.where(forward_lane[0 : 2 * HALO], later, earlier)) * cstep
    cvf = cv.astype(F32)
    cscaled = (jnp.concatenate([cvf, cvf], axis=1) * expand(cweight, spread[...])).astype(BF16)
    for g in range(2):
        wg = cw[:, g * 128 : (g + 1) * 128]
        for d in range(2):
            ls = slice((d * 2 + g) * 256, (d * 2 + g + 1) * 256)
            ends_c[:, ls] = dot_on(wg, cscaled[:, ls], 0, 0).astype(BF16)

    def expand3(v):
        high = v.astype(BF16)
        return jnp.dot(high, spread[...], preferred_element_type=F32) + expand(
            v - high.astype(F32), spread[...]
        )

    ctotal = jnp.broadcast_to(jnp.exp(jnp.sum(cdecay, axis=0, keepdims=True)), (8, 128))
    tot_c[...] = expand3(ctotal)[0:1]

    def state_copies(states, tots, got, gtot, a_send, a_recv, t_send, t_recv):
        def outgoing(p):
            t = lax.rem(s + p, NS)
            tz, tx = t // NX, lax.rem(t, NX)
            return (
                remote(
                    states.at[rows(tz * 16, 16), lanes(tx * 256, 256)], got.at[s],
                    a_send.at[t], a_recv.at[s], **at(t),
                ),
                remote(
                    tots.at[:, lanes(tx * 256, 256)], gtot.at[s],
                    t_send.at[t], t_recv.at[s], **at(t),
                ),
            )

        def send(p, none):
            for copy in outgoing(p):
                copy.start()
            return none

        def take(p, none):
            f = lax.rem(s + NS - p, NS)
            remote(got.at[f], got.at[f], a_send.at[f], a_recv.at[f], **at(f)).wait_recv()
            remote(gtot.at[f], gtot.at[f], t_send.at[f], t_recv.at[f], **at(f)).wait_recv()
            return none

        def done(p, none):
            for copy in outgoing(p):
                copy.wait_send()
            return none

        def keep():
            got[s] = states[rows(z * 16, 16), lanes(x * 256, 256)]
            gtot[s] = tots[:, lanes(x * 256, 256)]

        return send, take, done, keep

    send_c, take_c, done_c, keep_c = state_copies(
        ends_c, tot_c, got_c, gtot_c, c_send, c_recv, ct_send, ct_recv
    )
    lax.fori_loop(1, NS, send_c, 0)
    keep_c()

    def project(k, none):
        @pl.when(k == 1)
        def _():
            l_copies[0, 1].wait_recv()

        @pl.when(k == 2)
        def _():
            l_copies[1, 0].wait_recv()

        @pl.when(k == 3)
        def _():
            ahead.wait_recv()
            back.wait_recv()

        b = lax.rem(y + (lax.rem(k + 1, 3) + 1) * ((k + 3) // 4), NY)
        at_b = rows(b * 128, 128)

        def norm_part(i, none):
            rs = rows(b * 128 + i * 32, 32)
            hid[rs, :] = normed_rows(gat[rs, :], mod[0:1, :], mod[2:3, :])
            return none

        lax.fori_loop(0, 4, norm_part, 0)
        hidden = hid[at_b, :]
        pre = jnp.dot(hidden, w_value[...], preferred_element_type=F32).astype(BF16).astype(F32)
        vb = conv_rows(pre, value_taps, ROW).astype(BF16)
        val[at_b, :] = vb
        pre = jnp.dot(hidden, w_write[...], preferred_element_type=F32).astype(BF16).astype(F32)
        w = conv_rows(pre, write_taps, ROW).astype(BF16)
        wri[at_b, :] = w
        pace_row = pace[pl.ds(s * 4 + b, 1), :]
        step = steps_of(hidden) * jnp.transpose(jnp.broadcast_to(pace_row, (128, 128)))
        decay = -rate_row * step
        down = jnp.dot(lower, decay, precision=HIGHEST, preferred_element_type=F32)
        up = jnp.dot(upper, decay, precision=HIGHEST, preferred_element_type=F32)
        cums = jnp.where(forward_lane, down, up)
        total = jnp.where(fl, down[127:128], up[0:1])
        cum[at_b, :] = cums
        stp[at_b, :] = step
        weight = jnp.exp(total - cums) * step
        vf = vb.astype(F32)
        scaled = (jnp.concatenate([vf, vf], axis=1) * expand(weight, spread[...])).astype(BF16)
        for g in range(2):
            wg = w[:, g * 128 : (g + 1) * 128]
            for d in range(2):
                ls = slice((d * 2 + g) * 256, (d * 2 + g + 1) * 256)
                inc[b, :, ls] = dot_on(wg, scaled[:, ls], 0, 0)
        tot[pl.ds(b, 1), :] = total
        return none

    lax.fori_loop(0, 4, project, 0)

    t0, t1, t2, t3 = (tot[b : b + 1, :] for b in range(4))
    zero = jnp.zeros_like(t0)
    etot[...] = expand3(
        jnp.concatenate(
            [jnp.exp(t0), jnp.exp(t1), jnp.exp(t2), jnp.exp(t3), jnp.exp(t0 + t1 + t2 + t3),
             zero, zero, zero], axis=0,
        )
    )
    tot_s[...] = etot[4:5, :]
    tot[0:1, :] = jnp.where(fl, zero, t1 + t2 + t3)
    tot[1:2, :] = jnp.where(fl, t0, t2 + t3)
    tot[2:3, :] = jnp.where(fl, t0 + t1, t3)
    tot[3:4, :] = jnp.where(fl, t0 + t1 + t2, zero)
    for d, order in ((0, (0, 1, 2, 3)), (1, (3, 2, 1, 0))):
        for g in range(2):
            ls = slice((d * 2 + g) * 256, (d * 2 + g + 1) * 256)
            state = jnp.zeros((STATE, 256), F32)
            for b in order:
                before[b, :, ls] = state.astype(BF16)
                state = etot[b : b + 1, ls] * state + inc[b, :, ls]
            ends_s[:, ls] = state.astype(BF16)
    send_s, take_s, done_s, keep_s = state_copies(
        ends_s, tot_s, got_s, gtot_s, s_send, s_recv, st_send, st_recv
    )
    lax.fori_loop(1, NS, send_s, 0)
    keep_s()

    def within(b, none):
        at_b = rows(b * 128, 128)
        hidden = hid[at_b, :]
        pre = jnp.dot(hidden, w_read[...], preferred_element_type=F32).astype(BF16).astype(F32)
        rb = conv_rows(pre, read_taps, ROW).astype(BF16)
        reads[at_b, :] = rb
        gates[at_b, :] = silu(
            jnp.dot(hidden, w_gate[...], preferred_element_type=F32).astype(BF16).astype(F32)
        )
        cums = cum[at_b, :]
        step = stp[at_b, :]
        cums_t = jnp.transpose(cums)
        step_t = jnp.transpose(step)
        cdec[at_b, :] = jnp.exp(cums + tot[pl.ds(b, 1), :])
        grown = expand(jnp.exp(cums), spread[...])
        for g in range(2):
            r = rb[:, g * 128 : (g + 1) * 128]
            affinity = dot_on(r, wri[at_b, g * 128 : (g + 1) * 128], 1, 1)
            carried = jnp.zeros((128, 256), F32)
            for d in range(2):
                ls = slice((d * 2 + g) * 256, (d * 2 + g + 1) * 256)
                carried = carried + (
                    jnp.dot(r, before[b, :, ls], preferred_element_type=F32) * grown[:, ls]
                )
            for q in range(2):
                mixes = []
                for h in (g * 4 + q * 2, g * 4 + q * 2 + 1):
                    exponent = jnp.where(
                        col <= row,
                        cums[:, h : h + 1] - cums_t[h : h + 1, :],
                        cums[:, 8 + h : 9 + h] - cums_t[8 + h : 9 + h, :],
                    )
                    sf, sb = step_t[h : h + 1, :], step_t[8 + h : 9 + h, :]
                    amount = jnp.where(col < row, sf, jnp.where(col > row, sb, sf + sb))
                    mixes.append((affinity * jnp.exp(exponent) * amount).astype(BF16))
                ls = slice((g * 2 + q) * 128, (g * 2 + q + 1) * 128)
                pair = val[at_b, ls]
                none16 = jnp.zeros_like(pair)
                tall = jnp.concatenate(
                    [jnp.where(col < HEAD, pair, none16), jnp.where(col >= HEAD, pair, none16)],
                    axis=0,
                )
                got = jnp.dot(jnp.concatenate(mixes, axis=1), tall, preferred_element_type=F32)
                local[at_b, ls] = got + carried[:, q * 128 : (q + 1) * 128]
        return none

    lax.fori_loop(0, 4, within, 0)

    turned = x // 2

    def order_of(k):
        return k + turned * (NS - 1 - 2 * k)

    lax.fori_loop(1, NS, take_c, 0)

    def context_scan(k, state):
        j = order_of(k)
        return gtot_c[j] * state + got_c[j].astype(F32)

    state = lax.fori_loop(0, NS, context_scan, jnp.zeros((16, 256), F32))
    lax.fori_loop(1, NS, take_s, 0)

    def back_copy(j):
        return remote(
            sent.at[j], start.at[rows(z * 16, 16), lanes(x * 256, 256)],
            b_send.at[j], b_recv.at[s], **at(j),
        )

    def latent_scan(k, state):
        j = order_of(k)
        sent[j] = state.astype(BF16)

        @pl.when(j != s)
        def _():
            back_copy(j).start()

        return gtot_s[j] * state + got_s[j].astype(F32)

    lax.fori_loop(0, NS, latent_scan, state)
    start[rows(z * 16, 16), lanes(x * 256, 256)] = sent[s]

    def take_start(p, none):
        f = lax.rem(s + NS - p, NS)
        piece = start.at[rows((f // NX) * 16, 16), lanes(lax.rem(f, NX) * 256, 256)]
        remote(piece, piece, b_send.at[f], b_recv.at[f], **at(f)).wait_recv()
        return none

    lax.fori_loop(1, NS, take_start, 0)

    half = w_out.shape[1] // 2

    def make_inner(b):
        at_b = rows(b * 128, 128)
        grown = expand(cdec[at_b, :], spread[...])
        for g in range(2):
            r = reads[at_b, g * 128 : (g + 1) * 128]
            ch = slice(g * 256, (g + 1) * 256)
            total = local[at_b, ch]
            for d in range(2):
                ls = slice((d * 2 + g) * 256, (d * 2 + g + 1) * 256)
                total = total + jnp.dot(r, start[:, ls], preferred_element_type=F32) * grown[:, ls]
            gated = total * gates[at_b, ch]
            power = jnp.mean(gated * gated, -1, keepdims=True)
            gains = jnp.concatenate(
                [gain[pl.ds(y * 4 + g * 2, 1), :], gain[pl.ds(y * 4 + g * 2 + 1, 1), :]], axis=1
            )
            inner[:, ch] = (gated * lax.rsqrt(power + GATED_FLOOR) * gains).astype(BF16)

    def product(side):
        return jnp.dot(
            inner[...], w_out[:, side * half : (side + 1) * half], preferred_element_type=F32
        ).astype(BF16)

    make_inner(opposite)
    far[0] = product(0)
    far_r = remote(far.at[0], got_far.at[0], s1.at[0], r1.at[0], tp=right)
    far_r.start()
    far[1] = product(1)
    far_l = remote(far.at[1], got_far.at[1], s1.at[1], r1.at[1], tp=left)
    far_l.start()
    make_inner(right)
    near_r[1] = product(1)
    raw_r = remote(near_r.at[1], got_r.at[1], s2.at[0], r2.at[0], tp=right)
    raw_r.start()
    near_r[0] = product(0)
    make_inner(left)
    near_l[0] = product(0)
    raw_l = remote(near_l.at[0], got_l.at[0], s2.at[1], r2.at[1], tp=left)
    raw_l.start()
    near_l[1] = product(1)
    far_r.wait_recv()
    near_r[0] = (near_r[0].astype(F32) + got_far[0].astype(F32)).astype(BF16)
    sum_r = remote(near_r.at[0], got_r.at[0], s2.at[2], r2.at[2], tp=right)
    sum_r.start()
    far_l.wait_recv()
    near_l[1] = (near_l[1].astype(F32) + got_far[1].astype(F32)).astype(BF16)
    sum_l = remote(near_l.at[1], got_l.at[1], s2.at[3], r2.at[3], tp=left)
    sum_l.start()
    make_inner(y)
    mine[0] = product(0)
    mine[1] = product(1)

    def send_done(p, none):
        back_copy(lax.rem(s + p, NS)).wait_send()
        return done_s(p, done_c(p, none))

    lax.fori_loop(1, NS, send_done, 0)
    for copy in l_copies.values():
        copy.wait_send()
    ahead.wait_send()
    back.wait_send()

    def close(side):
        cs = slice(side * half, (side + 1) * half)
        mixed = (
            mine[side].astype(F32) + got_r[side].astype(F32) + got_l[side].astype(F32)
        ).astype(BF16)
        own = gat[rows(y * 128, 128), cs]
        out[:, cs] = (own.astype(F32) + mod[4:5, cs] * mixed.astype(F32)).astype(BF16)

    raw_r.wait_recv()
    raw_l.wait_recv()
    sum_r.wait_recv()
    sum_l.wait_recv()
    close(0)
    close(1)
    for copy in (far_r, far_l, raw_r, raw_l, sum_r, sum_l):
        copy.wait_send()


def mixer_call(*args):
    width = args[0].shape[1]
    tokens = NY * 128
    dma = pltpu.SemaphoreType.DMA
    vm = pltpu.VMEM
    copied = [vm(args[k].shape, args[k].dtype) for k in (2, 3, 4, 5, 6, 7, 8, 9, 10, 11, 12, 13,
                                                         14, 15, 16, 17, 18)]
    piece = vm((2, 128, width // 2), BF16)
    return pl.pallas_call(
        mixer_kernel,
        out_shape=jax.ShapeDtypeStruct((128, width), BF16),
        in_specs=[ANY] * 19,
        out_specs=VMEM,
        scratch_shapes=copied
        + [
            vm((8, width), F32), vm((NZ - 1, 8, 256), F32), vm((8, 256), F32),
            vm((NY - 1, 8, 256), F32), vm((8, 256), F32), vm((NX - 1, 8, 256), F32),
            vm((8, 256), F32), vm((8, width), F32),
            vm((tokens, width), BF16), vm((4 * HALO, width), BF16), vm((tokens, width), BF16),
            vm((4 * HALO, width), BF16), vm((tokens, 512), BF16), vm((tokens, 256), BF16),
            vm((tokens, 256), BF16), vm((tokens, 512), F32), vm((tokens, 512), F32),
            vm((tokens, 128), F32), vm((tokens, 128), F32), vm((tokens, 128), F32),
            vm((128, 1024), BF16), vm((4, STATE, 1024), F32), vm((4, STATE, 1024), BF16),
            vm((8, 1024), F32), vm((8, 128), F32),
            vm((STATE, 1024), BF16), vm((STATE, 1024), BF16), vm((1, 1024), F32),
            vm((1, 1024), F32), vm((NS, 16, 256), BF16), vm((NS, 16, 256), BF16),
            vm((NS, 1, 256), F32), vm((NS, 1, 256), F32), vm((NS, 16, 256), BF16),
            vm((STATE, 1024), BF16),
            vm((128, 512), BF16), piece, piece, piece, piece, piece, piece, piece,
            dma((19,)),
        ]
        + [dma((NZ - 1,))] * 2 + [dma((NY - 1,))] * 2 + [dma((NX - 1,))] * 2
        + [dma((NZ - 1,))] * 2
        + [dma((4,))] * 2 + [dma((2,))] * 2 + [dma((2,))] * 2
        + [dma((NS,))] * 10
        + [dma((2,)), dma((2,)), dma((4,)), dma((4,))],
        compiler_params=pltpu.CompilerParams(
            collective_id=0, has_side_effects=True, vmem_limit_bytes=60 << 20
        ),
        name="mixer",
    )(*args)


def per_device(
    latent, condition, context, context_cond, shift_matrix, scale_matrix, gate_matrix,
    value_proj, gate_proj, write_proj, read_proj, step_proj, decay_rate, pacing,
    value_taps, write_taps, read_taps, norm_gain, out_proj,
):
    width = latent.shape[2]
    updated = mixer_call(
        latent[0], context[0], condition.reshape(width // 128, 128),
        context_cond.reshape(width // 128, 128), shift_matrix, scale_matrix, gate_matrix,
        value_proj, gate_proj, write_proj, read_proj,
        step_proj.transpose(1, 2, 0).reshape(64, width), decay_rate, pacing.reshape(128, 128),
        value_taps, write_taps, read_taps, norm_gain.reshape(-1, 128), out_proj,
    )
    return updated[None]


def solution(mesh):
    torus = Mesh(
        mesh.devices.reshape(NZ, NX, mesh.shape["tp"], mesh.shape["dp"]),
        ("sp_0", "sp_1", "tp", "dp"),
    )
    placed = (
        P("dp", SP_TP, None), P("dp", None), P("dp", SP, None), P(),
        P(SP_TP, None), P(SP_TP, None), P(SP_TP, None),
        P(None, "tp"), P(None, "tp"), P(None, "tp"), P(None, "tp"),
        P(), P(), P("dp", None), P(), P(), P(), P(), P("tp", None),
    )
    return jax.shard_map(
        per_device, mesh=torus, in_specs=placed, out_specs=P("dp", SP_TP, None), check_vma=False
    )
```

time: 117 us -> 79.6 us (0.68); the launches traced: 115 us -> 79.2 us
  Pallas kernels: 99.4 us -> 77.3 us
  local copies, waits for them, and re-layouts: 15.6 us -> 1.88 us
    pallas_call x4 -> x1, Pallas kernels: 99.4 us -> 77.3 us  [mixer_call(): pl.pallas_call(mixer_kernel, out_shape=jax.ShapeDtypeStruct((128, width),...]
    unnamed x35 -> x1, local copies, waits for them, and re-layouts: 13.6 us -> 1.88 us
    reshape x2 -> x0, local copies, waits for them, and re-layouts: 1.98 us -> none  [the longest x1 1.22 us: per_device(): step_proj.reshape(width, 64)]
where the time goes in v2:
time: 79.6 us; the launch traced here: 79.2 us
  Pallas kernels  77.3 us (97%)
  local copies, waits for them, and re-layouts  1.88 us (2%)
    pallas_call x1, Pallas kernels, mixer_call(): pl.pallas_call(mixer_kernel, out_shape=jax.ShapeDtypeStruct((128, width),...  77.3 us
    unnamed x1, local copies, waits for them, and re-layouts  1.88 us

profile of v2, /device:TPU:8, one launch (start us, length us, event | category | flops | bytes accessed | tf_op | source)
XLA Modules:
  0.0 79.2 jit_solution(14059026983934227619)
XLA Ops:
  0.0 77.3 %mixer.1 = bf16[128,2048]{1,0:T(8,128)(2,1)} custom-call(bf16[128,2048]{1,0:T(8,128)(2,1)} %bitcast.11, bf16[32,2048]{1,0:T(8,128)(2,1)} %bitcast.13, f32[16,128]{1,0:T(8,128)} %bitcast.15, f32[16,128]{1,0:T(8,128)} %bitcast.16, bf16[16,2048]{1,0:T(8,128)(2,1)} %shift_h.1, bf16[16,2048]{1,0:T(8,128)(2,1)} %scale_h.1, bf16[16,2048]{1,0:T(8,128)(2,1)} %gatem_h.1, ...), custom_call_target="tpu_custom_call" | custom-call | tf_op jit(solution)/shard_map/mixer/pallas_call | solution.py:641
  77.4 1.9 %copy.21 = bf16[1,128,2048]{2,1,0:T(8,128)(2,1)} copy(bf16[1,128,2048]{2,1,0:T(8,128)(2,1)} %bitcast.10) | data formatting | bytes 1048576

commit v3 on v2

--- a/solution.py
+++ b/solution.py
@@ -48,12 +48,12 @@
     return pl.ds(pl.multiple_of(start, 16), size)
 
 
-def normed_rows(block, shift, scale):
+def normed_rows(block):
     values = block.astype(F32)
     center = jnp.mean(values, -1, keepdims=True)
     off = values - center
     spread = jnp.mean(off * off, -1, keepdims=True)
-    return (off * lax.rsqrt(spread + NORM_FLOOR) * (1.0 + scale) + shift).astype(BF16)
+    return off * lax.rsqrt(spread + NORM_FLOOR)
 
 
 def conv_rows(pre, taps, run):
@@ -67,16 +67,19 @@
     return silu(total)
 
 
-def split2(v):
+def expand(v, spread):
     high = v.astype(BF16)
-    return high, (v - high.astype(F32)).astype(BF16)
-
-
-def expand(v, spread):
-    high, low = split2(v)
-    return jnp.dot(high, spread, preferred_element_type=F32) + jnp.dot(
-        low, spread, preferred_element_type=F32
-    )
+    low = (v - high.astype(F32)).astype(BF16)
+    return jnp.dot(
+        jnp.concatenate([high, low], axis=1), spread, preferred_element_type=F32
+    )
+
+
+def three_parts(v):
+    high = v.astype(BF16)
+    rest = v - high.astype(F32)
+    mid = rest.astype(BF16)
+    return high, mid, (rest - mid.astype(F32)).astype(BF16)
 
 
 def softplus(v):
@@ -85,7 +88,7 @@
 
 def spread_matrix(spread):
     shape = spread.shape
-    row = lax.broadcasted_iota(jnp.int32, shape, 0)
+    row = lax.rem(lax.broadcasted_iota(jnp.int32, shape, 0), 128)
     col = lax.broadcasted_iota(jnp.int32, shape, 1)
     spread[...] = jnp.where(row == col // HEAD, 1.0, 0.0).astype(BF16)
 
@@ -99,15 +102,15 @@
     wv_h, wg_h, ww_h, wr_h, ws_h, rate_h, pace_h, tv_h, tw_h, tr_h, gain_h, wo_h,
     out,
     cond, ccond, shift_m, scale_m, gate_m,
-    w_value, w_gate, w_write, w_read, w_step, rates, pace, t_value, t_write, t_read, gain, w_out,
-    part, zbuf, qbuf, ybuf, ybox, xbuf, fbuf, mod,
-    gat, ctx_ext, hid, hid_c, val, wri, reads, gates, local,
-    cum, stp, cdec, spread, inc, before, etot, tot,
-    ends_s, ends_c, tot_s, tot_c, got_s, got_c, gtot_s, gtot_c, sent, start,
+    w_first, w_second, w_step, rates, pace, t_value, t_write, t_read, gain, w_out,
+    part, zbuf, qbuf, xybuf, fbuf, mod,
+    gat, ctx_ext, nrm, hid, pre_a, pre_b, val, wri, reads, gates, local,
+    cum, stp, cdec, pcol, grown_c, spread, inc, before, etot, tot,
+    ends_s, ends_c, tot_b, got_s, got_c, gtot, sent, start,
     inner, far, near_r, near_l, mine, got_far, got_r, got_l,
-    in_sem, z_send, z_recv, y_send, y_recv, x_send, x_recv, g_send, g_recv,
+    in_sem, z_send, z_recv, xy_send, xy_recv, g_send, g_recv,
     l_send, l_recv, f_send, f_recv, h_send, h_recv,
-    s_send, s_recv, st_send, st_recv, c_send, c_recv, ct_send, ct_recv, b_send, b_recv,
+    s_send, s_recv, t_send, t_recv, c_send, c_recv, b_send, b_recv,
     s1, r1, s2, r2,
 ):
     z, x, y = position()
@@ -115,16 +118,25 @@
     rank = s * NY + y
     right, left = lax.rem(y + 1, NY), lax.rem(y + NY - 1, NY)
     opposite = lax.rem(y + 2, NY)
+    heads = 8
 
     def at(t):
         return {"sp_0": t // NX, "sp_1": lax.rem(t, NX)}
+
+    def at_xy(q, sign):
+        return {
+            "sp_1": lax.rem(x + NX + sign * (q // NY), NX),
+            "tp": lax.rem(y + NY + sign * lax.rem(q, NY), NY),
+        }
 
     own_rows = gat.at[rows(y * 128, 128)]
     pairs = [
         (cond_h, cond), (ccond_h, ccond), (shift_h, shift_m), (scale_h, scale_m),
         (gatem_h, gate_m), (lat_h, own_rows), (ctx_h, ctx_ext.at[pl.ds(HALO, 2 * HALO)]),
-        (wv_h, w_value), (ww_h, w_write), (ws_h, w_step), (rate_h, rates), (pace_h, pace),
-        (tv_h, t_value), (tw_h, t_write), (wr_h, w_read), (wg_h, w_gate), (tr_h, t_read),
+        (ws_h, w_step), (rate_h, rates), (pace_h, pace),
+        (wv_h, w_first.at[:, pl.ds(0, 512)]), (ww_h, w_first.at[:, pl.ds(512, 256)]),
+        (tv_h, t_value), (tw_h, t_write), (wr_h, w_second.at[:, pl.ds(0, 256)]),
+        (wg_h, w_second.at[:, pl.ds(256, 512)]), (tr_h, t_read),
         (gain_h, gain), (wo_h, w_out),
     ]
     fetch = [pltpu.make_async_copy(a, b, in_sem.at[k]) for k, (a, b) in enumerate(pairs)]
@@ -140,10 +152,15 @@
         return none
 
     lax.fori_loop(1, NS, greet, 0)
-    for d in range(1, NY):
-        pl.semaphore_signal(
-            barrier, inc=1, device_id={"tp": lax.rem(y + d, NY)}, device_id_type=MESH
-        )
+
+    def greet_xy(q, none):
+        @pl.when(lax.rem(q, NY) != 0)
+        def _():
+            pl.semaphore_signal(barrier, inc=1, device_id=at_xy(q, 1), device_id_type=MESH)
+
+        return none
+
+    lax.fori_loop(1, NX * NY, greet_xy, 0)
 
     for copy in fetch[:5]:
         copy.wait()
@@ -167,7 +184,20 @@
     part[4:8, :] = product_of(gate_m)[0:4]
     fetch[5].wait()
     fetch[6].wait()
-    pl.semaphore_wait(barrier, NS - 1 + NY - 1)
+
+    def norm_at(base, count):
+        def chunk(i, none):
+            rs = rows(base + i * 32, 32)
+            nrm[rs, :] = normed_rows(gat[rs, :])
+            return none
+
+        lax.fori_loop(0, count // 32, chunk, 0)
+
+    def norm_ctx(base):
+        nrm[pl.ds(512 + base, HALO), :] = normed_rows(ctx_ext[pl.ds(base, HALO), :])
+
+    norm_at(y * 128, 64)
+    pl.semaphore_wait(barrier, NS - 1 + NX * (NY - 1))
 
     z_copies = []
     for d in range(1, NZ):
@@ -193,6 +223,14 @@
 
     latent_half(0, 0)
     latent_half(1, 1)
+
+    def latent_ahead(side):
+        owner = left if side == 0 else right
+        piece = gat.at[rows(owner * 128 + side * 64, 64)]
+        return remote(
+            piece, piece, f_send.at[side], f_recv.at[side], tp=right if side == 0 else left
+        )
+
     nxt, prv = lax.rem(s + 1, NS), lax.rem(s + NS - 1, NS)
     halo_next = remote(
         ctx_ext.at[pl.ds(2 * HALO, HALO)], ctx_ext.at[pl.ds(0, HALO)],
@@ -204,59 +242,66 @@
     )
     halo_next.start()
     halo_prev.start()
+
+    norm_at(y * 128 + 64, 64)
+    norm_ctx(HALO)
+    norm_ctx(2 * HALO)
+    spread_matrix(spread)
+    row64 = lax.broadcasted_iota(jnp.int32, (64, 128), 0)
+    col64 = lax.broadcasted_iota(jnp.int32, (64, 128), 1)
+    wanted = jnp.where(col64 < heads, y * heads + col64, 32 + y * heads + col64 - heads)
+    pick = jnp.where((row64 == wanted) & (col64 < 2 * heads), 1.0, 0.0)
+    row = lax.broadcasted_iota(jnp.int32, (BLOCK, BLOCK), 0)
+    col = lax.broadcasted_iota(jnp.int32, (BLOCK, BLOCK), 1)
+    lower = jnp.where(col <= row, 1.0, 0.0).astype(BF16)
+    upper = jnp.where(col >= row, 1.0, 0.0).astype(BF16)
+    forward_lane = col < heads
+    fl = forward_lane[0:1]
+    for copy in fetch[7:10]:
+        copy.wait()
+    w_first[:, 768:896] = dot_on(w_step[...], pick.astype(BF16), 0, 0).astype(BF16)
+    for b in range(4):
+        pace_row = pace[pl.ds(s * 4 + b, 1), :]
+        pcol[b * 128 : (b + 1) * 128, :] = jnp.transpose(
+            jnp.broadcast_to(pace_row, (128, 128))
+        )
 
     total = part[:, lanes(z * 256, 256)]
     for d, copy in enumerate(z_copies):
         copy.wait()
         total = total + zbuf[d]
     qbuf[...] = total
-    y_copies = []
-    for d in range(1, NY):
-        y_copies.append(
-            remote(qbuf, ybuf.at[d - 1], y_send.at[d - 1], y_recv.at[d - 1], tp=lax.rem(y + d, NY))
-        )
-        y_copies[-1].start()
+    def xy_copy(q):
+        return remote(qbuf, xybuf.at[q], xy_send.at[q], xy_recv.at[q], **at_xy(q, 1))
+
+    def send_xy(k, none):
+        xy_copy(NX * NY - 1 - k).start()
+        return none
+
+    lax.fori_loop(0, NX * NY - 1, send_xy, 0)
     latent_half(0, 1)
     latent_half(1, 0)
 
-    spread_matrix(spread)
-    heads = 8
-    row64 = lax.broadcasted_iota(jnp.int32, (64, 128), 0)
-    col64 = lax.broadcasted_iota(jnp.int32, (64, 128), 1)
-    wanted = jnp.where(col64 < heads, y * heads + col64, 32 + y * heads + col64 - heads)
-    pick = jnp.where((row64 == wanted) & (col64 < 2 * heads), 1.0, 0.0)
-    pick16 = pick.astype(BF16)
-    row = lax.broadcasted_iota(jnp.int32, (BLOCK, BLOCK), 0)
-    col = lax.broadcasted_iota(jnp.int32, (BLOCK, BLOCK), 1)
-    lower = jnp.where(col <= row, 1.0, 0.0)
-    upper = jnp.where(col >= row, 1.0, 0.0)
-    forward_lane = col < heads
-    fl = forward_lane[0:1]
-
-    for copy in y_copies:
-        copy.wait()
-    ybox[...] = (qbuf[...] + ybuf[0]) + (ybuf[1] + ybuf[2])
-    x_copies = []
-    for d in range(1, NX):
-        x_copies.append(
-            remote(
-                ybox, xbuf.at[d - 1], x_send.at[d - 1], x_recv.at[d - 1], sp_1=lax.rem(x + d, NX)
-            )
-        )
-        x_copies[-1].start()
-
-    def forward(side):
-        owner = left if side == 0 else right
-        piece = gat.at[rows(owner * 128 + side * 64, 64)]
-        return remote(
-            piece, piece, f_send.at[side], f_recv.at[side], tp=right if side == 0 else left
-        )
-
-    for copy in x_copies:
-        copy.wait()
-    fbuf[...] = (ybox[...] + xbuf[0]) + (xbuf[1] + xbuf[2])
+    l_copies[0, 0].wait_recv()
+    ahead = latent_ahead(0)
+    ahead.start()
+    l_copies[1, 1].wait_recv()
+    back = latent_ahead(1)
+    back.start()
+    norm_at(left * 128, 64)
+    norm_at(right * 128 + 64, 64)
+
+    def wait_xy(q, none):
+        xy_copy(q).wait()
+        return none
+
+    lax.fori_loop(1, NX * NY, wait_xy, 0)
+    total = qbuf[...]
+    for q in range(1, NX * NY):
+        total = total + xybuf[q]
+    fbuf[...] = total
     g_copies = []
-    for d in range(1, NZ):
+    for d in (4, 3, 5, 2, 6, 1, 7):
         g_copies.append(
             remote(
                 fbuf, mod.at[:, lanes(z * 256, 256)], g_send.at[d - 1], g_recv.at[d - 1],
@@ -264,15 +309,18 @@
             )
         )
         g_copies[-1].start()
-    mod[:, lanes(z * 256, 256)] = fbuf[...]
-
-    ahead, back = forward(0), forward(1)
-    l_copies[0, 0].wait_recv()
-    ahead.start()
-    l_copies[1, 1].wait_recv()
-    back.start()
-
-    for copy in fetch[7:]:
+    mod[:, lanes(z * 256, 256)] = total
+
+    halo_next.wait()
+    halo_prev.wait()
+    norm_ctx(0)
+    norm_ctx(3 * HALO)
+    l_copies[0, 1].wait_recv()
+    l_copies[1, 0].wait_recv()
+    norm_at(left * 128 + 64, 64)
+    norm_at(right * 128, 64)
+
+    for copy in fetch[10:]:
         copy.wait()
     rate_row = (
         jnp.dot(
@@ -288,38 +336,54 @@
     write_taps = t_write[:, lanes(y * 256, 256)]
     read_taps = t_read[:, lanes(y * 256, 256)]
 
-    def steps_of(hidden):
-        raw = dot_on(hidden, w_step[...], 1, 1).astype(BF16)
-        return softplus(jnp.dot(raw, pick16, preferred_element_type=F32))
-
     for copy in g_copies:
         copy.wait()
 
-    halo_next.wait()
-    halo_prev.wait()
-    for k in range(4):
-        rs = pl.ds(k * HALO, HALO)
-        hid_c[rs, :] = normed_rows(ctx_ext[rs, :], mod[1:2, :], mod[3:4, :])
-    hidden_c = hid_c[...]
+    def modulate(b, none):
+        def chunk(i, none):
+            rs = rows(b * 128 + i * 32, 32)
+            hid[rs, :] = (nrm[rs, :] * (1.0 + mod[2:3, :]) + mod[0:1, :]).astype(BF16)
+            return none
+
+        lax.fori_loop(0, 4, chunk, 0)
+        return none
+
+    modulate(y, 0)
+    modulate(left, 0)
+    modulate(right, 0)
+    for k in range(2):
+        rs = pl.ds(512 + k * 32, 32)
+        hid[rs, :] = (nrm[rs, :] * (1.0 + mod[3:4, :]) + mod[1:2, :]).astype(BF16)
+    ahead.wait_recv()
+    back.wait_recv()
+    norm_at(opposite * 128, 128)
+    modulate(opposite, 0)
+
+    for c in (slice(0, 256), slice(256, 512), slice(512, 768), slice(768, 896)):
+        pre_a[:, c] = jnp.dot(hid[...], w_first[:, c], preferred_element_type=F32).astype(BF16)
+
     line_c = lax.broadcasted_iota(jnp.int32, (4 * HALO, 1), 0)
     first = jnp.where(s == 0, HALO, 0)
     last = jnp.where(s == NS - 1, 3 * HALO, 4 * HALO)
     present = (line_c >= first) & (line_c < last)
     own_c = slice(HALO, 3 * HALO)
-    cv = jnp.dot(hidden_c, w_value[...], preferred_element_type=F32).astype(BF16).astype(F32)
-    cw = jnp.dot(hidden_c, w_write[...], preferred_element_type=F32).astype(BF16).astype(F32)
+    cv = pre_a[512:576, 0:512].astype(F32)
+    cw = pre_a[512:576, 512:768].astype(F32)
     cv = conv_rows(jnp.where(present, cv, 0.0), value_taps, 4 * HALO)[own_c].astype(BF16)
     cw = conv_rows(jnp.where(present, cw, 0.0), write_taps, 4 * HALO)[own_c].astype(BF16)
-    cstep = steps_of(hidden_c)[own_c]
+    cstep = softplus(pre_a[512 + HALO : 512 + 3 * HALO, 768:896].astype(F32))
     cdecay = -rate_row * cstep
     r32 = lax.broadcasted_iota(jnp.int32, (2 * HALO, 2 * HALO), 0)
     c32 = lax.broadcasted_iota(jnp.int32, (2 * HALO, 2 * HALO), 1)
-    later = jnp.dot(
-        jnp.where(c32 > r32, 1.0, 0.0), cdecay, precision=HIGHEST, preferred_element_type=F32
-    )
-    earlier = jnp.dot(
-        jnp.where(c32 < r32, 1.0, 0.0), cdecay, precision=HIGHEST, preferred_element_type=F32
-    )
+    cparts = jnp.concatenate(three_parts(cdecay), axis=1)
+
+    def ctx_sum(allowed):
+        got = jnp.dot(
+            jnp.where(allowed, 1.0, 0.0).astype(BF16), cparts, preferred_element_type=F32
+        )
+        return got[:, 0:128] + got[:, 128:256] + got[:, 256:384]
+
+    later, earlier = ctx_sum(c32 > r32), ctx_sum(c32 < r32)
     cweight = jnp.exp(jnp.where(forward_lane[0 : 2 * HALO], later, earlier)) * cstep
     cvf = cv.astype(F32)
     cscaled = (jnp.concatenate([cvf, cvf], axis=1) * expand(cweight, spread[...])).astype(BF16)
@@ -331,93 +395,54 @@
 
     def expand3(v):
         high = v.astype(BF16)
-        return jnp.dot(high, spread[...], preferred_element_type=F32) + expand(
-            v - high.astype(F32), spread[...]
-        )
-
-    ctotal = jnp.broadcast_to(jnp.exp(jnp.sum(cdecay, axis=0, keepdims=True)), (8, 128))
-    tot_c[...] = expand3(ctotal)[0:1]
-
-    def state_copies(states, tots, got, gtot, a_send, a_recv, t_send, t_recv):
+        rest = v - high.astype(F32)
+        return jnp.dot(high, spread[0:128, :], preferred_element_type=F32) + expand(
+            rest, spread[...]
+        )
+
+    ctotal = jnp.exp(jnp.sum(cdecay, axis=0, keepdims=True))
+
+    def far_first(k):
+        return NS // 2 + ((k + 1) // 2) * (1 - 2 * lax.rem(k, 2))
+
+    def state_copies(states, got, a_send, a_recv):
         def outgoing(p):
             t = lax.rem(s + p, NS)
-            tz, tx = t // NX, lax.rem(t, NX)
-            return (
-                remote(
-                    states.at[rows(tz * 16, 16), lanes(tx * 256, 256)], got.at[s],
-                    a_send.at[t], a_recv.at[s], **at(t),
-                ),
-                remote(
-                    tots.at[:, lanes(tx * 256, 256)], gtot.at[s],
-                    t_send.at[t], t_recv.at[s], **at(t),
-                ),
+            return remote(
+                states.at[rows((t // NX) * 16, 16), lanes(lax.rem(t, NX) * 256, 256)],
+                got.at[s], a_send.at[t], a_recv.at[s], **at(t),
             )
-
-        def send(p, none):
-            for copy in outgoing(p):
-                copy.start()
-            return none
 
         def take(p, none):
             f = lax.rem(s + NS - p, NS)
             remote(got.at[f], got.at[f], a_send.at[f], a_recv.at[f], **at(f)).wait_recv()
-            remote(gtot.at[f], gtot.at[f], t_send.at[f], t_recv.at[f], **at(f)).wait_recv()
             return none
 
-        def done(p, none):
-            for copy in outgoing(p):
-                copy.wait_send()
-            return none
-
-        def keep():
-            got[s] = states[rows(z * 16, 16), lanes(x * 256, 256)]
-            gtot[s] = tots[:, lanes(x * 256, 256)]
-
-        return send, take, done, keep
-
-    send_c, take_c, done_c, keep_c = state_copies(
-        ends_c, tot_c, got_c, gtot_c, c_send, c_recv, ct_send, ct_recv
-    )
-    lax.fori_loop(1, NS, send_c, 0)
-    keep_c()
-
-    def project(k, none):
-        @pl.when(k == 1)
-        def _():
-            l_copies[0, 1].wait_recv()
-
-        @pl.when(k == 2)
-        def _():
-            l_copies[1, 0].wait_recv()
-
-        @pl.when(k == 3)
-        def _():
-            ahead.wait_recv()
-            back.wait_recv()
-
-        b = lax.rem(y + (lax.rem(k + 1, 3) + 1) * ((k + 3) // 4), NY)
+        return outgoing, take
+
+    out_c, take_c = state_copies(ends_c, got_c, c_send, c_recv)
+
+    def send_c(k, none):
+        out_c(far_first(k)).start()
+        return none
+
+    lax.fori_loop(0, NS - 1, send_c, 0)
+    got_c[s] = ends_c[rows(z * 16, 16), lanes(x * 256, 256)]
+
+    def block_states(b, none):
         at_b = rows(b * 128, 128)
-
-        def norm_part(i, none):
-            rs = rows(b * 128 + i * 32, 32)
-            hid[rs, :] = normed_rows(gat[rs, :], mod[0:1, :], mod[2:3, :])
-            return none
-
-        lax.fori_loop(0, 4, norm_part, 0)
-        hidden = hid[at_b, :]
-        pre = jnp.dot(hidden, w_value[...], preferred_element_type=F32).astype(BF16).astype(F32)
-        vb = conv_rows(pre, value_taps, ROW).astype(BF16)
+        vb = conv_rows(pre_a[at_b, 0:512].astype(F32), value_taps, ROW).astype(BF16)
         val[at_b, :] = vb
-        pre = jnp.dot(hidden, w_write[...], preferred_element_type=F32).astype(BF16).astype(F32)
-        w = conv_rows(pre, write_taps, ROW).astype(BF16)
+        w = conv_rows(pre_a[at_b, 512:768].astype(F32), write_taps, ROW).astype(BF16)
         wri[at_b, :] = w
-        pace_row = pace[pl.ds(s * 4 + b, 1), :]
-        step = steps_of(hidden) * jnp.transpose(jnp.broadcast_to(pace_row, (128, 128)))
+        step = softplus(pre_a[at_b, 768:896].astype(F32)) * pcol[at_b, :]
         decay = -rate_row * step
-        down = jnp.dot(lower, decay, precision=HIGHEST, preferred_element_type=F32)
-        up = jnp.dot(upper, decay, precision=HIGHEST, preferred_element_type=F32)
-        cums = jnp.where(forward_lane, down, up)
-        total = jnp.where(fl, down[127:128], up[0:1])
+        parts = jnp.concatenate(three_parts(decay), axis=1)
+        down = jnp.dot(lower, parts, preferred_element_type=F32)
+        up = jnp.dot(upper, parts, preferred_element_type=F32)
+        both = jnp.where(jnp.concatenate([forward_lane] * 3, axis=1), down, up)
+        cums = both[:, 0:128] + both[:, 128:256] + both[:, 256:384]
+        total = jnp.where(fl, cums[127:128], cums[0:1])
         cum[at_b, :] = cums
         stp[at_b, :] = step
         weight = jnp.exp(total - cums) * step
@@ -431,17 +456,17 @@
         tot[pl.ds(b, 1), :] = total
         return none
 
-    lax.fori_loop(0, 4, project, 0)
+    lax.fori_loop(0, 4, block_states, 0)
 
     t0, t1, t2, t3 = (tot[b : b + 1, :] for b in range(4))
     zero = jnp.zeros_like(t0)
     etot[...] = expand3(
         jnp.concatenate(
             [jnp.exp(t0), jnp.exp(t1), jnp.exp(t2), jnp.exp(t3), jnp.exp(t0 + t1 + t2 + t3),
-             zero, zero, zero], axis=0,
-        )
-    )
-    tot_s[...] = etot[4:5, :]
+             ctotal, zero, zero], axis=0,
+        )
+    )
+    tot_b[...] = etot[4:6, :]
     tot[0:1, :] = jnp.where(fl, zero, t1 + t2 + t3)
     tot[1:2, :] = jnp.where(fl, t0, t2 + t3)
     tot[2:3, :] = jnp.where(fl, t0 + t1, t3)
@@ -454,21 +479,33 @@
                 before[b, :, ls] = state.astype(BF16)
                 state = etot[b : b + 1, ls] * state + inc[b, :, ls]
             ends_s[:, ls] = state.astype(BF16)
-    send_s, take_s, done_s, keep_s = state_copies(
-        ends_s, tot_s, got_s, gtot_s, s_send, s_recv, st_send, st_recv
-    )
-    lax.fori_loop(1, NS, send_s, 0)
-    keep_s()
+    out_s, take_s = state_copies(ends_s, got_s, s_send, s_recv)
+
+    def out_t(p):
+        t = lax.rem(s + p, NS)
+        return remote(
+            tot_b.at[:, lanes(lax.rem(t, NX) * 256, 256)], gtot.at[s],
+            t_send.at[t], t_recv.at[s], **at(t),
+        )
+
+    def send_s(k, none):
+        out_s(far_first(k)).start()
+        out_t(far_first(k)).start()
+        return none
+
+    lax.fori_loop(0, NS - 1, send_s, 0)
+    got_s[s] = ends_s[rows(z * 16, 16), lanes(x * 256, 256)]
+    gtot[s] = tot_b[:, lanes(x * 256, 256)]
+
+    for c in (slice(0, 256), slice(256, 512), slice(512, 768)):
+        pre_b[:, c] = jnp.dot(
+            hid[0:512, :], w_second[:, c], preferred_element_type=F32
+        ).astype(BF16)
 
     def within(b, none):
         at_b = rows(b * 128, 128)
-        hidden = hid[at_b, :]
-        pre = jnp.dot(hidden, w_read[...], preferred_element_type=F32).astype(BF16).astype(F32)
-        rb = conv_rows(pre, read_taps, ROW).astype(BF16)
+        rb = conv_rows(pre_b[at_b, 0:256].astype(F32), read_taps, ROW).astype(BF16)
         reads[at_b, :] = rb
-        gates[at_b, :] = silu(
-            jnp.dot(hidden, w_gate[...], preferred_element_type=F32).astype(BF16).astype(F32)
-        )
         cums = cum[at_b, :]
         step = stp[at_b, :]
         cums_t = jnp.transpose(cums)
@@ -513,11 +550,17 @@
     def order_of(k):
         return k + turned * (NS - 1 - 2 * k)
 
+    def take_t(p, none):
+        f = lax.rem(s + NS - p, NS)
+        remote(gtot.at[f], gtot.at[f], t_send.at[f], t_recv.at[f], **at(f)).wait_recv()
+        return none
+
     lax.fori_loop(1, NS, take_c, 0)
+    lax.fori_loop(1, NS, take_t, 0)
 
     def context_scan(k, state):
         j = order_of(k)
-        return gtot_c[j] * state + got_c[j].astype(F32)
+        return gtot[j, 1:2, :] * state + got_c[j].astype(F32)
 
     state = lax.fori_loop(0, NS, context_scan, jnp.zeros((16, 256), F32))
     lax.fori_loop(1, NS, take_s, 0)
@@ -536,10 +579,18 @@
         def _():
             back_copy(j).start()
 
-        return gtot_s[j] * state + got_s[j].astype(F32)
+        return gtot[j, 0:1, :] * state + got_s[j].astype(F32)
 
     lax.fori_loop(0, NS, latent_scan, state)
     start[rows(z * 16, 16), lanes(x * 256, 256)] = sent[s]
+
+    def last_tables(b, none):
+        at_b = rows(b * 128, 128)
+        grown_c[at_b, :] = expand(cdec[at_b, :], spread[...])
+        gates[at_b, :] = silu(pre_b[at_b, 256:768].astype(F32))
+        return none
+
+    lax.fori_loop(0, 4, last_tables, 0)
 
     def take_start(p, none):
         f = lax.rem(s + NS - p, NS)
@@ -553,14 +604,15 @@
 
     def make_inner(b):
         at_b = rows(b * 128, 128)
-        grown = expand(cdec[at_b, :], spread[...])
         for g in range(2):
             r = reads[at_b, g * 128 : (g + 1) * 128]
             ch = slice(g * 256, (g + 1) * 256)
             total = local[at_b, ch]
             for d in range(2):
                 ls = slice((d * 2 + g) * 256, (d * 2 + g + 1) * 256)
-                total = total + jnp.dot(r, start[:, ls], preferred_element_type=F32) * grown[:, ls]
+                total = total + jnp.dot(r, start[:, ls], preferred_element_type=F32) * (
+                    grown_c[at_b, ls]
+                )
             gated = total * gates[at_b, ch]
             power = jnp.mean(gated * gated, -1, keepdims=True)
             gains = jnp.concatenate(
@@ -604,7 +656,10 @@
 
     def send_done(p, none):
         back_copy(lax.rem(s + p, NS)).wait_send()
-        return done_s(p, done_c(p, none))
+        out_s(p).wait_send()
+        out_t(p).wait_send()
+        out_c(p).wait_send()
+        return none
 
     lax.fori_loop(1, NS, send_done, 0)
     for copy in l_copies.values():
@@ -635,8 +690,8 @@
     tokens = NY * 128
     dma = pltpu.SemaphoreType.DMA
     vm = pltpu.VMEM
-    copied = [vm(args[k].shape, args[k].dtype) for k in (2, 3, 4, 5, 6, 7, 8, 9, 10, 11, 12, 13,
-                                                         14, 15, 16, 17, 18)]
+    same = [vm(args[k].shape, args[k].dtype) for k in range(19)]
+    copied = same[2:7] + [vm((width, 896), BF16), vm((width, 768), BF16)] + same[11:19]
     piece = vm((2, 128, width // 2), BF16)
     return pl.pallas_call(
         mixer_kernel,
@@ -646,25 +701,25 @@
         scratch_shapes=copied
         + [
             vm((8, width), F32), vm((NZ - 1, 8, 256), F32), vm((8, 256), F32),
-            vm((NY - 1, 8, 256), F32), vm((8, 256), F32), vm((NX - 1, 8, 256), F32),
-            vm((8, 256), F32), vm((8, width), F32),
-            vm((tokens, width), BF16), vm((4 * HALO, width), BF16), vm((tokens, width), BF16),
-            vm((4 * HALO, width), BF16), vm((tokens, 512), BF16), vm((tokens, 256), BF16),
-            vm((tokens, 256), BF16), vm((tokens, 512), F32), vm((tokens, 512), F32),
+            vm((NX * NY, 8, 256), F32), vm((8, 256), F32), vm((8, width), F32),
+            vm((tokens, width), BF16), vm((4 * HALO, width), BF16),
+            vm((tokens + 4 * HALO, width), F32), vm((tokens + 4 * HALO, width), BF16),
+            vm((tokens + 4 * HALO, 896), BF16), vm((tokens, 768), BF16),
+            vm((tokens, 512), BF16), vm((tokens, 256), BF16), vm((tokens, 256), BF16),
+            vm((tokens, 512), F32), vm((tokens, 512), F32),
             vm((tokens, 128), F32), vm((tokens, 128), F32), vm((tokens, 128), F32),
-            vm((128, 1024), BF16), vm((4, STATE, 1024), F32), vm((4, STATE, 1024), BF16),
+            vm((tokens, 128), F32), vm((tokens, 1024), F32),
+            vm((256, 1024), BF16), vm((4, STATE, 1024), F32), vm((4, STATE, 1024), BF16),
             vm((8, 1024), F32), vm((8, 128), F32),
-            vm((STATE, 1024), BF16), vm((STATE, 1024), BF16), vm((1, 1024), F32),
-            vm((1, 1024), F32), vm((NS, 16, 256), BF16), vm((NS, 16, 256), BF16),
-            vm((NS, 1, 256), F32), vm((NS, 1, 256), F32), vm((NS, 16, 256), BF16),
-            vm((STATE, 1024), BF16),
+            vm((STATE, 1024), BF16), vm((STATE, 1024), BF16), vm((2, 1024), F32),
+            vm((NS, 16, 256), BF16), vm((NS, 16, 256), BF16), vm((NS, 2, 256), F32),
+            vm((NS, 16, 256), BF16), vm((STATE, 1024), BF16),
             vm((128, 512), BF16), piece, piece, piece, piece, piece, piece, piece,
             dma((19,)),
         ]
-        + [dma((NZ - 1,))] * 2 + [dma((NY - 1,))] * 2 + [dma((NX - 1,))] * 2
-        + [dma((NZ - 1,))] * 2
+        + [dma((NZ - 1,))] * 2 + [dma((NX * NY,))] * 2 + [dma((NZ - 1,))] * 2
         + [dma((4,))] * 2 + [dma((2,))] * 2 + [dma((2,))] * 2
-        + [dma((NS,))] * 10
+        + [dma((NS,))] * 8
         + [dma((2,)), dma((2,)), dma((4,)), dma((4,))],
         compiler_params=pltpu.CompilerParams(
             collective_id=0, has_side_effects=True, vmem_limit_bytes=60 << 20

time: 79.6 us -> 86.5 us (1.087)
  Pallas kernels: 77.3 us -> 83.8 us
    pallas_call x1, Pallas kernels: 77.3 us -> 83.8 us  [mixer_call(): pl.pallas_call(mixer_kernel, out_shape=jax.ShapeDtypeStruct((128, width),...]
where the time goes in v3:
time: 86.5 us; the launch traced here: 85.7 us
  Pallas kernels  83.8 us (97%)
  local copies, waits for them, and re-layouts  1.88 us (2%)
    pallas_call x1, Pallas kernels, mixer_call(): pl.pallas_call(mixer_kernel, out_shape=jax.ShapeDtypeStruct((128, width),...  83.8 us
    unnamed x1, local copies, waits for them, and re-layouts  1.88 us

profile of v3, /device:TPU:8, one launch (start us, length us, event | category | flops | bytes accessed | tf_op | source)
XLA Modules:
  0.0 85.7 jit_solution(9527574106345618777)
XLA Ops:
  0.0 83.8 %mixer.1 = bf16[128,2048]{1,0:T(8,128)(2,1)} custom-call(bf16[128,2048]{1,0:T(8,128)(2,1)} %bitcast.11, bf16[32,2048]{1,0:T(8,128)(2,1)} %bitcast.13, f32[16,128]{1,0:T(8,128)} %bitcast.15, f32[16,128]{1,0:T(8,128)} %bitcast.16, bf16[16,2048]{1,0:T(8,128)(2,1)} %shift_h.1, bf16[16,2048]{1,0:T(8,128)(2,1)} %scale_h.1, bf16[16,2048]{1,0:T(8,128)(2,1)} %gatem_h.1, ...), custom_call_target="tpu_custom_call" | custom-call | tf_op jit(solution)/shard_map/mixer/pallas_call | solution.py:696
  83.8 1.9 %copy.21 = bf16[1,128,2048]{2,1,0:T(8,128)(2,1)} copy(bf16[1,128,2048]{2,1,0:T(8,128)(2,1)} %bitcast.10) | data formatting | bytes 1048576

commit v4 on v3

--- a/solution.py
+++ b/solution.py
@@ -199,30 +199,25 @@
     norm_at(y * 128, 64)
     pl.semaphore_wait(barrier, NS - 1 + NX * (NY - 1))
 
-    z_copies = []
-    for d in range(1, NZ):
+    nxt, prv = lax.rem(s + 1, NS), lax.rem(s + NS - 1, NS)
+
+    def got_all(ref, recv):
+        remote(ref, ref, recv, recv, **at(nxt)).wait_recv()
+
+    def sent_all(ref, send):
+        remote(ref, ref, send, send, **at(nxt)).wait_send()
+
+    for d in (4, 3, 5, 2, 6, 1, 7):
         to = lax.rem(z + d, NZ)
-        z_copies.append(
-            remote(
-                part.at[:, lanes(to * 256, 256)], zbuf.at[d - 1], z_send.at[d - 1],
-                z_recv.at[d - 1], sp_0=to,
-            )
-        )
-        z_copies[-1].start()
-
-    l_copies = {}
-
-    def latent_half(side, half):
-        piece = gat.at[rows(y * 128 + half * 64, 64)]
-        k = side * 2 + half
-        copy = remote(
+        remote(
+            part.at[:, lanes(to * 256, 256)], zbuf.at[d - 1], z_send.at[0], z_recv.at[0], sp_0=to
+        ).start()
+
+    def latent_piece(side, first_row, count, k):
+        piece = gat.at[rows(y * 128 + first_row, count)]
+        return remote(
             piece, piece, l_send.at[k], l_recv.at[k], tp=right if side == 0 else left
         )
-        copy.start()
-        l_copies[side, half] = copy
-
-    latent_half(0, 0)
-    latent_half(1, 1)
 
     def latent_ahead(side):
         owner = left if side == 0 else right
@@ -231,7 +226,24 @@
             piece, piece, f_send.at[side], f_recv.at[side], tp=right if side == 0 else left
         )
 
-    nxt, prv = lax.rem(s + 1, NS), lax.rem(s + NS - 1, NS)
+    l_first = [latent_piece(0, 0, 64, 0), latent_piece(1, 64, 64, 1)]
+    l_next = [latent_piece(0, 64, 32, 2), latent_piece(1, 0, 32, 3)]
+    l_last = [latent_piece(0, 96, 32, 4), latent_piece(1, 32, 32, 5)]
+    ahead, back = latent_ahead(0), latent_ahead(1)
+
+    def start_all(copies):
+        for copy in copies:
+            copy.start()
+
+    def start_ahead():
+        l_first[0].wait_recv()
+        ahead.start()
+        l_first[1].wait_recv()
+        back.start()
+
+    early = lax.axis_index("dp") == 1
+    late = lax.axis_index("dp") == 0
+    pl.when(early)(lambda: start_all(l_first + l_next))
     halo_next = remote(
         ctx_ext.at[pl.ds(2 * HALO, HALO)], ctx_ext.at[pl.ds(0, HALO)],
         h_send.at[0], h_recv.at[0], **at(nxt),
@@ -267,58 +279,57 @@
         )
 
     total = part[:, lanes(z * 256, 256)]
-    for d, copy in enumerate(z_copies):
-        copy.wait()
-        total = total + zbuf[d]
+    got_all(zbuf, z_recv.at[0])
+    for d in range(1, NZ):
+        total = total + zbuf[d - 1]
     qbuf[...] = total
     def xy_copy(q):
-        return remote(qbuf, xybuf.at[q], xy_send.at[q], xy_recv.at[q], **at_xy(q, 1))
+        return remote(qbuf, xybuf.at[q], xy_send.at[0], xy_recv.at[0], **at_xy(q, 1))
 
     def send_xy(k, none):
         xy_copy(NX * NY - 1 - k).start()
         return none
 
     lax.fori_loop(0, NX * NY - 1, send_xy, 0)
-    latent_half(0, 1)
-    latent_half(1, 0)
-
-    l_copies[0, 0].wait_recv()
-    ahead = latent_ahead(0)
-    ahead.start()
-    l_copies[1, 1].wait_recv()
-    back = latent_ahead(1)
-    back.start()
-    norm_at(left * 128, 64)
-    norm_at(right * 128 + 64, 64)
-
-    def wait_xy(q, none):
-        xy_copy(q).wait()
-        return none
-
-    lax.fori_loop(1, NX * NY, wait_xy, 0)
+
+    @pl.when(early)
+    def _():
+        start_all(l_last)
+        start_ahead()
+        norm_at(left * 128, 64)
+        norm_at(right * 128 + 64, 64)
+
+    pl.when(late)(lambda: start_all(l_first + l_next + l_last))
+
+    got_all(xybuf.at[pl.ds(1, NX * NY - 1)], xy_recv.at[0])
     total = qbuf[...]
     for q in range(1, NX * NY):
         total = total + xybuf[q]
     fbuf[...] = total
-    g_copies = []
     for d in (4, 3, 5, 2, 6, 1, 7):
-        g_copies.append(
-            remote(
-                fbuf, mod.at[:, lanes(z * 256, 256)], g_send.at[d - 1], g_recv.at[d - 1],
-                sp_0=lax.rem(z + d, NZ),
-            )
-        )
-        g_copies[-1].start()
+        remote(
+            fbuf, mod.at[:, lanes(z * 256, 256)], g_send.at[0], g_recv.at[0],
+            sp_0=lax.rem(z + d, NZ),
+        ).start()
     mod[:, lanes(z * 256, 256)] = total
 
     halo_next.wait()
     halo_prev.wait()
     norm_ctx(0)
     norm_ctx(3 * HALO)
-    l_copies[0, 1].wait_recv()
-    l_copies[1, 0].wait_recv()
-    norm_at(left * 128 + 64, 64)
-    norm_at(right * 128, 64)
+    def second_halves():
+        for copy in l_next + l_last:
+            copy.wait_recv()
+        norm_at(left * 128 + 64, 64)
+        norm_at(right * 128, 64)
+
+    pl.when(early)(second_halves)
+
+    @pl.when(late)
+    def _():
+        start_ahead()
+        norm_at(left * 128, 64)
+        norm_at(right * 128 + 64, 64)
 
     for copy in fetch[10:]:
         copy.wait()
@@ -336,42 +347,47 @@
     write_taps = t_write[:, lanes(y * 256, 256)]
     read_taps = t_read[:, lanes(y * 256, 256)]
 
-    for copy in g_copies:
-        copy.wait()
-
-    def modulate(b, none):
+    got_all(zbuf, g_recv.at[0])
+
+    def block_of(k):
+        return lax.rem(y + (lax.rem(k + 1, 3) + 1) * ((k + 3) // 4), NY)
+
+    def modulate(k, none):
+        b = block_of(k)
+
         def chunk(i, none):
             rs = rows(b * 128 + i * 32, 32)
-            hid[rs, :] = (nrm[rs, :] * (1.0 + mod[2:3, :]) + mod[0:1, :]).astype(BF16)
+            hid[rows(64 + k * 128 + i * 32, 32), :] = (
+                nrm[rs, :] * (1.0 + mod[2:3, :]) + mod[0:1, :]
+            ).astype(BF16)
             return none
 
         lax.fori_loop(0, 4, chunk, 0)
         return none
 
-    modulate(y, 0)
-    modulate(left, 0)
-    modulate(right, 0)
+    def project(rs):
+        for c in (slice(0, 256), slice(256, 512), slice(512, 768), slice(768, 896)):
+            pre_a[rs, c] = jnp.dot(
+                hid[rs, :], w_first[:, c], preferred_element_type=F32
+            ).astype(BF16)
+
     for k in range(2):
-        rs = pl.ds(512 + k * 32, 32)
-        hid[rs, :] = (nrm[rs, :] * (1.0 + mod[3:4, :]) + mod[1:2, :]).astype(BF16)
-    ahead.wait_recv()
-    back.wait_recv()
-    norm_at(opposite * 128, 128)
-    modulate(opposite, 0)
-
-    for c in (slice(0, 256), slice(256, 512), slice(512, 768), slice(768, 896)):
-        pre_a[:, c] = jnp.dot(hid[...], w_first[:, c], preferred_element_type=F32).astype(BF16)
+        hid[pl.ds(k * 32, 32), :] = (
+            nrm[pl.ds(512 + k * 32, 32), :] * (1.0 + mod[3:4, :]) + mod[1:2, :]
+        ).astype(BF16)
+    modulate(0, 0)
+    project(slice(0, 192))
 
     line_c = lax.broadcasted_iota(jnp.int32, (4 * HALO, 1), 0)
     first = jnp.where(s == 0, HALO, 0)
     last = jnp.where(s == NS - 1, 3 * HALO, 4 * HALO)
     present = (line_c >= first) & (line_c < last)
     own_c = slice(HALO, 3 * HALO)
-    cv = pre_a[512:576, 0:512].astype(F32)
-    cw = pre_a[512:576, 512:768].astype(F32)
+    cv = pre_a[0:64, 0:512].astype(F32)
+    cw = pre_a[0:64, 512:768].astype(F32)
     cv = conv_rows(jnp.where(present, cv, 0.0), value_taps, 4 * HALO)[own_c].astype(BF16)
     cw = conv_rows(jnp.where(present, cw, 0.0), write_taps, 4 * HALO)[own_c].astype(BF16)
-    cstep = softplus(pre_a[512 + HALO : 512 + 3 * HALO, 768:896].astype(F32))
+    cstep = softplus(pre_a[HALO : 3 * HALO, 768:896].astype(F32))
     cdecay = -rate_row * cstep
     r32 = lax.broadcasted_iota(jnp.int32, (2 * HALO, 2 * HALO), 0)
     c32 = lax.broadcasted_iota(jnp.int32, (2 * HALO, 2 * HALO), 1)
@@ -402,40 +418,41 @@
 
     ctotal = jnp.exp(jnp.sum(cdecay, axis=0, keepdims=True))
 
-    def far_first(k):
-        return NS // 2 + ((k + 1) // 2) * (1 - 2 * lax.rem(k, 2))
+    xts = [x] + [lax.rem(x + dx, NX) for dx in range(1, NX)]
+
+    def each_other(start):
+        def line(k, none):
+            zt = lax.rem(z + NZ // 2 + ((k + 1) // 2) * (1 - 2 * lax.rem(k, 2)), NZ)
+            for xt in (xts[2], xts[1], xts[3], xts[0]):
+                start(zt, xt)
+            return none
+
+        lax.fori_loop(0, NZ - 1, line, 0)
+        for xt in (xts[2], xts[1], xts[3]):
+            start(z, xt)
 
     def state_copies(states, got, a_send, a_recv):
-        def outgoing(p):
-            t = lax.rem(s + p, NS)
+        def outgoing(zt, xt):
             return remote(
-                states.at[rows((t // NX) * 16, 16), lanes(lax.rem(t, NX) * 256, 256)],
-                got.at[s], a_send.at[t], a_recv.at[s], **at(t),
+                states.at[rows(zt * 16, 16), lanes(xt * 256, 256)],
+                got.at[s], a_send.at[0], a_recv.at[0], sp_0=zt, sp_1=xt,
             )
 
-        def take(p, none):
-            f = lax.rem(s + NS - p, NS)
-            remote(got.at[f], got.at[f], a_send.at[f], a_recv.at[f], **at(f)).wait_recv()
-            return none
-
-        return outgoing, take
-
-    out_c, take_c = state_copies(ends_c, got_c, c_send, c_recv)
-
-    def send_c(k, none):
-        out_c(far_first(k)).start()
-        return none
-
-    lax.fori_loop(0, NS - 1, send_c, 0)
+        return outgoing
+
+    out_c = state_copies(ends_c, got_c, c_send, c_recv)
+    each_other(lambda zt, xt: out_c(zt, xt).start())
     got_c[s] = ends_c[rows(z * 16, 16), lanes(x * 256, 256)]
 
-    def block_states(b, none):
+    def block_states(k, none):
+        b = block_of(k)
         at_b = rows(b * 128, 128)
-        vb = conv_rows(pre_a[at_b, 0:512].astype(F32), value_taps, ROW).astype(BF16)
+        at_k = rows(64 + k * 128, 128)
+        vb = conv_rows(pre_a[at_k, 0:512].astype(F32), value_taps, ROW).astype(BF16)
         val[at_b, :] = vb
-        w = conv_rows(pre_a[at_b, 512:768].astype(F32), write_taps, ROW).astype(BF16)
+        w = conv_rows(pre_a[at_k, 512:768].astype(F32), write_taps, ROW).astype(BF16)
         wri[at_b, :] = w
-        step = softplus(pre_a[at_b, 768:896].astype(F32)) * pcol[at_b, :]
+        step = softplus(pre_a[at_k, 768:896].astype(F32)) * pcol[at_b, :]
         decay = -rate_row * step
         parts = jnp.concatenate(three_parts(decay), axis=1)
         down = jnp.dot(lower, parts, preferred_element_type=F32)
@@ -456,7 +473,17 @@
         tot[pl.ds(b, 1), :] = total
         return none
 
-    lax.fori_loop(0, 4, block_states, 0)
+    block_states(0, 0)
+
+    pl.when(late)(second_halves)
+    modulate(1, 0)
+    modulate(2, 0)
+    ahead.wait_recv()
+    back.wait_recv()
+    norm_at(opposite * 128, 128)
+    modulate(3, 0)
+    project(slice(192, 576))
+    lax.fori_loop(1, 4, block_states, 0)
 
     t0, t1, t2, t3 = (tot[b : b + 1, :] for b in range(4))
     zero = jnp.zeros_like(t0)
@@ -479,32 +506,32 @@
                 before[b, :, ls] = state.astype(BF16)
                 state = etot[b : b + 1, ls] * state + inc[b, :, ls]
             ends_s[:, ls] = state.astype(BF16)
-    out_s, take_s = state_copies(ends_s, got_s, s_send, s_recv)
-
-    def out_t(p):
-        t = lax.rem(s + p, NS)
+    out_s = state_copies(ends_s, got_s, s_send, s_recv)
+
+    def out_t(zt, xt):
         return remote(
-            tot_b.at[:, lanes(lax.rem(t, NX) * 256, 256)], gtot.at[s],
-            t_send.at[t], t_recv.at[s], **at(t),
-        )
-
-    def send_s(k, none):
-        out_s(far_first(k)).start()
-        out_t(far_first(k)).start()
-        return none
-
-    lax.fori_loop(0, NS - 1, send_s, 0)
+            tot_b.at[:, lanes(xt * 256, 256)], gtot.at[s],
+            t_send.at[0], t_recv.at[0], sp_0=zt, sp_1=xt,
+        )
+
+    def send_s(zt, xt):
+        out_s(zt, xt).start()
+        out_t(zt, xt).start()
+
+    each_other(send_s)
     got_s[s] = ends_s[rows(z * 16, 16), lanes(x * 256, 256)]
     gtot[s] = tot_b[:, lanes(x * 256, 256)]
 
     for c in (slice(0, 256), slice(256, 512), slice(512, 768)):
         pre_b[:, c] = jnp.dot(
-            hid[0:512, :], w_second[:, c], preferred_element_type=F32
+            hid[64:576, :], w_second[:, c], preferred_element_type=F32
         ).astype(BF16)
 
-    def within(b, none):
+    def within(k, none):
+        b = block_of(k)
         at_b = rows(b * 128, 128)
-        rb = conv_rows(pre_b[at_b, 0:256].astype(F32), read_taps, ROW).astype(BF16)
+        at_k = rows(k * 128, 128)
+        rb = conv_rows(pre_b[at_k, 0:256].astype(F32), read_taps, ROW).astype(BF16)
         reads[at_b, :] = rb
         cums = cum[at_b, :]
         step = stp[at_b, :]
@@ -550,25 +577,20 @@
     def order_of(k):
         return k + turned * (NS - 1 - 2 * k)
 
-    def take_t(p, none):
-        f = lax.rem(s + NS - p, NS)
-        remote(gtot.at[f], gtot.at[f], t_send.at[f], t_recv.at[f], **at(f)).wait_recv()
-        return none
-
-    lax.fori_loop(1, NS, take_c, 0)
-    lax.fori_loop(1, NS, take_t, 0)
+    got_all(got_c.at[pl.ds(0, NS - 1)], c_recv.at[0])
+    got_all(gtot.at[pl.ds(0, NS - 1)], t_recv.at[0])
 
     def context_scan(k, state):
         j = order_of(k)
         return gtot[j, 1:2, :] * state + got_c[j].astype(F32)
 
     state = lax.fori_loop(0, NS, context_scan, jnp.zeros((16, 256), F32))
-    lax.fori_loop(1, NS, take_s, 0)
+    got_all(got_s.at[pl.ds(0, NS - 1)], s_recv.at[0])
 
     def back_copy(j):
         return remote(
             sent.at[j], start.at[rows(z * 16, 16), lanes(x * 256, 256)],
-            b_send.at[j], b_recv.at[s], **at(j),
+            b_send.at[0], b_recv.at[0], **at(j),
         )
 
     def latent_scan(k, state):
@@ -584,21 +606,15 @@
     lax.fori_loop(0, NS, latent_scan, state)
     start[rows(z * 16, 16), lanes(x * 256, 256)] = sent[s]
 
-    def last_tables(b, none):
-        at_b = rows(b * 128, 128)
+    def last_tables(k, none):
+        at_b = rows(block_of(k) * 128, 128)
         grown_c[at_b, :] = expand(cdec[at_b, :], spread[...])
-        gates[at_b, :] = silu(pre_b[at_b, 256:768].astype(F32))
+        gates[at_b, :] = silu(pre_b[rows(k * 128, 128), 256:768].astype(F32))
         return none
 
     lax.fori_loop(0, 4, last_tables, 0)
 
-    def take_start(p, none):
-        f = lax.rem(s + NS - p, NS)
-        piece = start.at[rows((f // NX) * 16, 16), lanes(lax.rem(f, NX) * 256, 256)]
-        remote(piece, piece, b_send.at[f], b_recv.at[f], **at(f)).wait_recv()
-        return none
-
-    lax.fori_loop(1, NS, take_start, 0)
+    got_all(got_s.at[pl.ds(0, NS - 1)], b_recv.at[0])
 
     half = w_out.shape[1] // 2
 
@@ -654,15 +670,13 @@
     mine[0] = product(0)
     mine[1] = product(1)
 
-    def send_done(p, none):
-        back_copy(lax.rem(s + p, NS)).wait_send()
-        out_s(p).wait_send()
-        out_t(p).wait_send()
-        out_c(p).wait_send()
-        return none
-
-    lax.fori_loop(1, NS, send_done, 0)
-    for copy in l_copies.values():
+    sent_all(zbuf, z_send.at[0])
+    sent_all(xybuf.at[pl.ds(1, NX * NY - 1)], xy_send.at[0])
+    sent_all(zbuf, g_send.at[0])
+    sent_all(gtot.at[pl.ds(0, NS - 1)], t_send.at[0])
+    for sem in (c_send, s_send, b_send):
+        sent_all(got_s.at[pl.ds(0, NS - 1)], sem.at[0])
+    for copy in l_first + l_next + l_last:
         copy.wait_send()
     ahead.wait_send()
     back.wait_send()
@@ -717,9 +731,9 @@
             vm((128, 512), BF16), piece, piece, piece, piece, piece, piece, piece,
             dma((19,)),
         ]
-        + [dma((NZ - 1,))] * 2 + [dma((NX * NY,))] * 2 + [dma((NZ - 1,))] * 2
-        + [dma((4,))] * 2 + [dma((2,))] * 2 + [dma((2,))] * 2
-        + [dma((NS,))] * 8
+        + [dma((1,))] * 6
+        + [dma((6,))] * 2 + [dma((2,))] * 2 + [dma((2,))] * 2
+        + [dma((1,))] * 8
         + [dma((2,)), dma((2,)), dma((4,)), dma((4,))],
         compiler_params=pltpu.CompilerParams(
             collective_id=0, has_side_effects=True, vmem_limit_bytes=60 << 20

time: 86.5 us -> 71.6 us (0.83)
  Pallas kernels: 83.8 us -> 69.6 us
    pallas_call x1, Pallas kernels: 83.8 us -> 69.6 us  [mixer_call(): pl.pallas_call(mixer_kernel, out_shape=jax.ShapeDtypeStruct((128, width),...]
where the time goes in v4:
time: 71.6 us; the launch traced here: 71.5 us
  Pallas kernels  69.6 us (97%)
  local copies, waits for them, and re-layouts  1.88 us (3%)
    pallas_call x1, Pallas kernels, mixer_call(): pl.pallas_call(mixer_kernel, out_shape=jax.ShapeDtypeStruct((128, width),...  69.6 us
    unnamed x1, local copies, waits for them, and re-layouts  1.88 us

profile of v4, /device:TPU:8, one launch (start us, length us, event | category | flops | bytes accessed | tf_op | source)
XLA Modules:
  0.0 71.5 jit_solution(13107403785258752477)
XLA Ops:
  0.0 69.6 %mixer.1 = bf16[128,2048]{1,0:T(8,128)(2,1)} custom-call(bf16[128,2048]{1,0:T(8,128)(2,1)} %bitcast.11, bf16[32,2048]{1,0:T(8,128)(2,1)} %bitcast.13, f32[16,128]{1,0:T(8,128)} %bitcast.15, f32[16,128]{1,0:T(8,128)} %bitcast.16, bf16[16,2048]{1,0:T(8,128)(2,1)} %shift_h.1, bf16[16,2048]{1,0:T(8,128)(2,1)} %scale_h.1, bf16[16,2048]{1,0:T(8,128)(2,1)} %gatem_h.1, ...), custom_call_target="tpu_custom_call" | custom-call | tf_op jit(solution)/shard_map/mixer/pallas_call | solution.py:710
  69.6 1.9 %copy.21 = bf16[1,128,2048]{2,1,0:T(8,128)(2,1)} copy(bf16[1,128,2048]{2,1,0:T(8,128)(2,1)} %bitcast.10) | data formatting | bytes 1048576

commit v5 on v4

--- a/solution.py
+++ b/solution.py
@@ -106,7 +106,7 @@
     part, zbuf, qbuf, xybuf, fbuf, mod,
     gat, ctx_ext, nrm, hid, pre_a, pre_b, val, wri, reads, gates, local,
     cum, stp, cdec, pcol, grown_c, spread, inc, before, etot, tot,
-    ends_s, ends_c, tot_b, got_s, got_c, gtot, sent, start,
+    ends_s, ends_c, tot_b, got_s, got_c, gtot, grow_s, grow_c, sent, start,
     inner, far, near_r, near_l, mine, got_far, got_r, got_l,
     in_sem, z_send, z_recv, xy_send, xy_recv, g_send, g_recv,
     l_send, l_recv, f_send, f_recv, h_send, h_recv,
@@ -140,27 +140,34 @@
         (gain_h, gain), (wo_h, w_out),
     ]
     fetch = [pltpu.make_async_copy(a, b, in_sem.at[k]) for k, (a, b) in enumerate(pairs)]
-    for copy in fetch:
+    for copy in fetch[:7]:
         copy.start()
 
+    xts = [x] + [lax.rem(x + dx, NX) for dx in range(1, NX)]
+
+    def each_other(start):
+        def line(k, none):
+            zt = lax.rem(z + NZ // 2 + ((k + 1) // 2) * (1 - 2 * lax.rem(k, 2)), NZ)
+            for xt in (xts[2], xts[1], xts[3], xts[0]):
+                start(zt, xt)
+            return none
+
+        lax.fori_loop(0, NZ - 1, line, 0)
+        for xt in (xts[2], xts[1], xts[3]):
+            start(z, xt)
+
     barrier = pltpu.get_barrier_semaphore()
-
-    def greet(p, none):
-        pl.semaphore_signal(
-            barrier, inc=1, device_id=at(lax.rem(s + p, NS)), device_id_type=MESH
-        )
-        return none
-
-    lax.fori_loop(1, NS, greet, 0)
-
-    def greet_xy(q, none):
-        @pl.when(lax.rem(q, NY) != 0)
-        def _():
-            pl.semaphore_signal(barrier, inc=1, device_id=at_xy(q, 1), device_id_type=MESH)
-
-        return none
-
-    lax.fori_loop(1, NX * NY, greet_xy, 0)
+    each_other(
+        lambda zt, xt: pl.semaphore_signal(
+            barrier, inc=1, device_id={"sp_0": zt, "sp_1": xt}, device_id_type=MESH
+        )
+    )
+    for dy in (2, 1, 3):
+        for xt in xts:
+            pl.semaphore_signal(
+                barrier, inc=1, device_id={"sp_1": xt, "tp": lax.rem(y + dy, NY)},
+                device_id_type=MESH,
+            )
 
     for copy in fetch[:5]:
         copy.wait()
@@ -182,21 +189,14 @@
     part[0:2, :] = product_of(shift_m)[0:2]
     part[2:4, :] = product_of(scale_m)[0:2]
     part[4:8, :] = product_of(gate_m)[0:4]
-    fetch[5].wait()
-    fetch[6].wait()
-
     def norm_at(base, count):
-        def chunk(i, none):
-            rs = rows(base + i * 32, 32)
+        for k in range(count // 64):
+            rs = rows(base + k * 64, 64)
             nrm[rs, :] = normed_rows(gat[rs, :])
-            return none
-
-        lax.fori_loop(0, count // 32, chunk, 0)
 
     def norm_ctx(base):
         nrm[pl.ds(512 + base, HALO), :] = normed_rows(ctx_ext[pl.ds(base, HALO), :])
 
-    norm_at(y * 128, 64)
     pl.semaphore_wait(barrier, NS - 1 + NX * (NY - 1))
 
     nxt, prv = lax.rem(s + 1, NS), lax.rem(s + NS - 1, NS)
@@ -243,6 +243,8 @@
 
     early = lax.axis_index("dp") == 1
     late = lax.axis_index("dp") == 0
+    fetch[5].wait()
+    fetch[6].wait()
     pl.when(early)(lambda: start_all(l_first + l_next))
     halo_next = remote(
         ctx_ext.at[pl.ds(2 * HALO, HALO)], ctx_ext.at[pl.ds(0, HALO)],
@@ -255,7 +257,9 @@
     halo_next.start()
     halo_prev.start()
 
-    norm_at(y * 128 + 64, 64)
+    for copy in fetch[7:]:
+        copy.start()
+    norm_at(y * 128, 128)
     norm_ctx(HALO)
     norm_ctx(2 * HALO)
     spread_matrix(spread)
@@ -355,14 +359,11 @@
     def modulate(k, none):
         b = block_of(k)
 
-        def chunk(i, none):
-            rs = rows(b * 128 + i * 32, 32)
-            hid[rows(64 + k * 128 + i * 32, 32), :] = (
+        for i in range(2):
+            rs = rows(b * 128 + i * 64, 64)
+            hid[rows(64 + k * 128 + i * 64, 64), :] = (
                 nrm[rs, :] * (1.0 + mod[2:3, :]) + mod[0:1, :]
             ).astype(BF16)
-            return none
-
-        lax.fori_loop(0, 4, chunk, 0)
         return none
 
     def project(rs):
@@ -417,19 +418,6 @@
         )
 
     ctotal = jnp.exp(jnp.sum(cdecay, axis=0, keepdims=True))
-
-    xts = [x] + [lax.rem(x + dx, NX) for dx in range(1, NX)]
-
-    def each_other(start):
-        def line(k, none):
-            zt = lax.rem(z + NZ // 2 + ((k + 1) // 2) * (1 - 2 * lax.rem(k, 2)), NZ)
-            for xt in (xts[2], xts[1], xts[3], xts[0]):
-                start(zt, xt)
-            return none
-
-        lax.fori_loop(0, NZ - 1, line, 0)
-        for xt in (xts[2], xts[1], xts[3]):
-            start(z, xt)
 
     def state_copies(states, got, a_send, a_recv):
         def outgoing(zt, xt):
@@ -466,10 +454,14 @@
         vf = vb.astype(F32)
         scaled = (jnp.concatenate([vf, vf], axis=1) * expand(weight, spread[...])).astype(BF16)
         for g in range(2):
-            wg = w[:, g * 128 : (g + 1) * 128]
-            for d in range(2):
-                ls = slice((d * 2 + g) * 256, (d * 2 + g + 1) * 256)
-                inc[b, :, ls] = dot_on(wg, scaled[:, ls], 0, 0)
+            fs = slice(g * 256, (g + 1) * 256)
+            bs = slice(512 + g * 256, 512 + (g + 1) * 256)
+            states = dot_on(
+                w[:, g * 128 : (g + 1) * 128],
+                jnp.concatenate([scaled[:, fs], scaled[:, bs]], axis=1), 0, 0,
+            )
+            inc[b, :, fs] = states[:, 0:256]
+            inc[b, :, bs] = states[:, 256:512]
         tot[pl.ds(b, 1), :] = total
         return none
 
@@ -490,10 +482,14 @@
     etot[...] = expand3(
         jnp.concatenate(
             [jnp.exp(t0), jnp.exp(t1), jnp.exp(t2), jnp.exp(t3), jnp.exp(t0 + t1 + t2 + t3),
-             ctotal, zero, zero], axis=0,
-        )
-    )
-    tot_b[...] = etot[4:6, :]
+             zero, zero, zero], axis=0,
+        )
+    )
+    lane1 = lane[0:1]
+    tot_b[...] = jnp.where(
+        lane1 < 2 * heads, jnp.exp(t0 + t1 + t2 + t3),
+        jnp.where(lane1 < 4 * heads, pltpu.roll(ctotal, 2 * heads, 1), 0.0),
+    )
     tot[0:1, :] = jnp.where(fl, zero, t1 + t2 + t3)
     tot[1:2, :] = jnp.where(fl, t0, t2 + t3)
     tot[2:3, :] = jnp.where(fl, t0 + t1, t3)
@@ -509,18 +505,15 @@
     out_s = state_copies(ends_s, got_s, s_send, s_recv)
 
     def out_t(zt, xt):
-        return remote(
-            tot_b.at[:, lanes(xt * 256, 256)], gtot.at[s],
-            t_send.at[0], t_recv.at[0], sp_0=zt, sp_1=xt,
-        )
+        return remote(tot_b, gtot.at[s], t_send.at[0], t_recv.at[0], sp_0=zt, sp_1=xt)
 
     def send_s(zt, xt):
+        out_t(zt, xt).start()
         out_s(zt, xt).start()
-        out_t(zt, xt).start()
 
     each_other(send_s)
     got_s[s] = ends_s[rows(z * 16, 16), lanes(x * 256, 256)]
-    gtot[s] = tot_b[:, lanes(x * 256, 256)]
+    gtot[s] = tot_b[...]
 
     for c in (slice(0, 256), slice(256, 512), slice(512, 768)):
         pre_b[:, c] = jnp.dot(
@@ -577,12 +570,23 @@
     def order_of(k):
         return k + turned * (NS - 1 - 2 * k)
 
+    got_all(gtot.at[pl.ds(0, NS - 1)], t_recv.at[0])
+
+    def spread_own(v):
+        high, mid, low = three_parts(v)
+        own = lanes(x * 256, 256)
+        return jnp.dot(high, spread[0:128, own], preferred_element_type=F32) + jnp.dot(
+            jnp.concatenate([mid, low], axis=1), spread[:, own], preferred_element_type=F32
+        )
+
+    ranges = gtot[...].reshape(NS, 128)
+    grow_s[...] = spread_own(ranges)
+    grow_c[...] = spread_own(pltpu.roll(ranges, 128 - 2 * heads, 1))
     got_all(got_c.at[pl.ds(0, NS - 1)], c_recv.at[0])
-    got_all(gtot.at[pl.ds(0, NS - 1)], t_recv.at[0])
 
     def context_scan(k, state):
         j = order_of(k)
-        return gtot[j, 1:2, :] * state + got_c[j].astype(F32)
+        return grow_c[pl.ds(j, 1), :] * state + got_c[j].astype(F32)
 
     state = lax.fori_loop(0, NS, context_scan, jnp.zeros((16, 256), F32))
     got_all(got_s.at[pl.ds(0, NS - 1)], s_recv.at[0])
@@ -601,7 +605,7 @@
         def _():
             back_copy(j).start()
 
-        return gtot[j, 0:1, :] * state + got_s[j].astype(F32)
+        return grow_s[pl.ds(j, 1), :] * state + got_s[j].astype(F32)
 
     lax.fori_loop(0, NS, latent_scan, state)
     start[rows(z * 16, 16), lanes(x * 256, 256)] = sent[s]
@@ -709,7 +713,7 @@
     piece = vm((2, 128, width // 2), BF16)
     return pl.pallas_call(
         mixer_kernel,
-        out_shape=jax.ShapeDtypeStruct((128, width), BF16),
+        out_shape=pltpu.VMEM((128, width), BF16),
         in_specs=[ANY] * 19,
         out_specs=VMEM,
         scratch_shapes=copied
@@ -725,8 +729,9 @@
             vm((tokens, 128), F32), vm((tokens, 1024), F32),
             vm((256, 1024), BF16), vm((4, STATE, 1024), F32), vm((4, STATE, 1024), BF16),
             vm((8, 1024), F32), vm((8, 128), F32),
-            vm((STATE, 1024), BF16), vm((STATE, 1024), BF16), vm((2, 1024), F32),
-            vm((NS, 16, 256), BF16), vm((NS, 16, 256), BF16), vm((NS, 2, 256), F32),
+            vm((STATE, 1024), BF16), vm((STATE, 1024), BF16), vm((1, 128), F32),
+            vm((NS, 16, 256), BF16), vm((NS, 16, 256), BF16), vm((NS, 1, 128), F32),
+            vm((NS, 256), F32), vm((NS, 256), F32),
             vm((NS, 16, 256), BF16), vm((STATE, 1024), BF16),
             vm((128, 512), BF16), piece, piece, piece, piece, piece, piece, piece,
             dma((19,)),
@@ -736,7 +741,7 @@
         + [dma((1,))] * 8
         + [dma((2,)), dma((2,)), dma((4,)), dma((4,))],
         compiler_params=pltpu.CompilerParams(
-            collective_id=0, has_side_effects=True, vmem_limit_bytes=60 << 20
+            collective_id=0, has_side_effects=True, vmem_limit_bytes=56 << 20
         ),
         name="mixer",
     )(*args)

time: 71.6 us -> 68 us (0.950)
  Pallas kernels: 69.6 us -> 67.1 us
  local copies, waits for them, and re-layouts: 1.88 us -> 0.8 us
    pallas_call x1, Pallas kernels: 69.6 us -> 67.1 us  [mixer_call(): pl.pallas_call(mixer_kernel, out_shape=pltpu.VMEM((128, width), BF16), in...]
    unnamed x1, local copies, waits for them, and re-layouts: 1.88 us -> 0.8 us
where the time goes in v5:
time: 68 us; the launch traced here: 67.9 us
  Pallas kernels  67.1 us (99%)
  local copies, waits for them, and re-layouts  0.8 us (1%)
    pallas_call x1, Pallas kernels, mixer_call(): pl.pallas_call(mixer_kernel, out_shape=pltpu.VMEM((128, width), BF16), in...  67.1 us

profile of v5, /device:TPU:8, one launch (start us, length us, event | category | flops | bytes accessed | tf_op | source)
XLA Modules:
  0.0 67.9 jit_solution(317562359463621793)
XLA Ops:
  0.0 67.1 %mixer.1 = bf16[128,2048]{1,0:T(8,128)(2,1)S(1)} custom-call(bf16[128,2048]{1,0:T(8,128)(2,1)} %bitcast.11, bf16[32,2048]{1,0:T(8,128)(2,1)} %bitcast.13, f32[16,128]{1,0:T(8,128)} %bitcast.15, f32[16,128]{1,0:T(8,128)} %bitcast.16, bf16[16,2048]{1,0:T(8,128)(2,1)} %shift_h.1, bf16[16,2048]{1,0:T(8,128)(2,1)} %scale_h.1, bf16[16,2048]{1,0:T(8,128)(2,1)} %gatem_h.1, ...), custom_call_target="tpu_custom_call" | custom-call | tf_op jit(solution)/shard_map/mixer/pallas_call | solution.py:714
  67.1 0.8 %copy.21 = bf16[1,128,2048]{2,1,0:T(8,128)(2,1)} copy(bf16[1,128,2048]{2,1,0:T(8,128)(2,1)S(1)} %bitcast.10) | data formatting | bytes 1048576

commit v6 on v5

--- a/solution.py
+++ b/solution.py
@@ -104,11 +104,13 @@
     cond, ccond, shift_m, scale_m, gate_m,
     w_first, w_second, w_step, rates, pace, t_value, t_write, t_read, gain, w_out,
     part, zbuf, qbuf, xybuf, fbuf, mod,
+    gpart, gz, gq, gxy, gf, gmod,
     gat, ctx_ext, nrm, hid, pre_a, pre_b, val, wri, reads, gates, local,
     cum, stp, cdec, pcol, grown_c, spread, inc, before, etot, tot,
     ends_s, ends_c, tot_b, got_s, got_c, gtot, grow_s, grow_c, sent, start,
     inner, far, near_r, near_l, mine, got_far, got_r, got_l,
     in_sem, z_send, z_recv, xy_send, xy_recv, g_send, g_recv,
+    gz_send, gz_recv, gxy_send, gxy_recv, gg_send, gg_recv,
     l_send, l_recv, f_send, f_recv, h_send, h_recv,
     s_send, s_recv, t_send, t_recv, c_send, c_recv, b_send, b_recv,
     s1, r1, s2, r2,
@@ -188,7 +190,7 @@
 
     part[0:2, :] = product_of(shift_m)[0:2]
     part[2:4, :] = product_of(scale_m)[0:2]
-    part[4:8, :] = product_of(gate_m)[0:4]
+    gpart[...] = product_of(gate_m)[0:1]
     def norm_at(base, count):
         for k in range(count // 64):
             rs = rows(base + k * 64, 64)
@@ -207,11 +209,44 @@
     def sent_all(ref, send):
         remote(ref, ref, send, send, **at(nxt)).wait_send()
 
-    for d in (4, 3, 5, 2, 6, 1, 7):
-        to = lax.rem(z + d, NZ)
-        remote(
-            part.at[:, lanes(to * 256, 256)], zbuf.at[d - 1], z_send.at[0], z_recv.at[0], sp_0=to
-        ).start()
+    def scatter_z(whole, buf, send, recv):
+        for d in (4, 3, 5, 2, 6, 1, 7):
+            to = lax.rem(z + d, NZ)
+            remote(
+                whole.at[:, lanes(to * 256, 256)], buf.at[d - 1], send.at[0], recv.at[0], sp_0=to
+            ).start()
+
+    def sum_z(whole, buf, recv, piece):
+        got_all(buf, recv.at[0])
+        total = whole[:, lanes(z * 256, 256)]
+        for d in range(1, NZ):
+            total = total + buf[d - 1]
+        piece[...] = total
+
+    def send_xy(piece, buf, send, recv):
+        def one(k, none):
+            q = NX * NY - 1 - k
+            remote(piece, buf.at[q], send.at[0], recv.at[0], **at_xy(q, 1)).start()
+            return none
+
+        lax.fori_loop(0, NX * NY - 1, one, 0)
+
+    def sum_xy(piece, buf, recv, last):
+        got_all(buf.at[pl.ds(1, NX * NY - 1)], recv.at[0])
+        total = piece[...]
+        for q in range(1, NX * NY):
+            total = total + buf[q]
+        last[...] = total
+
+    def gather_z(last, whole, send, recv):
+        for d in (4, 3, 5, 2, 6, 1, 7):
+            remote(
+                last, whole.at[:, lanes(z * 256, 256)], send.at[0], recv.at[0],
+                sp_0=lax.rem(z + d, NZ),
+            ).start()
+        whole[:, lanes(z * 256, 256)] = last[...]
+
+    scatter_z(part, zbuf, z_send, z_recv)
 
     def latent_piece(side, first_row, count, k):
         piece = gat.at[rows(y * 128 + first_row, count)]
@@ -257,6 +292,7 @@
     halo_next.start()
     halo_prev.start()
 
+    scatter_z(gpart, gz, gz_send, gz_recv)
     for copy in fetch[7:]:
         copy.start()
     norm_at(y * 128, 128)
@@ -282,19 +318,8 @@
             jnp.broadcast_to(pace_row, (128, 128))
         )
 
-    total = part[:, lanes(z * 256, 256)]
-    got_all(zbuf, z_recv.at[0])
-    for d in range(1, NZ):
-        total = total + zbuf[d - 1]
-    qbuf[...] = total
-    def xy_copy(q):
-        return remote(qbuf, xybuf.at[q], xy_send.at[0], xy_recv.at[0], **at_xy(q, 1))
-
-    def send_xy(k, none):
-        xy_copy(NX * NY - 1 - k).start()
-        return none
-
-    lax.fori_loop(0, NX * NY - 1, send_xy, 0)
+    sum_z(part, zbuf, z_recv, qbuf)
+    send_xy(qbuf, xybuf, xy_send, xy_recv)
 
     @pl.when(early)
     def _():
@@ -305,17 +330,8 @@
 
     pl.when(late)(lambda: start_all(l_first + l_next + l_last))
 
-    got_all(xybuf.at[pl.ds(1, NX * NY - 1)], xy_recv.at[0])
-    total = qbuf[...]
-    for q in range(1, NX * NY):
-        total = total + xybuf[q]
-    fbuf[...] = total
-    for d in (4, 3, 5, 2, 6, 1, 7):
-        remote(
-            fbuf, mod.at[:, lanes(z * 256, 256)], g_send.at[0], g_recv.at[0],
-            sp_0=lax.rem(z + d, NZ),
-        ).start()
-    mod[:, lanes(z * 256, 256)] = total
+    sum_xy(qbuf, xybuf, xy_recv, fbuf)
+    gather_z(fbuf, mod, g_send, g_recv)
 
     halo_next.wait()
     halo_prev.wait()
@@ -366,10 +382,11 @@
             ).astype(BF16)
         return none
 
-    def project(rs):
-        for c in (slice(0, 256), slice(256, 512), slice(512, 768), slice(768, 896)):
-            pre_a[rs, c] = jnp.dot(
-                hid[rs, :], w_first[:, c], preferred_element_type=F32
+    def project(lo, count):
+        for c in range(4):
+            cs = slice(c * 256, min(c * 256 + 256, 896))
+            pre_a[lo : lo + count, cs] = jnp.dot(
+                hid[lo : lo + count, :], w_first[:, cs], preferred_element_type=F32
             ).astype(BF16)
 
     for k in range(2):
@@ -377,7 +394,7 @@
             nrm[pl.ds(512 + k * 32, 32), :] * (1.0 + mod[3:4, :]) + mod[1:2, :]
         ).astype(BF16)
     modulate(0, 0)
-    project(slice(0, 192))
+    project(0, 192)
 
     line_c = lax.broadcasted_iota(jnp.int32, (4 * HALO, 1), 0)
     first = jnp.where(s == 0, HALO, 0)
@@ -434,13 +451,13 @@
 
     def block_states(k, none):
         b = block_of(k)
-        at_b = rows(b * 128, 128)
-        at_k = rows(64 + k * 128, 128)
-        vb = conv_rows(pre_a[at_k, 0:512].astype(F32), value_taps, ROW).astype(BF16)
-        val[at_b, :] = vb
-        w = conv_rows(pre_a[at_k, 512:768].astype(F32), write_taps, ROW).astype(BF16)
-        wri[at_b, :] = w
-        step = softplus(pre_a[at_k, 768:896].astype(F32)) * pcol[at_b, :]
+        at_k = rows(k * 128, 128)
+        at_a = rows(64 + k * 128, 128)
+        vb = conv_rows(pre_a[at_a, 0:512].astype(F32), value_taps, ROW).astype(BF16)
+        val[at_k, :] = vb
+        w = conv_rows(pre_a[at_a, 512:768].astype(F32), write_taps, ROW).astype(BF16)
+        wri[at_k, :] = w
+        step = softplus(pre_a[at_a, 768:896].astype(F32)) * pcol[rows(b * 128, 128), :]
         decay = -rate_row * step
         parts = jnp.concatenate(three_parts(decay), axis=1)
         down = jnp.dot(lower, parts, preferred_element_type=F32)
@@ -448,8 +465,8 @@
         both = jnp.where(jnp.concatenate([forward_lane] * 3, axis=1), down, up)
         cums = both[:, 0:128] + both[:, 128:256] + both[:, 256:384]
         total = jnp.where(fl, cums[127:128], cums[0:1])
-        cum[at_b, :] = cums
-        stp[at_b, :] = step
+        cum[at_k, :] = cums
+        stp[at_k, :] = step
         weight = jnp.exp(total - cums) * step
         vf = vb.astype(F32)
         scaled = (jnp.concatenate([vf, vf], axis=1) * expand(weight, spread[...])).astype(BF16)
@@ -470,12 +487,15 @@
     pl.when(late)(second_halves)
     modulate(1, 0)
     modulate(2, 0)
+    pl.when(late)(lambda: project(192, 256))
     ahead.wait_recv()
     back.wait_recv()
     norm_at(opposite * 128, 128)
     modulate(3, 0)
-    project(slice(192, 576))
-    lax.fori_loop(1, 4, block_states, 0)
+    pl.when(early)(lambda: project(192, 384))
+    pl.when(late)(lambda: project(448, 128))
+    for k in (1, 2, 3):
+        block_states(k, 0)
 
     t0, t1, t2, t3 = (tot[b : b + 1, :] for b in range(4))
     zero = jnp.zeros_like(t0)
@@ -494,47 +514,59 @@
     tot[1:2, :] = jnp.where(fl, t0, t2 + t3)
     tot[2:3, :] = jnp.where(fl, t0 + t1, t3)
     tot[3:4, :] = jnp.where(fl, t0 + t1 + t2, zero)
+    each_other(
+        lambda zt, xt: remote(
+            tot_b, gtot.at[s], t_send.at[0], t_recv.at[0], sp_0=zt, sp_1=xt
+        ).start()
+    )
+    gtot[s] = tot_b[...]
+    out_s = state_copies(ends_s, got_s, s_send, s_recv)
     for d, order in ((0, (0, 1, 2, 3)), (1, (3, 2, 1, 0))):
         for g in range(2):
-            ls = slice((d * 2 + g) * 256, (d * 2 + g + 1) * 256)
+            lg = d * 2 + g
+            ls = slice(lg * 256, (lg + 1) * 256)
             state = jnp.zeros((STATE, 256), F32)
             for b in order:
                 before[b, :, ls] = state.astype(BF16)
                 state = etot[b : b + 1, ls] * state + inc[b, :, ls]
             ends_s[:, ls] = state.astype(BF16)
-    out_s = state_copies(ends_s, got_s, s_send, s_recv)
-
-    def out_t(zt, xt):
-        return remote(tot_b, gtot.at[s], t_send.at[0], t_recv.at[0], sp_0=zt, sp_1=xt)
-
-    def send_s(zt, xt):
-        out_t(zt, xt).start()
-        out_s(zt, xt).start()
-
-    each_other(send_s)
+
+            def send_line(k, none, lg=lg):
+                turn = NZ // 2 + ((k + 1) // 2) * (1 - 2 * lax.rem(k, 2))
+                out_s(lax.rem(z + turn, NZ), lg).start()
+                return none
+
+            lax.fori_loop(0, NZ - 1, send_line, 0)
+
+            @pl.when(x != lg)
+            def _(lg=lg):
+                out_s(z, lg).start()
+
     got_s[s] = ends_s[rows(z * 16, 16), lanes(x * 256, 256)]
-    gtot[s] = tot_b[...]
-
-    for c in (slice(0, 256), slice(256, 512), slice(512, 768)):
+
+    sum_z(gpart, gz, gz_recv, gq)
+    send_xy(gq, gxy, gxy_send, gxy_recv)
+    def project_second(c):
         pre_b[:, c] = jnp.dot(
             hid[64:576, :], w_second[:, c], preferred_element_type=F32
         ).astype(BF16)
 
+    project_second(slice(0, 256))
+
     def within(k, none):
         b = block_of(k)
-        at_b = rows(b * 128, 128)
         at_k = rows(k * 128, 128)
         rb = conv_rows(pre_b[at_k, 0:256].astype(F32), read_taps, ROW).astype(BF16)
-        reads[at_b, :] = rb
-        cums = cum[at_b, :]
-        step = stp[at_b, :]
+        reads[at_k, :] = rb
+        cums = cum[at_k, :]
+        step = stp[at_k, :]
         cums_t = jnp.transpose(cums)
         step_t = jnp.transpose(step)
-        cdec[at_b, :] = jnp.exp(cums + tot[pl.ds(b, 1), :])
+        cdec[at_k, :] = jnp.exp(cums + tot[pl.ds(b, 1), :])
         grown = expand(jnp.exp(cums), spread[...])
         for g in range(2):
             r = rb[:, g * 128 : (g + 1) * 128]
-            affinity = dot_on(r, wri[at_b, g * 128 : (g + 1) * 128], 1, 1)
+            affinity = dot_on(r, wri[at_k, g * 128 : (g + 1) * 128], 1, 1)
             carried = jnp.zeros((128, 256), F32)
             for d in range(2):
                 ls = slice((d * 2 + g) * 256, (d * 2 + g + 1) * 256)
@@ -553,14 +585,14 @@
                     amount = jnp.where(col < row, sf, jnp.where(col > row, sb, sf + sb))
                     mixes.append((affinity * jnp.exp(exponent) * amount).astype(BF16))
                 ls = slice((g * 2 + q) * 128, (g * 2 + q + 1) * 128)
-                pair = val[at_b, ls]
+                pair = val[at_k, ls]
                 none16 = jnp.zeros_like(pair)
                 tall = jnp.concatenate(
                     [jnp.where(col < HEAD, pair, none16), jnp.where(col >= HEAD, pair, none16)],
                     axis=0,
                 )
                 got = jnp.dot(jnp.concatenate(mixes, axis=1), tall, preferred_element_type=F32)
-                local[at_b, ls] = got + carried[:, q * 128 : (q + 1) * 128]
+                local[at_k, ls] = got + carried[:, q * 128 : (q + 1) * 128]
         return none
 
     lax.fori_loop(0, 4, within, 0)
@@ -611,29 +643,33 @@
     start[rows(z * 16, 16), lanes(x * 256, 256)] = sent[s]
 
     def last_tables(k, none):
-        at_b = rows(block_of(k) * 128, 128)
-        grown_c[at_b, :] = expand(cdec[at_b, :], spread[...])
-        gates[at_b, :] = silu(pre_b[rows(k * 128, 128), 256:768].astype(F32))
+        at_k = rows(k * 128, 128)
+        grown_c[at_k, :] = expand(cdec[at_k, :], spread[...])
+        gates[at_k, :] = silu(pre_b[at_k, 256:768].astype(F32))
         return none
 
+    sum_xy(gq, gxy, gxy_recv, gf)
+    gather_z(gf, gmod, gg_send, gg_recv)
+    project_second(slice(256, 512))
+    project_second(slice(512, 768))
     lax.fori_loop(0, 4, last_tables, 0)
 
     got_all(got_s.at[pl.ds(0, NS - 1)], b_recv.at[0])
 
     half = w_out.shape[1] // 2
 
-    def make_inner(b):
-        at_b = rows(b * 128, 128)
+    def make_inner(slot):
+        at_k = slice(slot * 128, (slot + 1) * 128)
         for g in range(2):
-            r = reads[at_b, g * 128 : (g + 1) * 128]
+            r = reads[at_k, g * 128 : (g + 1) * 128]
             ch = slice(g * 256, (g + 1) * 256)
-            total = local[at_b, ch]
+            total = local[at_k, ch]
             for d in range(2):
                 ls = slice((d * 2 + g) * 256, (d * 2 + g + 1) * 256)
                 total = total + jnp.dot(r, start[:, ls], preferred_element_type=F32) * (
-                    grown_c[at_b, ls]
+                    grown_c[at_k, ls]
                 )
-            gated = total * gates[at_b, ch]
+            gated = total * gates[at_k, ch]
             power = jnp.mean(gated * gated, -1, keepdims=True)
             gains = jnp.concatenate(
                 [gain[pl.ds(y * 4 + g * 2, 1), :], gain[pl.ds(y * 4 + g * 2 + 1, 1), :]], axis=1
@@ -645,19 +681,19 @@
             inner[...], w_out[:, side * half : (side + 1) * half], preferred_element_type=F32
         ).astype(BF16)
 
-    make_inner(opposite)
+    make_inner(3)
     far[0] = product(0)
     far_r = remote(far.at[0], got_far.at[0], s1.at[0], r1.at[0], tp=right)
     far_r.start()
     far[1] = product(1)
     far_l = remote(far.at[1], got_far.at[1], s1.at[1], r1.at[1], tp=left)
     far_l.start()
-    make_inner(right)
+    make_inner(2)
     near_r[1] = product(1)
     raw_r = remote(near_r.at[1], got_r.at[1], s2.at[0], r2.at[0], tp=right)
     raw_r.start()
     near_r[0] = product(0)
-    make_inner(left)
+    make_inner(1)
     near_l[0] = product(0)
     raw_l = remote(near_l.at[0], got_l.at[0], s2.at[1], r2.at[1], tp=left)
     raw_l.start()
@@ -670,13 +706,17 @@
     near_l[1] = (near_l[1].astype(F32) + got_far[1].astype(F32)).astype(BF16)
     sum_l = remote(near_l.at[1], got_l.at[1], s2.at[3], r2.at[3], tp=left)
     sum_l.start()
-    make_inner(y)
+    make_inner(0)
     mine[0] = product(0)
     mine[1] = product(1)
 
+    got_all(gz, gg_recv.at[0])
     sent_all(zbuf, z_send.at[0])
     sent_all(xybuf.at[pl.ds(1, NX * NY - 1)], xy_send.at[0])
     sent_all(zbuf, g_send.at[0])
+    sent_all(gz, gz_send.at[0])
+    sent_all(gxy.at[pl.ds(1, NX * NY - 1)], gxy_send.at[0])
+    sent_all(gz, gg_send.at[0])
     sent_all(gtot.at[pl.ds(0, NS - 1)], t_send.at[0])
     for sem in (c_send, s_send, b_send):
         sent_all(got_s.at[pl.ds(0, NS - 1)], sem.at[0])
@@ -691,7 +731,7 @@
             mine[side].astype(F32) + got_r[side].astype(F32) + got_l[side].astype(F32)
         ).astype(BF16)
         own = gat[rows(y * 128, 128), cs]
-        out[:, cs] = (own.astype(F32) + mod[4:5, cs] * mixed.astype(F32)).astype(BF16)
+        out[:, cs] = (own.astype(F32) + gmod[:, cs] * mixed.astype(F32)).astype(BF16)
 
     raw_r.wait_recv()
     raw_l.wait_recv()
@@ -718,8 +758,10 @@
         out_specs=VMEM,
         scratch_shapes=copied
         + [
-            vm((8, width), F32), vm((NZ - 1, 8, 256), F32), vm((8, 256), F32),
-            vm((NX * NY, 8, 256), F32), vm((8, 256), F32), vm((8, width), F32),
+            vm((4, width), F32), vm((NZ - 1, 4, 256), F32), vm((4, 256), F32),
+            vm((NX * NY, 4, 256), F32), vm((4, 256), F32), vm((4, width), F32),
+            vm((1, width), F32), vm((NZ - 1, 1, 256), F32), vm((1, 256), F32),
+            vm((NX * NY, 1, 256), F32), vm((1, 256), F32), vm((1, width), F32),
             vm((tokens, width), BF16), vm((4 * HALO, width), BF16),
             vm((tokens + 4 * HALO, width), F32), vm((tokens + 4 * HALO, width), BF16),
             vm((tokens + 4 * HALO, 896), BF16), vm((tokens, 768), BF16),
@@ -736,7 +778,7 @@
             vm((128, 512), BF16), piece, piece, piece, piece, piece, piece, piece,
             dma((19,)),
         ]
-        + [dma((1,))] * 6
+        + [dma((1,))] * 12
         + [dma((6,))] * 2 + [dma((2,))] * 2 + [dma((2,))] * 2
         + [dma((1,))] * 8
         + [dma((2,)), dma((2,)), dma((4,)), dma((4,))],

time: 68 us -> 66.9 us (0.984)
  Pallas kernels: 67.1 us -> 65.7 us
    pallas_call x1, Pallas kernels: 67.1 us -> 65.7 us  [mixer_call(): pl.pallas_call(mixer_kernel, out_shape=pltpu.VMEM((128, width), BF16), in...]
where the time goes in v6:
time: 66.9 us; the launch traced here: 66.5 us
  Pallas kernels  65.7 us (98%)
  local copies, waits for them, and re-layouts  0.8 us (1%)
    pallas_call x1, Pallas kernels, mixer_call(): pl.pallas_call(mixer_kernel, out_shape=pltpu.VMEM((128, width), BF16), in...  65.7 us

profile of v6, /device:TPU:8, one launch (start us, length us, event | category | flops | bytes accessed | tf_op | source)
XLA Modules:
  0.0 66.5 jit_solution(14536291115925231423)
XLA Ops:
  0.0 65.7 %mixer.1 = bf16[128,2048]{1,0:T(8,128)(2,1)S(1)} custom-call(bf16[128,2048]{1,0:T(8,128)(2,1)} %bitcast.11, bf16[32,2048]{1,0:T(8,128)(2,1)} %bitcast.13, f32[16,128]{1,0:T(8,128)} %bitcast.15, f32[16,128]{1,0:T(8,128)} %bitcast.16, bf16[16,2048]{1,0:T(8,128)(2,1)} %shift_h.1, bf16[16,2048]{1,0:T(8,128)(2,1)} %scale_h.1, bf16[16,2048]{1,0:T(8,128)(2,1)} %gatem_h.1, ...), custom_call_target="tpu_custom_call" | custom-call | tf_op jit(solution)/shard_map/mixer/pallas_call | solution.py:754
  65.7 0.8 %copy.21 = bf16[1,128,2048]{2,1,0:T(8,128)(2,1)} copy(bf16[1,128,2048]{2,1,0:T(8,128)(2,1)S(1)} %bitcast.10) | data formatting | bytes 1048576

commit v7 on v6

--- a/solution.py
+++ b/solution.py
@@ -90,7 +90,12 @@
     shape = spread.shape
     row = lax.rem(lax.broadcasted_iota(jnp.int32, shape, 0), 128)
     col = lax.broadcasted_iota(jnp.int32, shape, 1)
-    spread[...] = jnp.where(row == col // HEAD, 1.0, 0.0).astype(BF16)
+    head = lax.rem(col // 256, 2) * 8 + (col // 512) * 4 + lax.rem(col, 256) // HEAD
+    spread[...] = jnp.where(row == head, 1.0, 0.0).astype(BF16)
+
+
+def both_ways(v):
+    return jnp.concatenate([v[:, 0:256], v[:, 0:256], v[:, 256:512], v[:, 256:512]], axis=1)
 
 
 def dot_on(a, b, ca, cb):
@@ -159,17 +164,20 @@
             start(z, xt)
 
     barrier = pltpu.get_barrier_semaphore()
-    each_other(
-        lambda zt, xt: pl.semaphore_signal(
-            barrier, inc=1, device_id={"sp_0": zt, "sp_1": xt}, device_id_type=MESH
-        )
-    )
+    nxt, prv = lax.rem(s + 1, NS), lax.rem(s + NS - 1, NS)
+
+    def greet(**where):
+        pl.semaphore_signal(barrier, inc=1, device_id=where, device_id_type=MESH)
+
+    for d in (4, 3, 5, 2, 6, 1, 7):
+        greet(sp_0=lax.rem(z + d, NZ))
     for dy in (2, 1, 3):
         for xt in xts:
-            pl.semaphore_signal(
-                barrier, inc=1, device_id={"sp_1": xt, "tp": lax.rem(y + dy, NY)},
-                device_id_type=MESH,
-            )
+            greet(sp_1=xt, tp=lax.rem(y + dy, NY))
+    for xt in xts[1:]:
+        greet(sp_1=xt)
+    greet(**at(nxt))
+    greet(**at(prv))
 
     for copy in fetch[:5]:
         copy.wait()
@@ -199,9 +207,7 @@
     def norm_ctx(base):
         nrm[pl.ds(512 + base, HALO), :] = normed_rows(ctx_ext[pl.ds(base, HALO), :])
 
-    pl.semaphore_wait(barrier, NS - 1 + NX * (NY - 1))
-
-    nxt, prv = lax.rem(s + 1, NS), lax.rem(s + NS - 1, NS)
+    pl.semaphore_wait(barrier, NZ - 1 + NX * NY - 1 + 2)
 
     def got_all(ref, recv):
         remote(ref, ref, recv, recv, **at(nxt)).wait_recv()
@@ -383,8 +389,7 @@
         return none
 
     def project(lo, count):
-        for c in range(4):
-            cs = slice(c * 256, min(c * 256 + 256, 896))
+        for cs in (slice(0, 512), slice(512, 896)):
             pre_a[lo : lo + count, cs] = jnp.dot(
                 hid[lo : lo + count, :], w_first[:, cs], preferred_element_type=F32
             ).astype(BF16)
@@ -420,12 +425,12 @@
     later, earlier = ctx_sum(c32 > r32), ctx_sum(c32 < r32)
     cweight = jnp.exp(jnp.where(forward_lane[0 : 2 * HALO], later, earlier)) * cstep
     cvf = cv.astype(F32)
-    cscaled = (jnp.concatenate([cvf, cvf], axis=1) * expand(cweight, spread[...])).astype(BF16)
+    cscaled = (both_ways(cvf) * expand(cweight, spread[...])).astype(BF16)
     for g in range(2):
-        wg = cw[:, g * 128 : (g + 1) * 128]
-        for d in range(2):
-            ls = slice((d * 2 + g) * 256, (d * 2 + g + 1) * 256)
-            ends_c[:, ls] = dot_on(wg, cscaled[:, ls], 0, 0).astype(BF16)
+        gs = slice(g * 512, (g + 1) * 512)
+        ends_c[:, gs] = dot_on(
+            cw[:, g * 128 : (g + 1) * 128], cscaled[:, gs], 0, 0
+        ).astype(BF16)
 
     def expand3(v):
         high = v.astype(BF16)
@@ -469,16 +474,10 @@
         stp[at_k, :] = step
         weight = jnp.exp(total - cums) * step
         vf = vb.astype(F32)
-        scaled = (jnp.concatenate([vf, vf], axis=1) * expand(weight, spread[...])).astype(BF16)
+        scaled = (both_ways(vf) * expand(weight, spread[...])).astype(BF16)
         for g in range(2):
-            fs = slice(g * 256, (g + 1) * 256)
-            bs = slice(512 + g * 256, 512 + (g + 1) * 256)
-            states = dot_on(
-                w[:, g * 128 : (g + 1) * 128],
-                jnp.concatenate([scaled[:, fs], scaled[:, bs]], axis=1), 0, 0,
-            )
-            inc[b, :, fs] = states[:, 0:256]
-            inc[b, :, bs] = states[:, 256:512]
+            gs = slice(g * 512, (g + 1) * 512)
+            inc[b, :, gs] = dot_on(w[:, g * 128 : (g + 1) * 128], scaled[:, gs], 0, 0)
         tot[pl.ds(b, 1), :] = total
         return none
 
@@ -521,9 +520,9 @@
     )
     gtot[s] = tot_b[...]
     out_s = state_copies(ends_s, got_s, s_send, s_recv)
-    for d, order in ((0, (0, 1, 2, 3)), (1, (3, 2, 1, 0))):
-        for g in range(2):
-            lg = d * 2 + g
+    for g in range(2):
+        for d, order in ((0, (0, 1, 2, 3)), (1, (3, 2, 1, 0))):
+            lg = g * 2 + d
             ls = slice(lg * 256, (lg + 1) * 256)
             state = jnp.zeros((STATE, 256), F32)
             for b in order:
@@ -567,12 +566,9 @@
         for g in range(2):
             r = rb[:, g * 128 : (g + 1) * 128]
             affinity = dot_on(r, wri[at_k, g * 128 : (g + 1) * 128], 1, 1)
-            carried = jnp.zeros((128, 256), F32)
-            for d in range(2):
-                ls = slice((d * 2 + g) * 256, (d * 2 + g + 1) * 256)
-                carried = carried + (
-                    jnp.dot(r, before[b, :, ls], preferred_element_type=F32) * grown[:, ls]
-                )
+            gs = slice(g * 512, (g + 1) * 512)
+            carried = jnp.dot(r, before[b, :, gs], preferred_element_type=F32) * grown[:, gs]
+            carried = carried[:, 0:256] + carried[:, 256:512]
             for q in range(2):
                 mixes = []
                 for h in (g * 4 + q * 2, g * 4 + q * 2 + 1):
@@ -597,7 +593,7 @@
 
     lax.fori_loop(0, 4, within, 0)
 
-    turned = x // 2
+    turned = lax.rem(x, 2)
 
     def order_of(k):
         return k + turned * (NS - 1 - 2 * k)
@@ -650,8 +646,7 @@
 
     sum_xy(gq, gxy, gxy_recv, gf)
     gather_z(gf, gmod, gg_send, gg_recv)
-    project_second(slice(256, 512))
-    project_second(slice(512, 768))
+    project_second(slice(256, 768))
     lax.fori_loop(0, 4, last_tables, 0)
 
     got_all(got_s.at[pl.ds(0, NS - 1)], b_recv.at[0])
@@ -663,12 +658,9 @@
         for g in range(2):
             r = reads[at_k, g * 128 : (g + 1) * 128]
             ch = slice(g * 256, (g + 1) * 256)
-            total = local[at_k, ch]
-            for d in range(2):
-                ls = slice((d * 2 + g) * 256, (d * 2 + g + 1) * 256)
-                total = total + jnp.dot(r, start[:, ls], preferred_element_type=F32) * (
-                    grown_c[at_k, ls]
-                )
+            gs = slice(g * 512, (g + 1) * 512)
+            more = jnp.dot(r, start[:, gs], preferred_element_type=F32) * grown_c[at_k, gs]
+            total = local[at_k, ch] + more[:, 0:256] + more[:, 256:512]
             gated = total * gates[at_k, ch]
             power = jnp.mean(gated * gated, -1, keepdims=True)
             gains = jnp.concatenate(
@@ -736,8 +728,8 @@
     raw_r.wait_recv()
     raw_l.wait_recv()
     sum_r.wait_recv()
+    close(0)
     sum_l.wait_recv()
-    close(0)
     close(1)
     for copy in (far_r, far_l, raw_r, raw_l, sum_r, sum_l):
         copy.wait_send()

time: 66.9 us -> 65.6 us (0.981)
  Pallas kernels: 65.7 us -> 63.9 us
    pallas_call x1, Pallas kernels: 65.7 us -> 63.9 us  [mixer_call(): pl.pallas_call(mixer_kernel, out_shape=pltpu.VMEM((128, width), BF16), in...]
where the time goes in v7:
time: 65.6 us; the launch traced here: 64.8 us
  Pallas kernels  63.9 us (97%)
  local copies, waits for them, and re-layouts  0.8 us (1%)
    pallas_call x1, Pallas kernels, mixer_call(): pl.pallas_call(mixer_kernel, out_shape=pltpu.VMEM((128, width), BF16), in...  63.9 us

profile of v7, /device:TPU:8, one launch (start us, length us, event | category | flops | bytes accessed | tf_op | source)
XLA Modules:
  0.0 64.8 jit_solution(13307348398871704898)
XLA Ops:
  0.0 63.9 %mixer.1 = bf16[128,2048]{1,0:T(8,128)(2,1)S(1)} custom-call(bf16[128,2048]{1,0:T(8,128)(2,1)} %bitcast.11, bf16[32,2048]{1,0:T(8,128)(2,1)} %bitcast.13, f32[16,128]{1,0:T(8,128)} %bitcast.15, f32[16,128]{1,0:T(8,128)} %bitcast.16, bf16[16,2048]{1,0:T(8,128)(2,1)} %shift_h.1, bf16[16,2048]{1,0:T(8,128)(2,1)} %scale_h.1, bf16[16,2048]{1,0:T(8,128)(2,1)} %gatem_h.1, ...), custom_call_target="tpu_custom_call" | custom-call | tf_op jit(solution)/shard_map/mixer/pallas_call | solution.py:746
  64.0 0.8 %copy.21 = bf16[1,128,2048]{2,1,0:T(8,128)(2,1)} copy(bf16[1,128,2048]{2,1,0:T(8,128)(2,1)S(1)} %bitcast.10) | data formatting | bytes 1048576

commit v8 on v7

--- a/solution.py
+++ b/solution.py
@@ -432,13 +432,6 @@
             cw[:, g * 128 : (g + 1) * 128], cscaled[:, gs], 0, 0
         ).astype(BF16)
 
-    def expand3(v):
-        high = v.astype(BF16)
-        rest = v - high.astype(F32)
-        return jnp.dot(high, spread[0:128, :], preferred_element_type=F32) + expand(
-            rest, spread[...]
-        )
-
     ctotal = jnp.exp(jnp.sum(cdecay, axis=0, keepdims=True))
 
     def state_copies(states, got, a_send, a_recv):
@@ -474,7 +467,12 @@
         stp[at_k, :] = step
         weight = jnp.exp(total - cums) * step
         vf = vb.astype(F32)
-        scaled = (both_ways(vf) * expand(weight, spread[...])).astype(BF16)
+        wide = expand(
+            jnp.concatenate([weight, jnp.broadcast_to(jnp.exp(total), (8, 128))], axis=0),
+            spread[...],
+        )
+        etot[pl.ds(b, 1), :] = wide[128:129]
+        scaled = (both_ways(vf) * wide[0:128]).astype(BF16)
         for g in range(2):
             gs = slice(g * 512, (g + 1) * 512)
             inc[b, :, gs] = dot_on(w[:, g * 128 : (g + 1) * 128], scaled[:, gs], 0, 0)
@@ -498,12 +496,6 @@
 
     t0, t1, t2, t3 = (tot[b : b + 1, :] for b in range(4))
     zero = jnp.zeros_like(t0)
-    etot[...] = expand3(
-        jnp.concatenate(
-            [jnp.exp(t0), jnp.exp(t1), jnp.exp(t2), jnp.exp(t3), jnp.exp(t0 + t1 + t2 + t3),
-             zero, zero, zero], axis=0,
-        )
-    )
     lane1 = lane[0:1]
     tot_b[...] = jnp.where(
         lane1 < 2 * heads, jnp.exp(t0 + t1 + t2 + t3),
@@ -674,12 +666,24 @@
         ).astype(BF16)
 
     make_inner(3)
-    far[0] = product(0)
-    far_r = remote(far.at[0], got_far.at[0], s1.at[0], r1.at[0], tp=right)
-    far_r.start()
-    far[1] = product(1)
-    far_l = remote(far.at[1], got_far.at[1], s1.at[1], r1.at[1], tp=left)
-    far_l.start()
+    quarter = half // 2
+    far_copies = []
+    for part in range(2):
+        for side in range(2):
+            cs = slice(part * quarter, (part + 1) * quarter)
+            far[side, :, cs] = jnp.dot(
+                inner[...],
+                w_out[:, side * half + part * quarter : side * half + (part + 1) * quarter],
+                preferred_element_type=F32,
+            ).astype(BF16)
+            piece = (side, slice(None), pl.ds(part * quarter, quarter))
+            far_copies.append(
+                remote(
+                    far.at[piece], got_far.at[piece], s1.at[part * 2 + side],
+                    r1.at[part * 2 + side], tp=right if side == 0 else left,
+                )
+            )
+            far_copies[-1].start()
     make_inner(2)
     near_r[1] = product(1)
     raw_r = remote(near_r.at[1], got_r.at[1], s2.at[0], r2.at[0], tp=right)
@@ -690,11 +694,13 @@
     raw_l = remote(near_l.at[0], got_l.at[0], s2.at[1], r2.at[1], tp=left)
     raw_l.start()
     near_l[1] = product(1)
-    far_r.wait_recv()
+    far_copies[0].wait_recv()
+    far_copies[2].wait_recv()
     near_r[0] = (near_r[0].astype(F32) + got_far[0].astype(F32)).astype(BF16)
     sum_r = remote(near_r.at[0], got_r.at[0], s2.at[2], r2.at[2], tp=right)
     sum_r.start()
-    far_l.wait_recv()
+    far_copies[1].wait_recv()
+    far_copies[3].wait_recv()
     near_l[1] = (near_l[1].astype(F32) + got_far[1].astype(F32)).astype(BF16)
     sum_l = remote(near_l.at[1], got_l.at[1], s2.at[3], r2.at[3], tp=left)
     sum_l.start()
@@ -731,7 +737,7 @@
     close(0)
     sum_l.wait_recv()
     close(1)
-    for copy in (far_r, far_l, raw_r, raw_l, sum_r, sum_l):
+    for copy in (*far_copies, raw_r, raw_l, sum_r, sum_l):
         copy.wait_send()
 
 
@@ -773,7 +779,7 @@
         + [dma((1,))] * 12
         + [dma((6,))] * 2 + [dma((2,))] * 2 + [dma((2,))] * 2
         + [dma((1,))] * 8
-        + [dma((2,)), dma((2,)), dma((4,)), dma((4,))],
+        + [dma((4,)), dma((4,)), dma((4,)), dma((4,))],
         compiler_params=pltpu.CompilerParams(
             collective_id=0, has_side_effects=True, vmem_limit_bytes=56 << 20
         ),

time: 65.6 us -> 65.5 us (level)
  no operation moved by 1% of the time
where the time goes in v8:
time: 65.5 us; the launch traced here: 64.7 us
  Pallas kernels  63.9 us (98%)
  local copies, waits for them, and re-layouts  0.8 us (1%)
    pallas_call x1, Pallas kernels, mixer_call(): pl.pallas_call(mixer_kernel, out_shape=pltpu.VMEM((128, width), BF16), in...  63.9 us

profile of v8, /device:TPU:8, one launch (start us, length us, event | category | flops | bytes accessed | tf_op | source)
XLA Modules:
  0.0 64.7 jit_solution(14599826607527794208)
XLA Ops:
  0.0 63.9 %mixer.1 = bf16[128,2048]{1,0:T(8,128)(2,1)S(1)} custom-call(bf16[128,2048]{1,0:T(8,128)(2,1)} %bitcast.11, bf16[32,2048]{1,0:T(8,128)(2,1)} %bitcast.13, f32[16,128]{1,0:T(8,128)} %bitcast.15, f32[16,128]{1,0:T(8,128)} %bitcast.16, bf16[16,2048]{1,0:T(8,128)(2,1)} %shift_h.1, bf16[16,2048]{1,0:T(8,128)(2,1)} %scale_h.1, bf16[16,2048]{1,0:T(8,128)(2,1)} %gatem_h.1, ...), custom_call_target="tpu_custom_call" | custom-call | tf_op jit(solution)/shard_map/mixer/pallas_call | solution.py:752
  63.9 0.8 %copy.21 = bf16[1,128,2048]{2,1,0:T(8,128)(2,1)} copy(bf16[1,128,2048]{2,1,0:T(8,128)(2,1)S(1)} %bitcast.10) | data formatting | bytes 1048576
